TPU v7x, 32 devices: a whole 2x2x4 slice. The times are simulated.
32 devices in a mesh: sp: 4 (over z), fs: 4 (over y, x), tp: 2 (over core).
Axes of the slice: x: 2, y: 2, z: 4, core: 2. Of those that a mesh axis runs over, the one named last changes fastest.
Arguments:
- tokens: bfloat16 [4, 1024, 2048], P('fs', 'sp'), may hold values from -6 to 6
- norm_gain: float32 [2048], replicated, may hold values from 0.1 to 1.9
- pool_input: bfloat16 [2048, 2048], P(('sp', 'fs'), 'tp'), may hold values from -0.125 to 0.125
- query_weight: bfloat16 [2048, 2048], P(('sp', 'fs'), 'tp'), may hold values from -20 to 20
- key_weight: bfloat16 [2048, 2048], P(('sp', 'fs'), 'tp'), may hold values from -1 to 1
- value_weight: bfloat16 [2048, 2048], P(('sp', 'fs'), 'tp'), may hold values from -0.125 to 0.125
- pool_map: bfloat16 [8, 256, 256], P('tp'), may hold values from -0.375 to 0.375
- pool_scale: float32 [2048], P('tp'), may hold values from 0.1 to 1.9
- head_gain: float32 [256], replicated, may hold values from 0.1 to 1.9
- diff_lambda: float32 [8], replicated, may hold values from 0.3 to 0.8
- out_pool: bfloat16 [2048, 2048], P('tp', ('sp', 'fs')), may hold values from -0.09375 to 0.09375
- out_heads: bfloat16 [2048, 2048], P('tp', ('sp', 'fs')), may hold values from -0.09375 to 0.09375
Outputs:
- layer_out: bfloat16 [4, 1024, 2048], P('fs', 'sp', 'tp')
All inputs are finite; a program needn't handle non-finite values.
Results may differ from a plain program's by a relative error of at most 0.018.
Values may be sent and summed in bfloat16 or wider, within the bound.
No kernel may reach another device: no remote copies, remote signals or barrier semaphores. Data moves between devices by JAX's collectives and lax.ppermute only.
A program may use at most 64 MiB of HBM per device.

v0:
```python
import math

import jax
import jax.numpy as jnp
from jax import lax
from jax.sharding import PartitionSpec as P

HEAD_DIM = 128
GROUP_DIM = 256


THETA = 500000.0
HEAD_SCALE = 0.8
NORM_EPS = 1e-06
HEAD_EPS = 1e-05


def from_behind(value, axis, steps):
    count = lax.axis_size(axis)
    first, last = (max(0, -steps), min(count, count - steps))
    return lax.ppermute(value, axis, [(source, source + steps) for source in range(first, last)])


def rotate(tensor, positions):
    half = HEAD_DIM // 2
    freqs = 1.0 / THETA ** (jnp.arange(half, dtype=jnp.float32) * 2.0 / HEAD_DIM)
    angles = positions[:, None] * freqs[None, :]
    cosine = jnp.cos(angles)[:, None, None, :]
    sine = jnp.sin(angles)[:, None, None, :]
    floated = tensor.astype(jnp.float32)
    first = floated[..., :half]
    second = floated[..., half:]
    turned = jnp.concatenate([first * cosine - second * sine, second * cosine + first * sine], -1)
    return turned.astype(jnp.bfloat16)


def local(
    tokens,
    norm_gain,
    pool_input,
    query_weight,
    key_weight,
    value_weight,
    pool_map,
    pool_scale,
    head_gain,
    diff_lambda,
    out_pool,
    out_heads,
):
    out_local = jnp.concatenate([out_pool, out_heads], 0)
    row_count = tokens.shape[1]
    floated = tokens[0].astype(jnp.float32)
    normed = (
        floated * lax.rsqrt(jnp.mean(floated * floated, -1, keepdims=True) + NORM_EPS) * norm_gain
    ).astype(jnp.bfloat16)
    fragments = (
        lax.all_gather(pool_input, ("sp", "fs"), axis=0, tiled=True),
        lax.all_gather(query_weight, ("sp", "fs"), axis=0, tiled=True),
        lax.all_gather(key_weight, ("sp", "fs"), axis=0, tiled=True),
        lax.all_gather(value_weight, ("sp", "fs"), axis=0, tiled=True),
    )
    projected = tuple(
        (jnp.dot(normed, fragment, preferred_element_type=jnp.float32) for fragment in fragments)
    )
    pool_in, queries, keys_flat, values_flat = [
        product.astype(jnp.bfloat16) for product in projected
    ]
    head_count = values_flat.shape[1] // (2 * HEAD_DIM)
    tp_index = lax.axis_index("tp")
    sp_index = lax.axis_index("sp")
    query_pos = sp_index * row_count + jnp.arange(row_count, dtype=jnp.int32)
    positions = query_pos.astype(jnp.float32)
    queries = rotate(queries.reshape(row_count, head_count, 2, HEAD_DIM), positions)
    keys_flat = rotate(keys_flat.reshape(row_count, head_count, 2, HEAD_DIM), positions).reshape(
        row_count, head_count * 2 * HEAD_DIM
    )
    lambdas = lax.dynamic_slice_in_dim(diff_lambda, tp_index * head_count, head_count, 0)

    def online_step(state, key_rows, value_rows, key_offset):
        largest, summed, accum = state
        width = key_rows.shape[0]
        shaped = key_rows.reshape(width, head_count, 2, HEAD_DIM)
        scores = jnp.einsum(
            "qhcd,khcd->chqk", queries, shaped, preferred_element_type=jnp.float32
        ) * HEAD_DIM ** (-0.5)
        key_pos = key_offset + jnp.arange(width, dtype=jnp.int32)
        scores = jnp.where(query_pos[:, None] >= key_pos[None, :], scores, -jnp.inf)
        newest = jnp.maximum(largest, jnp.max(scores, -1))
        anchor = jnp.where(jnp.isfinite(newest), newest, 0.0)
        rescale = jnp.exp(largest - anchor)
        expons = jnp.exp(scores - anchor[..., None])
        summed = summed * rescale + jnp.sum(expons, -1)
        value_shaped = value_rows.reshape(width, head_count, 2 * HEAD_DIM)
        added = jnp.einsum(
            "chqk,khe->chqe",
            expons.astype(jnp.bfloat16),
            value_shaped,
            preferred_element_type=jnp.float32,
        )
        accum = accum * rescale[..., None] + added
        return (newest, summed, accum)

    start_state = (
        jnp.full((2, head_count, row_count), -jnp.inf, jnp.float32),
        jnp.zeros((2, head_count, row_count), jnp.float32),
        jnp.zeros((2, head_count, row_count, 2 * HEAD_DIM), jnp.float32),
    )
    fragments = (
        lax.all_gather(keys_flat, "sp", axis=0, tiled=True),
        lax.all_gather(values_flat, "sp", axis=0, tiled=True),
    )
    span = math.gcd(fragments[0].shape[0], 1024)

    def inner_step(index, inner_state):
        key_rows = lax.dynamic_slice_in_dim(fragments[0], index * span, span, 0)
        value_rows = lax.dynamic_slice_in_dim(fragments[1], index * span, span, 0)
        return online_step(inner_state, key_rows, value_rows, index * span)

    final_state = lax.fori_loop(0, fragments[0].shape[0] // span, inner_step, start_state)
    summed_final = final_state[1]
    accum_final = final_state[2]
    heads_raw = (
        accum_final[0] / summed_final[0][..., None]
        - lambdas[:, None, None] * accum_final[1] / summed_final[1][..., None]
    )
    heads_raw = jnp.moveaxis(heads_raw, 0, 1)
    attn = (
        (
            heads_raw
            * lax.rsqrt(jnp.mean(heads_raw * heads_raw, -1, keepdims=True) + HEAD_EPS)
            * head_gain
            * HEAD_SCALE
        )
        .astype(jnp.bfloat16)
        .reshape(row_count, head_count * 2 * HEAD_DIM)
    )
    reach = 15
    rim_rows = from_behind(pool_in[row_count - reach :], "sp", 1)
    extended = jnp.concatenate([rim_rows, pool_in], 0).astype(jnp.float32)
    pair_sums = extended[1:] + extended[:-1]
    quad_sums = pair_sums[2:] + pair_sums[:-2]
    octet_sums = quad_sums[4:] + quad_sums[:-4]
    sixteen_sums = octet_sums[8:] + octet_sums[:-8]
    group_count = pool_in.shape[1] // GROUP_DIM
    stacked = jnp.stack(
        [
            pair_sums[14 : 14 + row_count],
            quad_sums[12 : 12 + row_count],
            octet_sums[8 : 8 + row_count],
            sixteen_sums,
        ],
        0,
    ).reshape(4, row_count, group_count, GROUP_DIM)
    levels = (tp_index * group_count + jnp.arange(group_count, dtype=jnp.int32)) % 4
    picked = jnp.sum(
        jnp.where(
            levels[None, None, :, None] == jnp.arange(4, dtype=jnp.int32)[:, None, None, None],
            stacked,
            0.0,
        ),
        0,
    )
    windows = 2 ** (1 + levels)
    counts = jnp.minimum(query_pos[:, None] + 1, windows[None, :]).astype(jnp.float32)
    window_mean = picked / counts[:, :, None]
    grouped = pool_in.reshape(row_count, group_count, GROUP_DIM).astype(jnp.float32)
    pool_mixed = (window_mean - grouped).astype(jnp.bfloat16)
    pooled = (
        (
            jnp.einsum("tgc,gce->tge", pool_mixed, pool_map, preferred_element_type=jnp.float32)
            * pool_scale.reshape(group_count, GROUP_DIM)
        )
        .astype(jnp.bfloat16)
        .reshape(row_count, group_count * GROUP_DIM)
    )
    branches = jnp.concatenate([pooled, attn], 1)
    partial_value = jnp.dot(
        branches,
        lax.all_gather(out_local, ("sp", "fs"), axis=1, tiled=True),
        preferred_element_type=jnp.float32,
    )
    layer_out = lax.psum_scatter(
        partial_value.astype(jnp.bfloat16), "tp", scatter_dimension=1, tiled=True
    )
    return layer_out[None]


def solution(mesh):
    placed = (
        P("fs", "sp", None),
        P(),
        P(("sp", "fs"), "tp"),
        P(("sp", "fs"), "tp"),
        P(("sp", "fs"), "tp"),
        P(("sp", "fs"), "tp"),
        P("tp", None, None),
        P("tp"),
        P(),
        P(),
        P("tp", ("sp", "fs")),
        P("tp", ("sp", "fs")),
    )
    return jax.shard_map(
        local, mesh=mesh, in_specs=placed, out_specs=P("fs", "sp", "tp"), check_vma=False
    )
```

profile of v0, /device:TPU:0, one launch (start us, length us, event | category | flops | bytes accessed | tf_op | source)
XLA Modules:
  0.0 574.7 jit_solution(961941928835282613)
XLA Ops:
  11.5 77.0 %all-gather.10.cloned.1.call-done = bf16[2048,1024]{1,0:T(8,128)(2,1)} async-done(((bf16[128,1024]{1,0:T(8,128)(2,1)}), bf16[2048,1024]{1,0:T(8,128)(2,1)}) %all-gather.10.cloned.1.call-update) | async-done | bytes 4194320 | tf_op jit(solution)/shard_map/all_gather | solution.py:59
  88.5 4.5 fusion.15
  92.9 2.1 reshape.246
  95.0 70.4 %all-gather.12.cloned.1.call-done = bf16[2048,1024]{1,0:T(8,128)(2,1)} async-done(((bf16[128,1024]{1,0:T(8,128)(2,1)}), bf16[2048,1024]{1,0:T(8,128)(2,1)}) %all-gather.12.cloned.1.call-update) | async-done | bytes 4194320 | tf_op jit(solution)/shard_map/all_gather | solution.py:60
  165.4 4.5 fusion.14
  172.0 2.9 fusion.41
  178.0 64.5 %all-gather.16.cloned.1.call-done = bf16[2048,1024]{1,0:T(8,128)(2,1)} async-done(((bf16[128,1024]{1,0:T(8,128)(2,1)}), bf16[2048,1024]{1,0:T(8,128)(2,1)}) %all-gather.16.cloned.1.call-update) | async-done | bytes 4194320 | tf_op jit(solution)/shard_map/all_gather | solution.py:61
  242.4 4.3 convolution_convert_fusion.1
  248.1 71.2 %all-gather.8.cloned.1.call-done = bf16[2048,1024]{1,0:T(8,128)(2,1)} async-done(((bf16[128,1024]{1,0:T(8,128)(2,1)}), bf16[2048,1024]{1,0:T(8,128)(2,1)}) %all-gather.8.cloned.1.call-update) | async-done | bytes 4194320 | tf_op jit(solution)/shard_map/all_gather | solution.py:58
  319.3 3.5 convolution_convert_fusion.4
  322.8 3.6 collective-permute-start
  331.5 2.7 stack.17
  334.2 2.7 stack.18
  336.9 2.7 stack.16
  341.1 3.1 fusion.3
  345.8 19.8 %all-gather.14.cloned.1.call-done = bf16[1024,1024]{0,1:T(8,128)(2,1)} async-done(((bf16[256,1024]{0,1:T(8,128)(2,1)}), bf16[1024,1024]{0,1:T(8,128)(2,1)}) %all-gather.14.cloned.1.call-update) | async-done | bytes 2097168 | tf_op jit(solution)/shard_map/all_gather | solution.py:110
  365.6 3.6 fusion
  369.2 3.7 fusion.2
  372.9 38.0 %all-gather.18.cloned.1.call-done = bf16[1024,1024]{1,0:T(8,128)(2,1)} async-done(((bf16[256,1024]{1,0:T(8,128)(2,1)}), bf16[1024,1024]{1,0:T(8,128)(2,1)}) %all-gather.18.cloned.1.call-update) | async-done | bytes 2097168 | tf_op jit(solution)/shard_map/all_gather | solution.py:111
  410.9 2.9 copy.64
  413.8 3.5 bitcast_add_fusion
  418.1 136.2 %all-gather.20.cloned.1.call-done = bf16[2048,2048]{1,0:T(8,128)(2,1)} async-done(((bf16[2048,128]{1,0:T(8,128)(2,1)}), bf16[2048,2048]{1,0:T(8,128)(2,1)}) %all-gather.20.cloned.1.call-update) | async-done | bytes 8388624 | tf_op jit(solution)/shard_map/all_gather | solution.py:180
  554.3 6.8 %convolution_convert_fusion = bf16[256,2048]{1,0:T(8,128)(2,1)} fusion(bf16[2048,2048]{1,0:T(8,128)(2,1)} %all-gather.20.cloned.1.call-done, bf16[256,1024]{0,1:T(8,128)(2,1)S(1)} %bitcast.59, bf16[256,1024]{0,1:T(8,128)(2,1)S(1)} %bitcast.60), kind=kOutput, calls=%fused_computation.11 | convolution fusion | flops 2150105088 | bytes 10485760 | tf_op jit(solution)/shard_map/dot_general | solution.py:178
  561.1 6.7 %reduce-scatter.2.cloned.1.call-done = bf16[256,1024]{1,0:T(8,128)(2,1)} async-done(((bf16[256,2048]{1,0:T(8,128)(2,1)}), bf16[256,1024]{1,0:T(8,128)(2,1)}) %reduce-scatter.2.cloned.1.call-update) | async-done | bytes 524304 | tf_op jit(solution)/shard_map/reduce_scatter | solution.py:183
  (80 shorter events, 20.3 us)
Async XLA Ops:
  6.5 338.1 %copy-start = (bf16[4,256,256]{2,1,0:T(8,128)(2,1)S(1)}, bf16[4,256,256]{2,1,0:T(8,128)(2,1)}, u32[]{:S(2)}) copy-start(bf16[4,256,256]{2,1,0:T(8,128)(2,1)} %param.18) | copy-start | bytes 1572868
  6.5 81.9 %copy-start.3 = (bf16[1,256,2048]{2,1,0:T(8,128)(2,1)S(1)}, bf16[1,256,2048]{2,1,0:T(8,128)(2,1)}, u32[]{:S(2)}) copy-start(bf16[1,256,2048]{2,1,0:T(8,128)(2,1)} %param.12) | copy-start | bytes 3145732
  6.5 81.9 %copy-start.10 = (f32[2048]{0:T(1024)S(1)}, f32[2048]{0:T(1024)}, u32[]{:S(2)}) copy-start(f32[2048]{0:T(1024)} %param.13) | copy-start | bytes 24580
  6.5 81.9 %all-gather.10.cloned.1.call-start = ((), (), s32[]{:S(2)}) async-start(), calls=%async_computation.2 | async-start | bytes 4456448 | tf_op jit(solution)/shard_map/all_gather | solution.py:59
  7.3 158.2 %all-gather.12.cloned.1.call-start = ((), (), s32[]{:S(2)}) async-start(), calls=%async_computation.3 | async-start | bytes 4456448 | tf_op jit(solution)/shard_map/all_gather | solution.py:60
  8.0 234.4 %all-gather.16.cloned.1.call-start = ((), (), s32[]{:S(2)}) async-start(), calls=%async_computation.5 | async-start | bytes 4456448 | tf_op jit(solution)/shard_map/all_gather | solution.py:61
  8.7 310.5 %all-gather.8.cloned.1.call-start = ((), (), s32[]{:S(2)}) async-start(), calls=%async_computation.1 | async-start | bytes 4456448 | tf_op jit(solution)/shard_map/all_gather | solution.py:58
  9.3 356.3 %all-gather.14.cloned.1.call-start = ((), (), s32[]{:S(2)}) async-start(), calls=%async_computation.4 | async-start | bytes 2621440 | tf_op jit(solution)/shard_map/all_gather | solution.py:110
  176.5 65.9 %copy-start.4 = (bf16[1,256,2048]{2,1,0:T(8,128)(2,1)S(1)}, bf16[1,256,2048]{2,1,0:T(8,128)(2,1)}, u32[]{:S(2)}) copy-start(bf16[1,256,2048]{2,1,0:T(8,128)(2,1)} %param.12) | copy-start | bytes 3145732
  177.9 68.9 %copy-start.6 = (bf16[1024,128]{1,0:T(8,128)(2,1)S(1)}, bf16[1024,128]{1,0:T(8,128)(2,1)}, u32[]{:S(2)}) copy-start(bf16[1024,128]{1,0:T(8,128)(2,1)} %param.23) | copy-start | bytes 786436
  177.9 68.9 %copy-start.7 = (bf16[1024,128]{1,0:T(8,128)(2,1)S(1)}, bf16[1024,128]{1,0:T(8,128)(2,1)}, u32[]{:S(2)}) copy-start(bf16[1024,128]{1,0:T(8,128)(2,1)} %param.22) | copy-start | bytes 786436
  177.9 233.0 %all-gather.18.cloned.1.call-start = ((), (), s32[]{:S(2)}) async-start(), calls=%async_computation.6 | async-start | bytes 2621440 | tf_op jit(solution)/shard_map/all_gather | solution.py:111
  246.8 72.5 %copy-start.5 = (bf16[1,256,2048]{2,1,0:T(8,128)(2,1)S(1)}, bf16[1,256,2048]{2,1,0:T(8,128)(2,1)}, u32[]{:S(2)}) copy-start(bf16[1,256,2048]{2,1,0:T(8,128)(2,1)} %param.12) | copy-start | bytes 3145732
  246.8 307.5 %all-gather.20.cloned.1.call-start = ((), (), s32[]{:S(2)}) async-start(), calls=%async_computation.7 | async-start | bytes 8912896 | tf_op jit(solution)/shard_map/all_gather | solution.py:180
  247.7 320.1 %reduce-scatter.2.cloned.1.call-start = ((), (), s32[]{:S(2)}) async-start(), calls=%async_computation.8 | async-start | bytes 1572864 | tf_op jit(solution)/shard_map/reduce_scatter | solution.py:183
  248.1 78.4 %copy-start.8 = (f32[1024]{0:T(1024)S(1)}, f32[1024]{0:T(1024)}, u32[]{:S(2)}) copy-start(f32[1024]{0:T(1024)} %param.19) | copy-start | bytes 12292
  248.1 78.5 %copy-start.11 = (f32[8]{0:T(128)S(1)}, f32[8]{0:T(128)}, u32[]{:S(2)}) copy-start(f32[8]{0:T(128)} %param.21) | copy-start | bytes 100
  322.8 5.0 collective-permute-start
  344.2 21.4 %copy-start.2 = (bf16[256,4,2,64]{3,0,1,2:T(8,128)(2,1)S(1)}, bf16[256,4,2,64]{3,0,1,2:T(8,128)(2,1)}, u32[]{:S(2)}) copy-start(bf16[256,4,2,64]{3,0,1,2:T(8,128)(2,1)} %get-tuple-element.26) | copy-start | bytes 786436
  417.2 0.7 copy-start.9
  417.3 137.0 %copy-start.12 = (bf16[4,256,256]{1,2,0:T(8,128)(2,1)S(1)}, bf16[4,256,256]{1,2,0:T(8,128)(2,1)}, u32[]{:S(2)}) copy-start(bf16[4,256,256]{1,2,0:T(8,128)(2,1)} %fusion.13) | copy-start | bytes 1572868
  554.3 13.6 %copy-start.1 = (bf16[4,256,256]{2,1,0:T(8,128)(2,1)S(1)}, bf16[4,256,256]{2,1,0:T(8,128)(2,1)}, u32[]{:S(2)}) copy-start(bf16[4,256,256]{2,1,0:T(8,128)(2,1)} %param.18) | copy-start | bytes 1572868
Sparse Core Ops, SparseCore 0:
  10.1 78.3 all-gather.9
  91.2 74.1 all-gather.11
  168.2 74.1 all-gather.15
  245.1 74.1 all-gather.7
  320.7 44.8 all-gather.13
  367.0 43.8 all-gather.17
  413.6 140.6 all-gather.19
  561.2 6.5 reduce-scatter.1
where the time goes:
time: 575 us
  waiting for transfers between devices  487 us (85%)
  matrix products  31.8 us (6%)
  local copies, waits for them, and re-layouts  23 us (4%)
  other arithmetic  15.2 us (3%)
  between operations  13.8 us (2%)
    all_gather x1, waiting for transfers between devices, local(): lax.all_gather(out_local, ('sp', 'fs'), axis=1, tiled=True)  136 us
    all_gather x1, waiting for transfers between devices, local(): lax.all_gather(query_weight, ('sp', 'fs'), axis=0, tiled=True)  77 us
    all_gather x1, waiting for transfers between devices, local(): lax.all_gather(pool_input, ('sp', 'fs'), axis=0, tiled=True)  71.2 us
    all_gather x1, waiting for transfers between devices, local(): lax.all_gather(key_weight, ('sp', 'fs'), axis=0, tiled=True)  70.4 us
    all_gather x1, waiting for transfers between devices, local(): lax.all_gather(value_weight, ('sp', 'fs'), axis=0, tiled=True)  64.5 us
    all_gather x1, waiting for transfers between devices, local(): lax.all_gather(values_flat, 'sp', axis=0, tiled=True)  38 us
    all_gather x1, waiting for transfers between devices, local(): lax.all_gather(keys_flat, 'sp', axis=0, tiled=True)  19.8 us
    dot_general x4, matrix products, local(): jnp.dot(normed, fragment, preferred_element_type=jnp.float32)  16.7 us
  transfers between devices with their start and end apart: 9, of which 9 were waited for; matrix products, arithmetic and copies ran while one was open for 11% of the time, Pallas kernels for 0%

commit v1 on v0

--- a/solution.py
+++ b/solution.py
@@ -1,8 +1,11 @@
+import functools
 import math
 
 import jax
 import jax.numpy as jnp
 from jax import lax
+from jax.experimental import pallas as pl
+from jax.experimental.pallas import tpu as pltpu
 from jax.sharding import PartitionSpec as P
 
 HEAD_DIM = 128
@@ -186,6 +189,228 @@
     return layer_out[None]
 
 
+def mix_kernel(meta_ref, proj_ref, cos_ref, sin_ref, map_ref, scale_ref, gain_ref, lam_ref, out_ref, keys_ref):
+    rows = out_ref.shape[0]
+    length = proj_ref.shape[0]
+    width = 2 * HEAD_DIM
+    step = pl.program_id(0)
+    first_pos = meta_ref[0]
+    level = meta_ref[1]
+
+    def turned(raw, cosine, sine):
+        raw = raw.astype(jnp.float32)
+        return (raw * cosine + pltpu.roll(raw, HEAD_DIM // 2, 1) * sine).astype(jnp.bfloat16)
+
+    @pl.when(step == 0)
+    def _():
+        for m in range(2):
+            begin = GROUP_DIM + width + m * HEAD_DIM
+            keys_ref[:, m * HEAD_DIM : (m + 1) * HEAD_DIM] = turned(
+                proj_ref[:, begin : begin + HEAD_DIM], cos_ref[...], sin_ref[...]
+            )
+
+    base = pl.multiple_of(step * rows, rows)
+    mine = pl.ds(base, rows)
+    start_pos = lax.rem(first_pos + base, length)
+    key_index = lax.broadcasted_iota(jnp.int32, (rows, length), 1)
+    key_pos = lax.rem(key_index + first_pos, length)
+    query_pos = start_pos + lax.broadcasted_iota(jnp.int32, (rows, length), 0)
+    allowed = query_pos >= key_pos
+    value = proj_ref[:, GROUP_DIM + 2 * width : GROUP_DIM + 3 * width]
+    halves = []
+    for m in range(2):
+        begin = GROUP_DIM + m * HEAD_DIM
+        query = turned(proj_ref[mine, begin : begin + HEAD_DIM], cos_ref[mine, :], sin_ref[mine, :])
+        scores = lax.dot_general(
+            query,
+            keys_ref[:, m * HEAD_DIM : (m + 1) * HEAD_DIM],
+            (((1,), (1,)), ((), ())),
+            preferred_element_type=jnp.float32,
+        ) * HEAD_DIM ** (-0.5)
+        scores = jnp.where(allowed, scores, -jnp.inf)
+        largest = jnp.max(scores, -1, keepdims=True)
+        expons = jnp.exp(scores - largest)
+        total = jnp.sum(expons, -1, keepdims=True)
+        summed = jnp.dot(expons.astype(jnp.bfloat16), value, preferred_element_type=jnp.float32)
+        halves.append(summed / total)
+    raw = halves[0] - lam_ref[0] * halves[1]
+    attn = (
+        raw
+        * lax.rsqrt(jnp.mean(raw * raw, -1, keepdims=True) + HEAD_EPS)
+        * gain_ref[...]
+        * HEAD_SCALE
+    ).astype(jnp.bfloat16)
+    out_ref[:, GROUP_DIM:] = attn
+
+    reach = 16
+    before = pl.multiple_of(lax.rem(base + length - reach, length), reach)
+    pos = start_pos - reach + lax.broadcasted_iota(jnp.int32, (rows + reach, GROUP_DIM), 0)
+    flat = jnp.concatenate(
+        [proj_ref[pl.ds(before, reach), :GROUP_DIM], proj_ref[mine, :GROUP_DIM]], 0
+    ).astype(jnp.float32)
+    flat = jnp.where(pos >= 0, flat, 0.0)
+    sums = flat
+    picked = jnp.zeros((rows, GROUP_DIM), jnp.float32)
+    for power in range(4):
+        sums = sums + pltpu.roll(sums, 2**power, 0)
+        picked = jnp.where(level == power, sums[reach:], picked)
+    window = lax.shift_left(jnp.int32(2), level)
+    own_pos = pos[reach:]
+    counts = jnp.minimum(own_pos + 1, window).astype(jnp.float32)
+    mixed = (picked / counts - flat[reach:]).astype(jnp.bfloat16)
+    pooled = jnp.dot(mixed, map_ref[...], preferred_element_type=jnp.float32) * scale_ref[...]
+    out_ref[:, :GROUP_DIM] = pooled.astype(jnp.bfloat16)
+
+
+def mix(meta, proj, cosine, sine, pool_map, pool_scale, head_gain, lam, blocks):
+    length = proj.shape[0]
+    rows = length // blocks
+    whole = lambda i, *_: (0, 0)
+    return pl.pallas_call(
+        mix_kernel,
+        out_shape=jax.ShapeDtypeStruct((length, GROUP_DIM + 2 * HEAD_DIM), jnp.bfloat16),
+        grid_spec=pltpu.PrefetchScalarGridSpec(
+            num_scalar_prefetch=1,
+            grid=(blocks,),
+            in_specs=[
+                pl.BlockSpec(proj.shape, whole),
+                pl.BlockSpec(cosine.shape, whole),
+                pl.BlockSpec(sine.shape, whole),
+                pl.BlockSpec(pool_map.shape, whole),
+                pl.BlockSpec(pool_scale.shape, whole),
+                pl.BlockSpec(head_gain.shape, whole),
+                pl.BlockSpec(memory_space=pltpu.SMEM),
+            ],
+            out_specs=pl.BlockSpec((rows, GROUP_DIM + 2 * HEAD_DIM), lambda i, *_: (i, 0)),
+            scratch_shapes=[pltpu.VMEM((length, 2 * HEAD_DIM), jnp.bfloat16)],
+        ),
+        compiler_params=pltpu.CompilerParams(dimension_semantics=("arbitrary",)),
+        cost_estimate=pl.CostEstimate(
+            flops=8 * length * length * HEAD_DIM, bytes_accessed=3 * proj.size, transcendentals=2 * length * length
+        ),
+        name="mix",
+    )(meta, proj, cosine, sine, pool_map, pool_scale, head_gain, lam)
+
+
+def fold_rows(value):
+    return value.reshape(-1, value.shape[-1])
+
+
+def swap(value, axis, bits):
+    return lax.ppermute(value, axis, [(i, i ^ bits) for i in range(lax.axis_size(axis))])
+
+
+def shift(value, axis, up, sources):
+    step = 1 if up else -1
+    return lax.ppermute(value, axis, [(i, i + step) for i in sources])
+
+
+def gather_square(block):
+    half = block.shape[0] // 2
+    one, two = swap(block, "fs", 1), swap(block, "fs", 2)
+    three = jnp.concatenate([swap(two[:half], "fs", 1), swap(one[half:], "fs", 2)], 0)
+    return [block, one, two, three]
+
+
+def spread(
+    tokens,
+    norm_gain,
+    pool_input,
+    query_weight,
+    key_weight,
+    value_weight,
+    pool_map,
+    pool_scale,
+    head_gain,
+    diff_lambda,
+    out_pool,
+    out_heads,
+):
+    n_sp, n_fs, n_tp = (lax.axis_size(axis) for axis in ("sp", "fs", "tp"))
+    sp, fs, tp = (lax.axis_index(axis) for axis in ("sp", "fs", "tp"))
+    rows, depth = tokens.shape[1:]
+    length = rows * n_sp
+    shard = depth // (n_sp * n_fs)
+
+    packed = jnp.stack(
+        [w.reshape(shard, n_sp, -1) for w in (pool_input, query_weight, key_weight, value_weight)], 2
+    )
+    packed = jnp.moveaxis(packed, 1, 0).reshape(n_sp, shard, -1)
+    arrived = fold_rows(lax.all_to_all(packed, "sp", 0, 0, tiled=True))
+    weight = jnp.concatenate(gather_square(arrived), 0)
+
+    floated = tokens[0].astype(jnp.float32)
+    normed = (
+        floated * lax.rsqrt(jnp.mean(floated * floated, -1, keepdims=True) + NORM_EPS) * norm_gain
+    ).astype(jnp.bfloat16)
+    split = normed.reshape(rows, n_sp, n_fs, shard)
+    own = jnp.concatenate(
+        [lax.dynamic_index_in_dim(split, fs ^ j, 2, False) for j in range(n_fs)], 1
+    ).reshape(rows, depth)
+    half = rows // n_tp
+    mine = lax.dynamic_slice_in_dim(own, tp * half, half, 0)
+    up, down = [mine], [mine]
+    for k in range(1, n_sp):
+        up.append(shift(up[-1], "sp", True, range(k - 1, n_sp - 1)))
+        down.append(shift(down[-1], "sp", False, range(1, n_sp + 1 - k)))
+    blocks = []
+    for k in range(n_sp - 1, 0, -1):
+        here = up[k] + down[n_sp - k]
+        there = swap(here, "tp", 1)
+        blocks += [jnp.where(tp == 0, here, there), jnp.where(tp == 0, there, here)]
+    sequence = jnp.concatenate(blocks + [own], 0)
+
+    proj = jnp.dot(sequence, weight, preferred_element_type=jnp.float32).astype(jnp.bfloat16)
+
+    first_pos = lax.rem((sp + 1) * rows, length)
+    positions = lax.rem(first_pos + jnp.arange(length, dtype=jnp.int32), length).astype(jnp.float32)
+    freqs = 1.0 / THETA ** (jnp.arange(HEAD_DIM // 2, dtype=jnp.float32) * 2.0 / HEAD_DIM)
+    angles = positions[:, None] * freqs[None, :]
+    cosine, sine = jnp.cos(angles), jnp.sin(angles)
+    group = tp * n_sp + sp
+    meta = jnp.stack([first_pos, lax.rem(group, 4)]).astype(jnp.int32)
+    branches = mix(
+        meta,
+        proj,
+        jnp.concatenate([cosine, cosine], 1),
+        jnp.concatenate([-sine, sine], 1),
+        lax.dynamic_index_in_dim(pool_map, sp, 0, False),
+        lax.dynamic_slice_in_dim(pool_scale, sp * GROUP_DIM, GROUP_DIM, 0)[None],
+        head_gain[None],
+        lax.dynamic_slice_in_dim(diff_lambda, group, 1, 0),
+        n_sp,
+    )
+
+    packed_out = jnp.concatenate(
+        [out_pool.reshape(n_sp, GROUP_DIM, shard), out_heads.reshape(n_sp, 2 * HEAD_DIM, shard)], 1
+    )
+    channels = packed_out.shape[1]
+    arrived_out = fold_rows(lax.all_to_all(packed_out, "sp", 0, 0, tiled=True))
+    pieces = [p.reshape(n_tp, n_sp // n_tp, channels, shard) for p in gather_square(arrived_out)]
+    out_weight = jnp.stack(pieces, 1)
+    out_weight = jnp.moveaxis(out_weight, 3, 1).reshape(n_tp, channels, depth // n_tp)
+    kept_weight = lax.dynamic_index_in_dim(out_weight, tp, 0, False)
+    sent_weight = lax.dynamic_index_in_dim(out_weight, 1 - tp, 0, False)
+
+    def block_sum(k):
+        part = branches[(n_sp - 1 - k) * rows : (n_sp - k) * rows]
+        sent = jnp.dot(part, sent_weight, preferred_element_type=jnp.float32).astype(jnp.bfloat16)
+        kept = jnp.dot(part, kept_weight, preferred_element_type=jnp.float32)
+        return kept + swap(sent, "tp", 1).astype(jnp.float32)
+
+    sums = {k: block_sum(k) for k in sorted(range(n_sp), key=lambda k: -abs(2 * k - n_sp) if k else 1)}
+    rising, falling = (jnp.zeros((rows, depth // n_tp), jnp.bfloat16),) * 2
+    for step in range(1, n_sp):
+        above = (sums[step] + rising.astype(jnp.float32)).astype(jnp.bfloat16)
+        below = (sums[n_sp - step] + falling.astype(jnp.float32)).astype(jnp.bfloat16)
+        rising = shift(above, "sp", True, range(0, step))
+        falling = shift(below, "sp", False, range(n_sp - step, n_sp))
+    result = (sums[0] + rising.astype(jnp.float32) + falling.astype(jnp.float32)).astype(jnp.bfloat16)
+    result = result.reshape(rows, n_fs, n_sp // n_tp, shard)
+    result = jnp.stack([lax.dynamic_index_in_dim(result, fs ^ j, 1, False) for j in range(n_fs)], 2)
+    return result.reshape(1, rows, depth // n_tp)
+
+
 def solution(mesh):
     placed = (
         P("fs", "sp", None),
@@ -201,6 +426,13 @@
         P("tp", ("sp", "fs")),
         P("tp", ("sp", "fs")),
     )
+
+    def body(*args):
+        n_sp, n_fs, n_tp = (mesh.shape[axis] for axis in ("sp", "fs", "tp"))
+        groups, heads = args[6].shape[0], args[5].shape[1] // (2 * HEAD_DIM)
+        pairs = groups == heads == n_sp and n_fs == 4 and n_tp == 2
+        return (spread if pairs else local)(*args)
+
     return jax.shard_map(
-        local, mesh=mesh, in_specs=placed, out_specs=P("fs", "sp", "tp"), check_vma=False
-    )
+        body, mesh=mesh, in_specs=placed, out_specs=P("fs", "sp", "tp"), check_vma=False
+    )

time: 575 us -> 230 us (0.40)
  waiting for transfers between devices: 487 us -> 96.1 us
  starting transfers between devices: 3.87 us -> 56.6 us
  matrix products: 31.8 us -> 13.3 us
  between operations: 13.8 us -> 0.62 us
  other arithmetic: 15.2 us -> 27.8 us
  Pallas kernels: 0 us -> 10.3 us
    all_gather x7 -> x0, waiting for transfers between devices: 477 us -> none  [the longest x1 136 us: local(): lax.all_gather(out_local, ('sp', 'fs'), axis=1, tiled=True)]
    ppermute x1 -> x27, waiting for transfers between devices: 0.67 us -> 95 us  [the longest x12 76.8 us: shift(): return lax.ppermute(value, axis, [(i, i + step) for i in sources])]
    ppermute x1 -> x27, starting transfers between devices: 3.59 us -> 44.9 us  [the longest x12 32.4 us: shift(): return lax.ppermute(value, axis, [(i, i + step) for i in sources])]
    dot_general x8 -> x9, matrix products: 31.8 us -> 13.3 us  [the longest x1 5.85 us: spread(): jnp.dot(sequence, weight, preferred_element_type=jnp.float32)]
    all_to_all x0 -> x2, starting transfers between devices: none -> 11.8 us  [the longest x1 6.35 us: spread(): arrived_out = fold_rows(lax.all_to_all(packed_out, 'sp', 0, 0, tiled=True))]
    pallas_call x0 -> x1, Pallas kernels: none -> 10.3 us  [mix(): pl.pallas_call(mix_kernel, out_shape=jax.ShapeDtypeStruct((length, GROUP_...]
    another operation x4 -> x1, local copies, waits for them, and re-layouts: 9.58 us -> 0.21 us  [spread(): jnp.stack([lax.dynamic_index_in_dim(result, fs ^ j, 1, False) for j in ra...]
    unnamed x26 -> x31, local copies, waits for them, and re-layouts: 0.42 us -> 9.06 us
  transfers between devices with their start and end apart: 9 -> 29, of which waited for: 9 -> 10; matrix products, arithmetic and copies ran while one was open for 11% -> 23% of each run, Pallas kernels for 0% -> 0%
where the time goes in v1:
time: 230 us; the launch traced here: 229 us
  waiting for transfers between devices  96.1 us (42%)
  starting transfers between devices  56.6 us (25%)
  other arithmetic  27.8 us (12%)
  local copies, waits for them, and re-layouts  24.3 us (11%)
  matrix products  13.3 us (6%)
  Pallas kernels  10.3 us (4%)
    ppermute x12, waiting for transfers between devices, shift(): return lax.ppermute(value, axis, [(i, i + step) for i in sources])  76.8 us
    ppermute x12, starting transfers between devices, shift(): return lax.ppermute(value, axis, [(i, i + step) for i in sources])  32.4 us
    ppermute x15, waiting for transfers between devices, swap(): lax.ppermute(value, axis, [(i, i ^ bits) for i in range(lax.axis_size(axi...  18.2 us
    ppermute x15, starting transfers between devices, swap(): lax.ppermute(value, axis, [(i, i ^ bits) for i in range(lax.axis_size(axi...  12.4 us
    pallas_call x1, Pallas kernels, mix(): pl.pallas_call(mix_kernel, out_shape=jax.ShapeDtypeStruct((length, GROUP_...  10.3 us
    unnamed x31, local copies, waits for them, and re-layouts  9.06 us
    unnamed x6, other arithmetic  6.66 us
    all_to_all x1, starting transfers between devices, spread(): arrived_out = fold_rows(lax.all_to_all(packed_out, 'sp', 0, 0, tiled=True))  6.35 us
  transfers between devices with their start and end apart: 29, of which 10 were waited for; matrix products, arithmetic and copies ran while one was open for 23% of the time, Pallas kernels for 0%

profile of v1, /device:TPU:0, one launch (start us, length us, event | category | flops | bytes accessed | tf_op | source)
XLA Modules:
  0.0 229.0 jit_solution(13000526831016232025)
XLA Ops:
  0.0 1.9 pad_maximum_fusion.4
  1.9 6.3 %all-to-all-start.1 = ((bf16[4,512,128]{2,1,0:T(8,128)(2,1)}), bf16[4,512,128]{2,1,0:T(8,128)(2,1)}, u32[]{:S(2)}, u32[]{:S(2)}) async-start(bf16[4,512,128]{2,1,0:T(8,128)(2,1)} %pad_maximum_fusion.4), calls=%async_computation.1 | async-start | bytes 1048576 | tf_op jit(solution)/shard_map/all_to_all | solution.py:388
  12.9 3.9 %collective-permute-start = (bf16[128,2048]{0,1:T(8,128)(2,1)}, bf16[128,2048]{0,1:T(8,128)(2,1)S(1)}, u32[]{:S(2)}, u32[]{:S(2)}) collective-permute-start(bf16[128,2048]{0,1:T(8,128)(2,1)} %constant_dynamic-slice_fusion.4), channel_id=1, source_target_pairs={{0,8},{8,16},{16,24},{1,9},{9,17},{17,25},{2,10},{10,18},{18,26},{... | collective-permute-start | bytes 1572872 | tf_op jit(solution)/shard_map/ppermute | solution.py:305
  23.9 5.4 %all-to-all-start = ((bf16[4,128,1024]{1,2,0:T(8,128)(2,1)}), bf16[4,128,1024]{1,2,0:T(8,128)(2,1)S(1)}, u32[]{:S(2)}, u32[]{:S(2)}) async-start(bf16[4,128,1024]{1,2,0:T(8,128)(2,1)} %bitcast.14), calls=%async_computation | async-start | bytes 2097152 | tf_op jit(solution)/shard_map/all_to_all | solution.py:339
  30.8 8.7 %collective-permute-done.3 = bf16[128,2048]{0,1:T(8,128)(2,1)} collective-permute-done((bf16[128,2048]{0,1:T(8,128)(2,1)}, bf16[128,2048]{0,1:T(8,128)(2,1)}, u32[]{:S(2)}, u32[]{:S(2)}) %collective-permute-start.3) | collective-permute-done | bytes 524320 | tf_op jit(solution)/shard_map/ppermute | solution.py:305
  45.4 16.4 %collective-permute-done.5 = bf16[128,2048]{0,1:T(8,128)(2,1)} collective-permute-done((bf16[128,2048]{0,1:T(8,128)(2,1)}, bf16[128,2048]{0,1:T(8,128)(2,1)}, u32[]{:S(2)}, u32[]{:S(2)}) %collective-permute-start.5) | collective-permute-done | bytes 524320 | tf_op jit(solution)/shard_map/ppermute | solution.py:305
  63.3 3.1 %fusion.30 = (f32[1024,64]{1,0:T(8,128)S(1)}, f32[1024,64]{1,0:T(8,128)}, f32[1024,64]{1,0:T(8,128)}) fusion(f32[64]{0:T(128)S(1)} %negate_power_fusion, f32[1024]{0:T(1024)S(1)} %fusion.32), kind=kLoop, calls=%fused_computation.61 | loop fusion | flops 131072 | bytes 790784 | tf_op jit(solution)/shard_map/neg | solution.py:376
  74.7 2.7 %pad_maximum_fusion.2 = (f32[1024,128]{1,0:T(8,128)}, f32[1024,128]{1,0:T(8,128)}) fusion(f32[1024,64]{1,0:T(8,128)} %get-tuple-element.17, f32[1024,64]{1,0:T(8,128)} %get-tuple-element.16, f32[1024,64]{1,0:T(8,128)S(1)} %get-tuple-element.15), kind=kLoop, calls=%fused_computation.42 | loop fusion | flops 262144 | bytes 1835008 | tf_op jit(solution)/shard_map/concatenate | solution.py:375
  78.9 2.1 add.116
  81.5 2.0 add.118
  88.5 3.0 %maximum_bitcast_fusion = bf16[2,512,4,2,128]{4,1,3,0,2:T(8,128)(2,1)} fusion(bf16[2,1,2,512,128]{4,3,2,0,1:T(8,128)(2,1)S(1)} %bitcast.79, bf16[2,1,2,512,128]{4,3,2,0,1:T(8,128)(2,1)} %bitcast.24, bf16[2,1,2,512,128]{4,3,2,0,1:T(8,128)(2,1)} %bitcast.23, bf16[2,1,2,512,128]{4,3,2,0,1:T(8,128)(2,1)} %bitcast.21), kind=kLoop, calls=%fused_computation | loop fusion | flops 3145728 | bytes 4194304 | tf_op jit(solution)/shard_map/transpose | solution.py:391
  91.5 2.8 %copy.34 = bf16[2,512,4,2,128]{1,4,3,2,0:T(8,128)(2,1)S(1)} copy(bf16[2,512,4,2,128]{4,1,3,0,2:T(8,128)(2,1)} %maximum_bitcast_fusion) | data formatting | bytes 4194304 | tf_op jit(solution)/shard_map/transpose | solution.py:391
  102.4 9.3 %collective-permute-done.10 = bf16[512,1024]{1,0:T(8,128)(2,1)} collective-permute-done((bf16[512,1024]{1,0:T(8,128)(2,1)}, bf16[512,1024]{1,0:T(8,128)(2,1)}, u32[]{:S(2)}, u32[]{:S(2)}) %collective-permute-start.10) | collective-permute-done | bytes 1048608 | tf_op jit(solution)/shard_map/ppermute | solution.py:300
  118.7 7.2 %collective-permute-done.11 = bf16[256,1024]{1,0:T(8,128)(2,1)S(1)} collective-permute-done((bf16[256,1024]{1,0:T(8,128)(2,1)S(1)}, bf16[256,1024]{1,0:T(8,128)(2,1)S(1)}, u32[]{:S(2)}, u32[]{:S(2)}) %collective-permute-start.11) | collective-permute-done | bytes 524320 | tf_op jit(solution)/shard_map/ppermute | solution.py:300
  127.7 5.8 %convolution_convert_fusion.proj_ref = bf16[1024,1024]{1,0:T(8,128)(2,1)} fusion(bf16[1024,2048]{0,1:T(8,128)(2,1)S(1)} %constant_dynamic-update-slice_fusion, bf16[2048,1024]{1,0:T(8,128)(2,1)S(1)} %constant_dynamic-update-slice_fusion.1), kind=kOutput, calls=%fused_computation.3 | convolution fusion | flops 4296015872 | bytes 10485760 | tf_op jit(solution)/shard_map/dot_general | solution.py:363
  133.5 10.3 %mix.1 = bf16[1024,512]{1,0:T(8,128)(2,1)} custom-call(s32[2]{0:T(128)} %pad_add_fusion.meta_ref, bf16[1024,1024]{1,0:T(8,128)(2,1)} %convolution_convert_fusion.proj_ref, f32[1024,128]{1,0:T(8,128)} %get-tuple-element.20.cos_ref, f32[1024,128]{1,0:T(8,128)} %get-tuple-element.21.sin_ref, bf16[256,256]{1,0:T(8,128)(2,1)} %dynamic-slice_bitcast_fusion.map_ref, ...), custom_call_target="tpu_custom_call" | custom-call | flops 1073741824 | bytes 3145728 | tf_op jit(solution)/shard_map/mix/pallas_call | solution.py:269
  143.8 2.2 convolution_convert_fusion.1
  149.6 9.2 %collective-permute-start.21 = (bf16[256,1024]{1,0:T(8,128)(2,1)S(1)}, bf16[256,1024]{1,0:T(8,128)(2,1)S(1)}, u32[]{:S(2)}, u32[]{:S(2)}) collective-permute-start(bf16[256,1024]{1,0:T(8,128)(2,1)S(1)} %get-tuple-element.18), channel_id=1, source_target_pairs={{0,8},{1,9},{2,10},{3,11},{4,12},{5,13},{6,14},{7,15}} | collective-permute-start | bytes 1572872 | tf_op jit(solution)/shard_map/ppermute | solution.py:305
  159.8 10.4 %collective-permute-done.21 = bf16[256,1024]{1,0:T(8,128)(2,1)S(1)} collective-permute-done((bf16[256,1024]{1,0:T(8,128)(2,1)S(1)}, bf16[256,1024]{1,0:T(8,128)(2,1)S(1)}, u32[]{:S(2)}, u32[]{:S(2)}) %collective-permute-start.21) | collective-permute-done | bytes 524320 | tf_op jit(solution)/shard_map/ppermute | solution.py:305
  170.4 4.4 %collective-permute-start.22 = (bf16[256,1024]{1,0:T(8,128)(2,1)S(1)}, bf16[256,1024]{1,0:T(8,128)(2,1)S(1)}, u32[]{:S(2)}, u32[]{:S(2)}) collective-permute-start(bf16[256,1024]{1,0:T(8,128)(2,1)S(1)} %add_convert_fusion.4), channel_id=1, source_target_pairs={{0,8},{8,16},{1,9},{9,17},{2,10},{10,18},{3,11},{11,19},{4,12},{12... | collective-permute-start | bytes 1572872 | tf_op jit(solution)/shard_map/ppermute | solution.py:305
  175.3 10.1 %collective-permute-done.22 = bf16[256,1024]{1,0:T(8,128)(2,1)S(1)} collective-permute-done((bf16[256,1024]{1,0:T(8,128)(2,1)S(1)}, bf16[256,1024]{1,0:T(8,128)(2,1)S(1)}, u32[]{:S(2)}, u32[]{:S(2)}) %collective-permute-start.22) | collective-permute-done | bytes 524320 | tf_op jit(solution)/shard_map/ppermute | solution.py:305
  188.2 5.0 %collective-permute-start.23 = (bf16[256,1024]{1,0:T(8,128)(2,1)S(1)}, bf16[256,1024]{1,0:T(8,128)(2,1)S(1)}, u32[]{:S(2)}, u32[]{:S(2)}) collective-permute-start(bf16[256,1024]{1,0:T(8,128)(2,1)S(1)} %get-tuple-element.5), channel_id=1, source_target_pairs={{0,8},{8,16},{16,24},{1,9},{9,17},{17,25},{2,10},{10,18},{18,26},{... | collective-permute-start | bytes 1572872 | tf_op jit(solution)/shard_map/ppermute | solution.py:305
  195.3 9.7 %collective-permute-done.23 = bf16[256,1024]{1,0:T(8,128)(2,1)S(1)} collective-permute-done((bf16[256,1024]{1,0:T(8,128)(2,1)S(1)}, bf16[256,1024]{1,0:T(8,128)(2,1)S(1)}, u32[]{:S(2)}, u32[]{:S(2)}) %collective-permute-start.23) | collective-permute-done | bytes 524320 | tf_op jit(solution)/shard_map/ppermute | solution.py:305
  205.0 21.6 %collective-permute-done.26 = bf16[256,1024]{1,0:T(8,128)(2,1)S(1)} collective-permute-done((bf16[256,1024]{1,0:T(8,128)(2,1)S(1)}, bf16[256,1024]{1,0:T(8,128)(2,1)S(1)}, u32[]{:S(2)}, u32[]{:S(2)}) %collective-permute-start.26) | collective-permute-done | bytes 524320 | tf_op jit(solution)/shard_map/ppermute | solution.py:305
  (125 shorter events, 64.8 us)
Async XLA Ops:
  1.9 21.9 %all-to-all-start.1 = ((bf16[4,512,128]{2,1,0:T(8,128)(2,1)}), bf16[4,512,128]{2,1,0:T(8,128)(2,1)}, u32[]{:S(2)}, u32[]{:S(2)}) async-start(bf16[4,512,128]{2,1,0:T(8,128)(2,1)} %pad_maximum_fusion.4), calls=%async_computation.1 | async-start | bytes 1048576 | tf_op jit(solution)/shard_map/all_to_all | solution.py:388
  12.9 16.4 %collective-permute-start = (bf16[128,2048]{0,1:T(8,128)(2,1)}, bf16[128,2048]{0,1:T(8,128)(2,1)S(1)}, u32[]{:S(2)}, u32[]{:S(2)}) collective-permute-start(bf16[128,2048]{0,1:T(8,128)(2,1)} %constant_dynamic-slice_fusion.4), channel_id=1, source_target_pairs={{0,8},{8,16},{16,24},{1,9},{9,17},{17,25},{2,10},{10,18},{18,26},{... | collective-permute-start | bytes 1572872 | tf_op jit(solution)/shard_map/ppermute | solution.py:305
  16.8 22.7 %collective-permute-start.3 = (bf16[128,2048]{0,1:T(8,128)(2,1)}, bf16[128,2048]{0,1:T(8,128)(2,1)}, u32[]{:S(2)}, u32[]{:S(2)}) collective-permute-start(bf16[128,2048]{0,1:T(8,128)(2,1)} %constant_dynamic-slice_fusion.4), channel_id=1, source_target_pairs={{8,0},{16,8},{24,16},{9,1},{17,9},{25,17},{10,2},{18,10},{26,18},{... | collective-permute-start | bytes 1572872 | tf_op jit(solution)/shard_map/ppermute | solution.py:305
  23.9 59.6 %all-to-all-start = ((bf16[4,128,1024]{1,2,0:T(8,128)(2,1)}), bf16[4,128,1024]{1,2,0:T(8,128)(2,1)S(1)}, u32[]{:S(2)}, u32[]{:S(2)}) async-start(bf16[4,128,1024]{1,2,0:T(8,128)(2,1)} %bitcast.14), calls=%async_computation | async-start | bytes 2097152 | tf_op jit(solution)/shard_map/all_to_all | solution.py:339
  29.3 14.6 %collective-permute-start.1 = (bf16[128,2048]{0,1:T(8,128)(2,1)S(1)}, bf16[128,2048]{0,1:T(8,128)(2,1)}, u32[]{:S(2)}, u32[]{:S(2)}) collective-permute-start(bf16[128,2048]{0,1:T(8,128)(2,1)S(1)} %collective-permute-done), channel_id=1, source_target_pairs={{8,16},{16,24},{9,17},{17,25},{10,18},{18,26},{11,19},{19,27},{12,... | collective-permute-start | bytes 1572872 | tf_op jit(solution)/shard_map/ppermute | solution.py:305
  39.5 22.3 %collective-permute-start.5 = (bf16[128,2048]{0,1:T(8,128)(2,1)}, bf16[128,2048]{0,1:T(8,128)(2,1)}, u32[]{:S(2)}, u32[]{:S(2)}) collective-permute-start(bf16[128,2048]{0,1:T(8,128)(2,1)} %collective-permute-done.3), channel_id=1, source_target_pairs={{8,0},{16,8},{9,1},{17,9},{10,2},{18,10},{11,3},{19,11},{12,4},{20... | collective-permute-start | bytes 1572872 | tf_op jit(solution)/shard_map/ppermute | solution.py:305
  40.8 25.5 %collective-permute-start.14 = (bf16[2048,128]{1,0:T(8,128)(2,1)}, bf16[2048,128]{1,0:T(8,128)(2,1)}, u32[]{:S(2)}, u32[]{:S(2)}) collective-permute-start(bf16[2048,128]{1,0:T(8,128)(2,1)} %bitcast.22), channel_id=1, source_target_pairs={{0,4},{2,6},{4,0},{6,2},{1,5},{3,7},{5,1},{7,3},{8,12},{10,14},{12... | collective-permute-start | bytes 1572872 | tf_op jit(solution)/shard_map/ppermute | solution.py:300
  42.4 26.5 %collective-permute-start.13 = (bf16[2048,128]{1,0:T(8,128)(2,1)}, bf16[2048,128]{1,0:T(8,128)(2,1)}, u32[]{:S(2)}, u32[]{:S(2)}) collective-permute-start(bf16[2048,128]{1,0:T(8,128)(2,1)} %bitcast.22), channel_id=1, source_target_pairs={{0,2},{2,0},{4,6},{6,4},{1,3},{3,1},{5,7},{7,5},{8,10},{10,8},{12,... | collective-permute-start | bytes 1572872 | tf_op jit(solution)/shard_map/ppermute | solution.py:300
  43.9 35.0 %collective-permute-start.2 = (bf16[128,2048]{0,1:T(8,128)(2,1)}, bf16[128,2048]{0,1:T(8,128)(2,1)}, u32[]{:S(2)}, u32[]{:S(2)}) collective-permute-start(bf16[128,2048]{0,1:T(8,128)(2,1)} %collective-permute-done.1), channel_id=1, source_target_pairs={{16,24},{17,25},{18,26},{19,27},{20,28},{21,29},{22,30},{23,31}} | collective-permute-start | bytes 1572872 | tf_op jit(solution)/shard_map/ppermute | solution.py:305
  61.8 19.7 %collective-permute-start.7 = (bf16[128,2048]{0,1:T(8,128)(2,1)}, bf16[128,2048]{0,1:T(8,128)(2,1)}, u32[]{:S(2)}, u32[]{:S(2)}) collective-permute-start(bf16[128,2048]{0,1:T(8,128)(2,1)} %collective-permute-done.5), channel_id=1, source_target_pairs={{8,0},{9,1},{10,2},{11,3},{12,4},{13,5},{14,6},{15,7}} | collective-permute-start | bytes 1572872 | tf_op jit(solution)/shard_map/ppermute | solution.py:305
  67.4 17.5 %collective-permute-start.15 = (bf16[1024,128]{1,0:T(8,128)(2,1)S(1)}, bf16[1024,128]{1,0:T(8,128)(2,1)S(1)}, u32[]{:S(2)}, u32[]{:S(2)}) collective-permute-start(bf16[1024,128]{1,0:T(8,128)(2,1)S(1)} %slice.35), channel_id=1, source_target_pairs={{0,2},{2,0},{4,6},{6,4},{1,3},{3,1},{5,7},{7,5},{8,10},{10,8},{12,... | collective-permute-start | bytes 786440 | tf_op jit(solution)/shard_map/ppermute | solution.py:300
  69.9 16.1 %collective-permute-start.16 = (bf16[1024,128]{1,0:T(8,128)(2,1)S(1)}, bf16[1024,128]{1,0:T(8,128)(2,1)}, u32[]{:S(2)}, u32[]{:S(2)}) collective-permute-start(bf16[1024,128]{1,0:T(8,128)(2,1)S(1)} %slice.36), channel_id=1, source_target_pairs={{0,4},{2,6},{4,0},{6,2},{1,5},{3,7},{5,1},{7,3},{8,12},{10,14},{12... | collective-permute-start | bytes 786440 | tf_op jit(solution)/shard_map/ppermute | solution.py:300
  78.8 19.4 %collective-permute-start.6 = (bf16[128,2048]{0,1:T(8,128)(2,1)S(1)}, bf16[128,2048]{0,1:T(8,128)(2,1)}, u32[]{:S(2)}, u32[]{:S(2)}) collective-permute-start(bf16[128,2048]{0,1:T(8,128)(2,1)S(1)} %add.117), channel_id=1, source_target_pairs={{0,1},{1,0},{2,3},{3,2},{4,5},{5,4},{6,7},{7,6},{8,9},{9,8},{10,11... | collective-permute-start | bytes 1572872 | tf_op jit(solution)/shard_map/ppermute | solution.py:300
  81.0 14.6 %collective-permute-start.4 = (bf16[128,2048]{0,1:T(8,128)(2,1)}, bf16[128,2048]{0,1:T(8,128)(2,1)}, u32[]{:S(2)}, u32[]{:S(2)}) collective-permute-start(bf16[128,2048]{0,1:T(8,128)(2,1)} %add.116), channel_id=1, source_target_pairs={{0,1},{1,0},{2,3},{3,2},{4,5},{5,4},{6,7},{7,6},{8,9},{9,8},{10,11... | collective-permute-start | bytes 1572872 | tf_op jit(solution)/shard_map/ppermute | solution.py:300
  83.5 16.3 %collective-permute-start.8 = (bf16[128,2048]{0,1:T(8,128)(2,1)}, bf16[128,2048]{0,1:T(8,128)(2,1)}, u32[]{:S(2)}, u32[]{:S(2)}) collective-permute-start(bf16[128,2048]{0,1:T(8,128)(2,1)} %add.118), channel_id=1, source_target_pairs={{0,1},{1,0},{2,3},{3,2},{4,5},{5,4},{6,7},{7,6},{8,9},{9,8},{10,11... | collective-permute-start | bytes 1572872 | tf_op jit(solution)/shard_map/ppermute | solution.py:300
  84.8 28.8 %collective-permute-start.9 = (bf16[512,1024]{1,0:T(8,128)(2,1)}, bf16[512,1024]{1,0:T(8,128)(2,1)}, u32[]{:S(2)}, u32[]{:S(2)}) collective-permute-start(bf16[512,1024]{1,0:T(8,128)(2,1)} %bitcast.15), channel_id=1, source_target_pairs={{0,2},{2,0},{4,6},{6,4},{1,3},{3,1},{5,7},{7,5},{8,10},{10,8},{12,... | collective-permute-start | bytes 3145736 | tf_op jit(solution)/shard_map/ppermute | solution.py:300
  86.0 25.6 %collective-permute-start.10 = (bf16[512,1024]{1,0:T(8,128)(2,1)}, bf16[512,1024]{1,0:T(8,128)(2,1)}, u32[]{:S(2)}, u32[]{:S(2)}) collective-permute-start(bf16[512,1024]{1,0:T(8,128)(2,1)} %bitcast.15), channel_id=1, source_target_pairs={{0,4},{2,6},{4,0},{6,2},{1,5},{3,7},{5,1},{7,3},{8,12},{10,14},{12... | collective-permute-start | bytes 3145736 | tf_op jit(solution)/shard_map/ppermute | solution.py:300
  112.7 13.3 %collective-permute-start.11 = (bf16[256,1024]{1,0:T(8,128)(2,1)S(1)}, bf16[256,1024]{1,0:T(8,128)(2,1)S(1)}, u32[]{:S(2)}, u32[]{:S(2)}) collective-permute-start(bf16[256,1024]{1,0:T(8,128)(2,1)S(1)} %slice.32), channel_id=1, source_target_pairs={{0,2},{2,0},{4,6},{6,4},{1,3},{3,1},{5,7},{7,5},{8,10},{10,8},{12,... | collective-permute-start | bytes 1572872 | tf_op jit(solution)/shard_map/ppermute | solution.py:300
  114.7 13.0 %collective-permute-start.12 = (bf16[256,1024]{1,0:T(8,128)(2,1)S(1)}, bf16[256,1024]{1,0:T(8,128)(2,1)S(1)}, u32[]{:S(2)}, u32[]{:S(2)}) collective-permute-start(bf16[256,1024]{1,0:T(8,128)(2,1)S(1)} %slice.33), channel_id=1, source_target_pairs={{0,4},{2,6},{4,0},{6,2},{1,5},{3,7},{5,1},{7,3},{8,12},{10,14},{12... | collective-permute-start | bytes 1572872 | tf_op jit(solution)/shard_map/ppermute | solution.py:300
  149.6 20.6 %collective-permute-start.21 = (bf16[256,1024]{1,0:T(8,128)(2,1)S(1)}, bf16[256,1024]{1,0:T(8,128)(2,1)S(1)}, u32[]{:S(2)}, u32[]{:S(2)}) collective-permute-start(bf16[256,1024]{1,0:T(8,128)(2,1)S(1)} %get-tuple-element.18), channel_id=1, source_target_pairs={{0,8},{1,9},{2,10},{3,11},{4,12},{5,13},{6,14},{7,15}} | collective-permute-start | bytes 1572872 | tf_op jit(solution)/shard_map/ppermute | solution.py:305
  159.2 16.1 %collective-permute-start.18 = (bf16[256,1024]{1,0:T(8,128)(2,1)S(1)}, bf16[256,1024]{1,0:T(8,128)(2,1)S(1)}, u32[]{:S(2)}, u32[]{:S(2)}) collective-permute-start(bf16[256,1024]{1,0:T(8,128)(2,1)S(1)} %convolution_convert_fusion.3), channel_id=1, source_target_pairs={{0,1},{1,0},{2,3},{3,2},{4,5},{5,4},{6,7},{7,6},{8,9},{9,8},{10,11... | collective-permute-start | bytes 1572872 | tf_op jit(solution)/shard_map/ppermute | solution.py:300
  170.4 15.0 %collective-permute-start.22 = (bf16[256,1024]{1,0:T(8,128)(2,1)S(1)}, bf16[256,1024]{1,0:T(8,128)(2,1)S(1)}, u32[]{:S(2)}, u32[]{:S(2)}) collective-permute-start(bf16[256,1024]{1,0:T(8,128)(2,1)S(1)} %add_convert_fusion.4), channel_id=1, source_target_pairs={{0,8},{8,16},{1,9},{9,17},{2,10},{10,18},{3,11},{11,19},{4,12},{12... | collective-permute-start | bytes 1572872 | tf_op jit(solution)/shard_map/ppermute | solution.py:305
  188.2 16.8 %collective-permute-start.23 = (bf16[256,1024]{1,0:T(8,128)(2,1)S(1)}, bf16[256,1024]{1,0:T(8,128)(2,1)S(1)}, u32[]{:S(2)}, u32[]{:S(2)}) collective-permute-start(bf16[256,1024]{1,0:T(8,128)(2,1)S(1)} %get-tuple-element.5), channel_id=1, source_target_pairs={{0,8},{8,16},{16,24},{1,9},{9,17},{17,25},{2,10},{10,18},{18,26},{... | collective-permute-start | bytes 1572872 | tf_op jit(solution)/shard_map/ppermute | solution.py:305
  193.5 33.1 %collective-permute-start.26 = (bf16[256,1024]{1,0:T(8,128)(2,1)S(1)}, bf16[256,1024]{1,0:T(8,128)(2,1)S(1)}, u32[]{:S(2)}, u32[]{:S(2)}) collective-permute-start(bf16[256,1024]{1,0:T(8,128)(2,1)S(1)} %add_convert_fusion.1), channel_id=1, source_target_pairs={{8,0},{16,8},{24,16},{9,1},{17,9},{25,17},{10,2},{18,10},{26,18},{... | collective-permute-start | bytes 1572872 | tf_op jit(solution)/shard_map/ppermute | solution.py:305
  (14 other events, 306.8 us)

commit v2 on v0

--- a/solution.py
+++ b/solution.py
@@ -1,9 +1,14 @@
+import functools
 import math
 
 import jax
 import jax.numpy as jnp
+import numpy as np
 from jax import lax
+from jax.experimental import pallas as pl
+from jax.experimental.pallas import tpu as pltpu
 from jax.sharding import PartitionSpec as P
+
 
 HEAD_DIM = 128
 GROUP_DIM = 256
@@ -186,6 +191,333 @@
     return layer_out[None]
 
 
+VMEM = pl.BlockSpec(memory_space=pltpu.VMEM)
+SMEM = pl.BlockSpec(memory_space=pltpu.SMEM)
+HBM = pl.BlockSpec(memory_space=pltpu.HBM)
+VMEM_LIMIT = 24 * 1024 * 1024
+WHOLE_VMEM = 60 * 1024 * 1024
+
+
+def call(kernel, outs, scratch, cost, specs, *args, limit=VMEM_LIMIT):
+    flops, moved, exps = cost
+    return pl.pallas_call(
+        kernel,
+        out_shape=[jax.ShapeDtypeStruct(shape, dtype) for shape, dtype in outs],
+        in_specs=specs,
+        out_specs=[VMEM] * len(outs),
+        scratch_shapes=scratch,
+        compiler_params=pltpu.CompilerParams(vmem_limit_bytes=limit),
+        cost_estimate=pl.CostEstimate(flops=flops, bytes_accessed=moved, transcendentals=exps),
+    )(*args)
+
+
+def move(pairs_of, outs, count, *args, limit=VMEM_LIMIT):
+    def kernel(*refs):
+        sems = refs[-1]
+        copies = [
+            pltpu.make_async_copy(source, target, sems.at[i])
+            for i, (source, target) in enumerate(pairs_of(refs[: len(args)], refs[len(args) : -1]))
+        ]
+        for copy in copies:
+            copy.start()
+        for copy in copies:
+            copy.wait()
+
+    moved = sum(2 * math.prod(shape) * 2 for shape, _ in outs)
+    return call(
+        kernel, outs, [pltpu.SemaphoreType.DMA((count,))], (0, moved, 0), [HBM] * len(args), *args,
+        limit=limit,
+    )
+
+
+def tiles(start, size):
+    return pl.ds(pl.multiple_of(start * size, size), size)
+
+
+def project_kernel(slot, *refs):
+    *xs, w_ref, turn_ref, out_ref = refs if slot == 0 else refs[:-1]
+    rows = out_ref.shape[0]
+    if slot:
+        x_ref = refs[-1]
+        tp = lax.axis_index("tp")
+        half = xs[0].shape[0]
+        x_ref[tiles(tp, half)] = xs[0][...]
+        x_ref[tiles(1 - tp, half)] = xs[1][...]
+    else:
+        x_ref = xs[0]
+    width = w_ref.shape[1] // 4
+    table = turn_ref[tiles(lax.axis_index("sp") ^ slot, rows)]
+    other = pltpu.roll(table, HEAD_DIM // 2, 1)
+    front = lax.broadcasted_iota(jnp.int32, table.shape, 1) < HEAD_DIM // 2
+    cosine, sine = jnp.where(front, table, other), jnp.where(front, -other, table)
+    for part in range(4):
+        product = jnp.dot(
+            x_ref[...], w_ref[:, part * width : (part + 1) * width], preferred_element_type=jnp.float32
+        ).astype(jnp.bfloat16)
+        if part in (1, 2):
+            raw = product.astype(jnp.float32)
+            turned = [
+                raw[:, m : m + HEAD_DIM] * cosine
+                + pltpu.roll(raw[:, m : m + HEAD_DIM], HEAD_DIM // 2, 1) * sine
+                for m in range(0, width, HEAD_DIM)
+            ]
+            product = jnp.concatenate(turned, 1).astype(jnp.bfloat16)
+        out_ref[:, part * width : (part + 1) * width] = product
+
+
+def mix_kernel(slot, total, *refs):
+    projs, (map_ref, scale_ref, gain_ref, lam_ref, w_ref, sent_ref, kept_ref, branch_ref) = (
+        refs[:total],
+        refs[total:],
+    )
+    rows = projs[0].shape[0]
+    width = 2 * HEAD_DIM
+    place = lax.axis_index("sp")
+    group = lax.axis_index("tp") * total + place
+    level = lax.rem(group, 4)
+    block = place ^ slot
+    scale = HEAD_DIM ** (-0.5)
+    ahead = lax.broadcasted_iota(jnp.int32, (rows, rows), 0) >= lax.broadcasted_iota(
+        jnp.int32, (rows, rows), 1
+    )
+    halves = []
+    for m in range(2):
+        begin = GROUP_DIM + m * HEAD_DIM
+        query = projs[slot][:, begin : begin + HEAD_DIM]
+        scores, tops = [], []
+        for j in range(total):
+            score = lax.dot_general(
+                query,
+                projs[j][:, begin + width : begin + width + HEAD_DIM],
+                (((1,), (1,)), ((), ())),
+                preferred_element_type=jnp.float32,
+            )
+            if j == slot:
+                score = jnp.where(ahead, score, -jnp.inf)
+                tops.append(jnp.max(score, -1, keepdims=True))
+            else:
+                bias = jnp.where((place ^ j) < block, 0.0, -jnp.inf)
+                tops.append(jnp.max(score, -1, keepdims=True) + bias)
+            scores.append(score)
+        largest = functools.reduce(jnp.maximum, tops)
+        sums, summed = 0.0, 0.0
+        for j in range(total):
+            limit = largest
+            if j != slot:
+                limit = largest + jnp.where((place ^ j) < block, 0.0, jnp.inf)
+            expons = jnp.exp((scores[j] - limit) * scale)
+            sums = sums + jnp.sum(expons, -1, keepdims=True)
+            summed = summed + jnp.dot(
+                expons.astype(jnp.bfloat16),
+                projs[j][:, GROUP_DIM + 2 * width :],
+                preferred_element_type=jnp.float32,
+            )
+        halves.append(summed / sums)
+    raw = halves[0] - lam_ref[group] * halves[1]
+    attn = (
+        raw
+        * lax.rsqrt(jnp.mean(raw * raw, -1, keepdims=True) + HEAD_EPS)
+        * gain_ref[...]
+        * HEAD_SCALE
+    ).astype(jnp.bfloat16)
+    branch_ref[:, GROUP_DIM:] = attn
+
+    reach = 16
+    rim = jnp.zeros((reach, GROUP_DIM), jnp.bfloat16)
+    for j in range(total):
+        rim = jnp.where((place ^ j) == block - 1, projs[j][rows - reach :, :GROUP_DIM], rim)
+    flat = jnp.concatenate([rim, projs[slot][:, :GROUP_DIM]], 0).astype(jnp.float32)
+    sums = flat
+    picked = jnp.zeros((rows, GROUP_DIM), jnp.float32)
+    for power in range(4):
+        sums = sums + pltpu.roll(sums, 2**power, 0)
+        picked = jnp.where(level == power, sums[reach:], picked)
+    window = lax.shift_left(jnp.int32(2), level)
+    own_pos = block * rows + lax.broadcasted_iota(jnp.int32, (rows, GROUP_DIM), 0)
+    counts = jnp.minimum(own_pos + 1, window).astype(jnp.float32)
+    mixed = (picked / counts - flat[reach:]).astype(jnp.bfloat16)
+    pooled = jnp.dot(mixed, map_ref[place], preferred_element_type=jnp.float32) * scale_ref[pl.ds(place, 1)]
+    branch_ref[:, :GROUP_DIM] = pooled.astype(jnp.bfloat16)
+    sent_ref[...] = jnp.dot(
+        branch_ref[...], w_ref[1], preferred_element_type=jnp.float32
+    ).astype(jnp.bfloat16)
+    kept_ref[...] = jnp.dot(branch_ref[...], w_ref[0], preferred_element_type=jnp.float32)
+
+
+def swap(value, axis, bits):
+    return lax.ppermute(value, axis, [(i, i ^ bits) for i in range(lax.axis_size(axis))])
+
+
+def after(value, *earlier):
+    return lax.optimization_barrier((value, *earlier))[0]
+
+
+def square(front, back):
+    back_one, front_two = swap(back, "fs", 1), swap(front, "fs", 2)
+    front_one, back_two = swap(front, "fs", 1), swap(back, "fs", 2)
+    front_three = swap(front_two, "fs", 1)
+    back_three = swap(back_one, "fs", 2)
+    return [(front, back), (front_one, back_one), (front_two, back_two), (front_three, back_three)]
+
+
+def spread(
+    tokens,
+    norm_gain,
+    pool_input,
+    query_weight,
+    key_weight,
+    value_weight,
+    pool_map,
+    pool_scale,
+    head_gain,
+    diff_lambda,
+    out_pool,
+    out_heads,
+):
+    low, wide = jnp.bfloat16, jnp.float32
+    n_sp, n_fs, n_tp = (lax.axis_size(axis) for axis in ("sp", "fs", "tp"))
+    tp = lax.axis_index("tp")
+    rows, depth = tokens.shape[1:]
+    shard = depth // (n_sp * n_fs)
+    channels = GROUP_DIM + 2 * HEAD_DIM
+    width = GROUP_DIM + 3 * 2 * HEAD_DIM
+    part = width // 4
+
+    def columns(sources, targets):
+        sp = lax.axis_index("sp")
+        return [
+            (source.at[:, tiles(sp ^ j, part)], targets[j].at[:, i * part : (i + 1) * part])
+            for j in (*range(n_sp - 1, 0, -1), 0)
+            for i, source in enumerate(sources)
+        ]
+
+    pieces = move(
+        columns, [((shard, width), low)] * n_sp, 4 * n_sp,
+        pool_input, query_weight, key_weight, value_weight, limit=WHOLE_VMEM,
+    )
+    near = [pieces[0]] + [swap(pieces[0], "fs", i) for i in range(1, n_fs)]
+    far = [swap(pieces[j], "sp", j) for j in range(1, n_sp)]
+    half_shard = shard // 2
+
+    def bundle(sources, targets):
+        return [
+            (source.at[tiles(side, half_shard)], targets[side].at[tiles(i, half_shard)])
+            for side in range(2)
+            for i, source in enumerate(sources)
+        ]
+
+    bundled = move(bundle, [(((n_sp - 1) * half_shard, width), low)] * 2, 2 * (n_sp - 1), *far)
+    distant = [part for pair in square(*bundled) for part in pair]
+
+    def assemble(sources, targets):
+        sp, fs = lax.axis_index("sp"), lax.axis_index("fs")
+        pairs = []
+        for i in range(n_fs):
+            pairs.append((sources[i], targets[0].at[tiles(sp * n_fs + (fs ^ i), shard)]))
+            for j in range(1, n_sp):
+                place = (sp ^ j) * n_fs + (fs ^ i)
+                for side in range(2):
+                    source = sources[n_fs + 2 * i + side].at[tiles(j - 1, half_shard)]
+                    pairs.append((source, targets[0].at[tiles(2 * place + side, half_shard)]))
+        return pairs
+
+    (weight,) = move(assemble, [((depth, width), low)], n_fs * (2 * n_sp - 1), *near, *distant)
+
+    size = channels // 2
+
+    def rows_of(sources, targets):
+        sp = lax.axis_index("sp")
+        return [
+            (source.at[tiles(sp ^ j, size)], targets[j].at[tiles(i, size)])
+            for j in range(n_sp)
+            for i, source in enumerate(sources)
+        ]
+
+    pieces_out = move(
+        rows_of, [((channels, shard), low)] * n_sp, 2 * n_sp, out_pool, out_heads,
+        limit=WHOLE_VMEM,
+    )
+    far_out = [pieces_out[0]] + [swap(pieces_out[j], "sp", j) for j in range(1, n_sp)]
+
+    def bundle_out(sources, targets):
+        return [
+            (source.at[tiles(side, size)], targets[side].at[tiles(j, size)])
+            for side in range(2)
+            for j, source in enumerate(sources)
+        ]
+
+    bundled_out = move(bundle_out, [((n_sp * size, shard), low)] * 2, 2 * n_sp, *far_out)
+
+    def assemble_out(sources, targets):
+        sp, fs, tp = (lax.axis_index(axis) for axis in ("sp", "fs", "tp"))
+        per = n_sp // n_tp
+        pairs = []
+        for i in range(n_fs):
+            for j in range(n_sp):
+                other = sp ^ j
+                here = tiles(lax.rem(other, per) * n_fs + (fs ^ i), shard)
+                target = targets[0].at[lax.div(other, per) ^ tp]
+                for side in range(2):
+                    source = sources[2 * i + side].at[tiles(j, size)]
+                    pairs.append((source, target.at[tiles(side, size), here]))
+        return pairs
+
+    (out_weight,) = move(
+        assemble_out, [((n_tp, channels, depth // n_tp), low)], 2 * n_sp * n_fs,
+        *[part for pair in square(*bundled_out) for part in pair],
+    )
+
+    floated = tokens[0].astype(wide)
+    own = (
+        floated * lax.rsqrt(jnp.mean(floated * floated, -1, keepdims=True) + NORM_EPS) * norm_gain
+    ).astype(low)
+    half = rows // n_tp
+    mine = lax.dynamic_slice_in_dim(own, tp * half, half, 0)
+    slots = {0: mine}
+    for bit in (2, 1):
+        for j in sorted(slots, reverse=True):
+            slots[j ^ bit] = swap(slots[j], "sp", bit)
+
+    half_dim = HEAD_DIM // 2
+    freqs = 1.0 / THETA ** (np.arange(half_dim, dtype=np.float32) * 2.0 / HEAD_DIM)
+    angles = np.arange(rows * n_sp, dtype=np.float64)[:, None] * freqs[None, :]
+    table = jnp.asarray(np.concatenate([np.cos(angles), np.sin(angles)], 1).astype(np.float32))
+
+    def project(j):
+        xs = [own] if j == 0 else [slots[j], swap(slots[j], "tp", 1)]
+        scratch = [pltpu.VMEM((rows, depth), low)] if j else []
+        return call(
+            functools.partial(project_kernel, j), [((rows, width), low)], scratch,
+            (2 * rows * depth * width, 2 * depth * width, 0), [VMEM] * (len(xs) + 2),
+            *xs, weight, table,
+        )[0]
+
+    projs = [project(j) for j in range(n_sp)]
+    gain = head_gain[None]
+
+    def block_sum(slot, gain):
+        sent, kept = call(
+            functools.partial(mix_kernel, slot, n_sp),
+            [((rows, depth // n_tp), low), ((rows, depth // n_tp), wide)],
+            [pltpu.VMEM((rows, channels), low)],
+            (8 * rows * rows * n_sp * HEAD_DIM + 2 * rows * channels * depth, 8 * rows * width + 2 * depth * channels,
+             2 * rows * rows * n_sp),
+            [VMEM] * (n_sp + 3) + [SMEM, VMEM],
+            *projs, pool_map, pool_scale.reshape(n_sp, GROUP_DIM), gain, diff_lambda, out_weight,
+        )
+        return kept + swap(sent, "tp", 1).astype(wide)
+
+    sum_three = block_sum(3, gain).astype(low)
+    from_three = swap(sum_three, "sp", 1)
+    gain = after(gain, sum_three)
+    sum_two = (block_sum(2, gain) + from_three.astype(wide)).astype(low)
+    sum_one = after(block_sum(1, gain).astype(low), from_three)
+    from_two = swap(sum_two, "sp", 2)
+    from_one = swap(sum_one, "sp", 1)
+    result = block_sum(0, gain) + from_one.astype(wide) + from_two.astype(wide)
+    return result.astype(low)[None]
+
+
 def solution(mesh):
     placed = (
         P("fs", "sp", None),
@@ -201,6 +533,13 @@
         P("tp", ("sp", "fs")),
         P("tp", ("sp", "fs")),
     )
+
+    def body(*args):
+        n_sp, n_fs, n_tp = (mesh.shape[axis] for axis in ("sp", "fs", "tp"))
+        groups, heads = args[6].shape[0], args[5].shape[1] // (2 * HEAD_DIM)
+        pairs = groups == heads == n_sp == n_fs == 4 and n_tp == 2
+        return (spread if pairs else local)(*args)
+
     return jax.shard_map(
-        local, mesh=mesh, in_specs=placed, out_specs=P("fs", "sp", "tp"), check_vma=False
-    )
+        body, mesh=mesh, in_specs=placed, out_specs=P("fs", "sp", "tp"), check_vma=False
+    )

time: 575 us -> 163 us (0.28)
  waiting for transfers between devices: 487 us -> 73.4 us
  starting transfers between devices: 3.87 us -> 36.7 us
  matrix products: 31.8 us -> 0 us
  Pallas kernels: 0 us -> 28.7 us
  between operations: 13.8 us -> 0.42 us
  other arithmetic: 15.2 us -> 3.45 us
    all_gather x7 -> x0, waiting for transfers between devices: 477 us -> none  [the longest x1 136 us: local(): lax.all_gather(out_local, ('sp', 'fs'), axis=1, tiled=True)]
    ppermute x1 -> x34, waiting for transfers between devices: 0.67 us -> 73.4 us  [swap(): lax.ppermute(value, axis, [(i, i ^ bits) for i in range(lax.axis_size(axi...]
    ppermute x1 -> x34, starting transfers between devices: 3.59 us -> 36.7 us  [swap(): lax.ppermute(value, axis, [(i, i ^ bits) for i in range(lax.axis_size(axi...]
    dot_general x8 -> x0, matrix products: 31.8 us -> none  [the longest x4 16.7 us: local(): jnp.dot(normed, fragment, preferred_element_type=jnp.float32)]
    pallas_call x0 -> x14, Pallas kernels: none -> 28.7 us  [call(): pl.pallas_call(kernel, out_shape=[jax.ShapeDtypeStruct(shape, dtype) for...]
    unnamed x26 -> x88, local copies, waits for them, and re-layouts: 0.42 us -> 19.9 us
    another operation x4 -> x0, local copies, waits for them, and re-layouts: 9.58 us -> none  [local(): jnp.stack([pair_sums[14:14 + row_count], quad_sums[12:12 + row_count], oc...]
    reduce_scatter x1 -> x0, waiting for transfers between devices: 6.73 us -> none  [local(): lax.psum_scatter(partial_value.astype(jnp.bfloat16), 'tp', scatter_dimens...]
  transfers between devices with their start and end apart: 9 -> 34, of which waited for: 9 -> 17; matrix products, arithmetic and copies ran while one was open for 11% -> 1% of each run, Pallas kernels for 0% -> 12%
where the time goes in v2:
time: 163 us
  waiting for transfers between devices  73.4 us (45%)
  starting transfers between devices  36.7 us (23%)
  Pallas kernels  28.7 us (18%)
  local copies, waits for them, and re-layouts  20 us (12%)
  other arithmetic  3.45 us (2%)
    ppermute x34, waiting for transfers between devices, swap(): lax.ppermute(value, axis, [(i, i ^ bits) for i in range(lax.axis_size(axi...  73.4 us
    ppermute x34, starting transfers between devices, swap(): lax.ppermute(value, axis, [(i, i ^ bits) for i in range(lax.axis_size(axi...  36.7 us
    pallas_call x14, Pallas kernels, call(): pl.pallas_call(kernel, out_shape=[jax.ShapeDtypeStruct(shape, dtype) for...  28.7 us
    unnamed x88, local copies, waits for them, and re-layouts  19.9 us
  transfers between devices with their start and end apart: 34, of which 17 were waited for; matrix products, arithmetic and copies ran while one was open for 1% of the time, Pallas kernels for 12%

profile of v2, /device:TPU:0, one launch (start us, length us, event | category | flops | bytes accessed | tf_op | source)
XLA Modules:
  0.0 162.7 jit_solution(305734647023731533)
XLA Ops:
  0.0 2.4 %shard_map.127 = (bf16[128,1024]{1,0:T(8,128)(2,1)}, bf16[128,1024]{1,0:T(8,128)(2,1)}, bf16[128,1024]{1,0:T(8,128)(2,1)}, bf16[128,1024]{1,0:T(8,128)(2,1)}) custom-call(bf16[128,1024]{1,0:T(8,128)(2,1)} %refs_0_.2, bf16[128,1024]{1,0:T(8,128)(2,1)} %refs_1_.2, bf16[128,1024]{1,0:T(8,128)(2,1)} %refs_2_.2, bf16[128,1024]{1,0:T(8,128)(2,1)} %refs_3_.4), custom_call_target="tpu_custom_call" | custom-call | bytes 2097152 | tf_op jit(solution)/shard_map/pallas_call | solution.py:203
  2.4 3.1 %collective-permute-start.3 = (bf16[128,1024]{1,0:T(8,128)(2,1)}, bf16[128,1024]{1,0:T(8,128)(2,1)S(1)}, u32[]{:S(2)}, u32[]{:S(2)}) collective-permute-start(bf16[128,1024]{1,0:T(8,128)(2,1)} %get-tuple-element.28), channel_id=1, source_target_pairs={{0,8},{8,0},{16,24},{24,16},{1,9},{9,1},{17,25},{25,17},{2,10},{10... | collective-permute-start | bytes 786440 | tf_op jit(solution)/shard_map/ppermute | solution.py:348
  5.6 2.6 %collective-permute-start.4 = (bf16[128,1024]{1,0:T(8,128)(2,1)}, bf16[128,1024]{1,0:T(8,128)(2,1)S(1)}, u32[]{:S(2)}, u32[]{:S(2)}) collective-permute-start(bf16[128,1024]{1,0:T(8,128)(2,1)} %get-tuple-element.29), channel_id=1, source_target_pairs={{0,16},{8,24},{16,0},{24,8},{1,17},{9,25},{17,1},{25,9},{2,18},{10... | collective-permute-start | bytes 786440 | tf_op jit(solution)/shard_map/ppermute | solution.py:348
  8.2 1.9 %shard_map.134 = (bf16[512,128]{1,0:T(8,128)(2,1)}, bf16[512,128]{1,0:T(8,128)(2,1)}, bf16[512,128]{1,0:T(8,128)(2,1)}, bf16[512,128]{1,0:T(8,128)(2,1)}) custom-call(bf16[1024,128]{1,0:T(8,128)(2,1)} %refs_0_.3, bf16[1024,128]{1,0:T(8,128)(2,1)} %refs_1_.3), custom_call_target="tpu_custom_call" | custom-call | bytes 1048576 | tf_op jit(solution)/shard_map/pallas_call | solution.py:203
  11.1 3.5 %collective-permute-start.19 = (bf16[512,128]{1,0:T(8,128)(2,1)}, bf16[512,128]{1,0:T(8,128)(2,1)S(1)}, u32[]{:S(2)}, u32[]{:S(2)}) collective-permute-start(bf16[512,128]{1,0:T(8,128)(2,1)} %get-tuple-element.35), channel_id=1, source_target_pairs={{0,16},{8,24},{16,0},{24,8},{1,17},{9,25},{17,1},{25,9},{2,18},{10... | collective-permute-start | bytes 393224 | tf_op jit(solution)/shard_map/ppermute | solution.py:348
  14.9 11.8 %collective-permute-done.18.refs_1_ = bf16[512,128]{1,0:T(8,128)(2,1)S(1)} collective-permute-done((bf16[512,128]{1,0:T(8,128)(2,1)}, bf16[512,128]{1,0:T(8,128)(2,1)S(1)}, u32[]{:S(2)}, u32[]{:S(2)}) %collective-permute-start.18) | collective-permute-done | bytes 131104 | tf_op jit(solution)/shard_map/ppermute | solution.py:348
  28.2 8.8 %collective-permute-done.19.refs_2_ = bf16[512,128]{1,0:T(8,128)(2,1)S(1)} collective-permute-done((bf16[512,128]{1,0:T(8,128)(2,1)}, bf16[512,128]{1,0:T(8,128)(2,1)S(1)}, u32[]{:S(2)}, u32[]{:S(2)}) %collective-permute-start.19) | collective-permute-done | bytes 131104 | tf_op jit(solution)/shard_map/ppermute | solution.py:348
  37.0 2.9 %collective-permute-start.20 = (bf16[512,128]{1,0:T(8,128)(2,1)}, bf16[512,128]{1,0:T(8,128)(2,1)S(1)}, u32[]{:S(2)}, u32[]{:S(2)}) collective-permute-start(bf16[512,128]{1,0:T(8,128)(2,1)} %get-tuple-element.36), channel_id=1, source_target_pairs={{0,24},{8,16},{16,8},{24,0},{1,25},{9,17},{17,9},{25,1},{2,26},{10... | collective-permute-start | bytes 393224 | tf_op jit(solution)/shard_map/ppermute | solution.py:348
  41.4 2.6 %collective-permute-done.20.refs_3_ = bf16[512,128]{1,0:T(8,128)(2,1)S(1)} collective-permute-done((bf16[512,128]{1,0:T(8,128)(2,1)}, bf16[512,128]{1,0:T(8,128)(2,1)S(1)}, u32[]{:S(2)}, u32[]{:S(2)}) %collective-permute-start.20) | collective-permute-done | bytes 131104 | tf_op jit(solution)/shard_map/ppermute | solution.py:348
  53.1 5.8 %collective-permute-done.1.refs_2_ = bf16[128,1024]{1,0:T(8,128)(2,1)S(1)} collective-permute-done((bf16[128,1024]{1,0:T(8,128)(2,1)S(1)}, bf16[128,1024]{1,0:T(8,128)(2,1)S(1)}, u32[]{:S(2)}, u32[]{:S(2)}) %collective-permute-start.1) | collective-permute-done | bytes 262176 | tf_op jit(solution)/shard_map/ppermute | solution.py:348
  60.3 1.9 %collective-permute-start.21 = (bf16[1024,128]{1,0:T(8,128)(2,1)S(1)}, bf16[1024,128]{1,0:T(8,128)(2,1)S(1)}, u32[]{:S(2)}, u32[]{:S(2)}) collective-permute-start(bf16[1024,128]{1,0:T(8,128)(2,1)S(1)} %get-tuple-element.37.refs_0_), channel_id=1, source_target_pairs={{0,2},{2,0},{4,6},{6,4},{1,3},{3,1},{5,7},{7,5},{8,10},{10,8},{12,... | collective-permute-start | bytes 786440 | tf_op jit(solution)/shard_map/ppermute | solution.py:348
  82.0 5.7 %collective-permute-done.6.refs_6_ = bf16[192,1024]{1,0:T(8,128)(2,1)S(1)} collective-permute-done((bf16[192,1024]{1,0:T(8,128)(2,1)S(1)}, bf16[192,1024]{1,0:T(8,128)(2,1)S(1)}, u32[]{:S(2)}, u32[]{:S(2)}) %collective-permute-start.6) | collective-permute-done | bytes 393248 | tf_op jit(solution)/shard_map/ppermute | solution.py:348
  102.2 3.9 %shard_map.129.refs_1_.refs_2_ = bf16[2048,1024]{1,0:T(8,128)(2,1)S(1)} custom-call(bf16[128,1024]{1,0:T(8,128)(2,1)S(1)} %copy-done.9, bf16[128,1024]{1,0:T(8,128)(2,1)S(1)} %copy-done.11, bf16[128,1024]{1,0:T(8,128)(2,1)S(1)} %copy-done.13, bf16[128,1024]{1,0:T(8,128)(2,1)S(1)} %copy-done.15, bf16[192,1024]{1,0:T(8,128)(2,1)S(1)} %get-tuple-element.31.refs_4_, ...), custom_call_target="tpu_custom_call" | custom-call | bytes 8388608 | tf_op jit(solution)/shard_map/pallas_call | solution.py:203
  108.9 2.4 %shard_map.131.refs_1_ = bf16[256,1024]{1,0:T(8,128)(2,1)S(1)} custom-call(bf16[128,2048]{1,0:T(8,128)(2,1)S(1)} %collective-permute-done.12.refs_0_, bf16[128,2048]{1,0:T(8,128)(2,1)} %collective-permute-done.13.refs_1_, bf16[2048,1024]{1,0:T(8,128)(2,1)S(1)} %shard_map.129.refs_1_.refs_2_, f32[1024,128]{1,0:T(8,128)S(1)} %copy-done.1), custom_call_target="tpu_custom_call" | custom-call | flops 1073741824 | bytes 4194304 | tf_op jit(solution)/shard_map/pallas_call | solution.py:203
  111.3 2.4 %shard_map.133.refs_3_ = bf16[256,1024]{1,0:T(8,128)(2,1)S(1)} custom-call(bf16[128,2048]{1,0:T(8,128)(2,1)S(1)} %collective-permute-done.16.refs_0_, bf16[128,2048]{1,0:T(8,128)(2,1)} %collective-permute-done.17.refs_1_, bf16[2048,1024]{1,0:T(8,128)(2,1)S(1)} %shard_map.129.refs_1_.refs_2_, f32[1024,128]{1,0:T(8,128)S(1)} %copy-done.1), custom_call_target="tpu_custom_call" | custom-call | flops 1073741824 | bytes 4194304 | tf_op jit(solution)/shard_map/pallas_call | solution.py:203
  113.8 2.6 %shard_map.137 = (bf16[256,1024]{1,0:T(8,128)(2,1)S(1)}, f32[256,1024]{1,0:T(8,128)S(1)}) custom-call(bf16[256,1024]{1,0:T(8,128)(2,1)S(1)} %shard_map.130.refs_0_, bf16[256,1024]{1,0:T(8,128)(2,1)S(1)} %shard_map.131.refs_1_, bf16[256,1024]{1,0:T(8,128)(2,1)S(1)} %shard_map.132.refs_2_, bf16[256,1024]{1,0:T(8,128)(2,1)S(1)} %shard_map.133.refs_3_, ...), custom_call_target="tpu_custom_call" | custom-call | flops 805306368 | bytes 4194304 | tf_op jit(solution)/shard_map/pallas_call | solution.py:203
  116.5 1.8 %collective-permute-done.27 = bf16[256,1024]{1,0:T(8,128)(2,1)S(1)} collective-permute-done((bf16[256,1024]{1,0:T(8,128)(2,1)S(1)}, bf16[256,1024]{1,0:T(8,128)(2,1)S(1)}, u32[]{:S(2)}, u32[]{:S(2)}) %collective-permute-start.27) | collective-permute-done | bytes 524320 | tf_op jit(solution)/shard_map/ppermute | solution.py:348
  118.5 2.5 %shard_map.139 = (bf16[256,1024]{1,0:T(8,128)(2,1)S(1)}, f32[256,1024]{1,0:T(8,128)S(1)}) custom-call(bf16[256,1024]{1,0:T(8,128)(2,1)S(1)} %shard_map.130.refs_0_, bf16[256,1024]{1,0:T(8,128)(2,1)S(1)} %shard_map.131.refs_1_, bf16[256,1024]{1,0:T(8,128)(2,1)S(1)} %shard_map.132.refs_2_, bf16[256,1024]{1,0:T(8,128)(2,1)S(1)} %shard_map.133.refs_3_, ...), custom_call_target="tpu_custom_call" | custom-call | flops 805306368 | bytes 4194304 | tf_op jit(solution)/shard_map/pallas_call | solution.py:203
  121.8 2.5 %shard_map.140 = (bf16[256,1024]{1,0:T(8,128)(2,1)S(1)}, f32[256,1024]{1,0:T(8,128)S(1)}) custom-call(bf16[256,1024]{1,0:T(8,128)(2,1)S(1)} %shard_map.130.refs_0_, bf16[256,1024]{1,0:T(8,128)(2,1)S(1)} %shard_map.131.refs_1_, bf16[256,1024]{1,0:T(8,128)(2,1)S(1)} %shard_map.132.refs_2_, bf16[256,1024]{1,0:T(8,128)(2,1)S(1)} %shard_map.133.refs_3_, ...), custom_call_target="tpu_custom_call" | custom-call | flops 805306368 | bytes 4194304 | tf_op jit(solution)/shard_map/pallas_call | solution.py:203
  124.5 2.5 %shard_map.138 = (bf16[256,1024]{1,0:T(8,128)(2,1)S(1)}, f32[256,1024]{1,0:T(8,128)S(1)}) custom-call(bf16[256,1024]{1,0:T(8,128)(2,1)S(1)} %shard_map.130.refs_0_, bf16[256,1024]{1,0:T(8,128)(2,1)S(1)} %shard_map.131.refs_1_, bf16[256,1024]{1,0:T(8,128)(2,1)S(1)} %shard_map.132.refs_2_, bf16[256,1024]{1,0:T(8,128)(2,1)S(1)} %shard_map.133.refs_3_, ...), custom_call_target="tpu_custom_call" | custom-call | flops 805306368 | bytes 4194304 | tf_op jit(solution)/shard_map/pallas_call | solution.py:203
  127.7 7.7 %collective-permute-done.30 = bf16[256,1024]{1,0:T(8,128)(2,1)S(1)} collective-permute-done((bf16[256,1024]{1,0:T(8,128)(2,1)S(1)}, bf16[256,1024]{1,0:T(8,128)(2,1)S(1)}, u32[]{:S(2)}, u32[]{:S(2)}) %collective-permute-start.30) | collective-permute-done | bytes 524320 | tf_op jit(solution)/shard_map/ppermute | solution.py:348
  136.3 2.4 %collective-permute-start.33 = (bf16[256,1024]{1,0:T(8,128)(2,1)S(1)}, bf16[256,1024]{1,0:T(8,128)(2,1)S(1)}, u32[]{:S(2)}, u32[]{:S(2)}) collective-permute-start(bf16[256,1024]{1,0:T(8,128)(2,1)S(1)} %add_convert_fusion.1), channel_id=1, source_target_pairs={{0,16},{8,24},{16,0},{24,8},{1,17},{9,25},{17,1},{25,9},{2,18},{10... | collective-permute-start | bytes 1572872 | tf_op jit(solution)/shard_map/ppermute | solution.py:348
  138.6 20.9 %collective-permute-done.31 = bf16[256,1024]{1,0:T(8,128)(2,1)S(1)} collective-permute-done((bf16[256,1024]{1,0:T(8,128)(2,1)S(1)}, bf16[256,1024]{1,0:T(8,128)(2,1)S(1)}, u32[]{:S(2)}, u32[]{:S(2)}) %collective-permute-start.31) | collective-permute-done | bytes 524320 | tf_op jit(solution)/shard_map/ppermute | solution.py:348
  159.5 2.1 %collective-permute-done.33 = bf16[256,1024]{1,0:T(8,128)(2,1)S(1)} collective-permute-done((bf16[256,1024]{1,0:T(8,128)(2,1)S(1)}, bf16[256,1024]{1,0:T(8,128)(2,1)S(1)}, u32[]{:S(2)}, u32[]{:S(2)}) %collective-permute-start.33) | collective-permute-done | bytes 524320 | tf_op jit(solution)/shard_map/ppermute | solution.py:348
  (155 shorter events, 55.4 us)
Async XLA Ops:
  2.4 45.4 %collective-permute-start.3 = (bf16[128,1024]{1,0:T(8,128)(2,1)}, bf16[128,1024]{1,0:T(8,128)(2,1)S(1)}, u32[]{:S(2)}, u32[]{:S(2)}) collective-permute-start(bf16[128,1024]{1,0:T(8,128)(2,1)} %get-tuple-element.28), channel_id=1, source_target_pairs={{0,8},{8,0},{16,24},{24,16},{1,9},{9,1},{17,25},{25,17},{2,10},{10... | collective-permute-start | bytes 786440 | tf_op jit(solution)/shard_map/ppermute | solution.py:348
  5.6 43.8 %collective-permute-start.4 = (bf16[128,1024]{1,0:T(8,128)(2,1)}, bf16[128,1024]{1,0:T(8,128)(2,1)S(1)}, u32[]{:S(2)}, u32[]{:S(2)}) collective-permute-start(bf16[128,1024]{1,0:T(8,128)(2,1)} %get-tuple-element.29), channel_id=1, source_target_pairs={{0,16},{8,24},{16,0},{24,8},{1,17},{9,25},{17,1},{25,9},{2,18},{10... | collective-permute-start | bytes 786440 | tf_op jit(solution)/shard_map/ppermute | solution.py:348
  8.2 42.8 %collective-permute-start.5 = (bf16[128,1024]{1,0:T(8,128)(2,1)}, bf16[128,1024]{1,0:T(8,128)(2,1)S(1)}, u32[]{:S(2)}, u32[]{:S(2)}) collective-permute-start(bf16[128,1024]{1,0:T(8,128)(2,1)} %get-tuple-element.30), channel_id=1, source_target_pairs={{0,24},{8,16},{16,8},{24,0},{1,25},{9,17},{17,9},{25,1},{2,26},{10... | collective-permute-start | bytes 786440 | tf_op jit(solution)/shard_map/ppermute | solution.py:348
  10.1 16.6 %collective-permute-start.18 = (bf16[512,128]{1,0:T(8,128)(2,1)}, bf16[512,128]{1,0:T(8,128)(2,1)S(1)}, u32[]{:S(2)}, u32[]{:S(2)}) collective-permute-start(bf16[512,128]{1,0:T(8,128)(2,1)} %get-tuple-element.34), channel_id=1, source_target_pairs={{0,8},{8,0},{16,24},{24,16},{1,9},{9,1},{17,25},{25,17},{2,10},{10... | collective-permute-start | bytes 393224 | tf_op jit(solution)/shard_map/ppermute | solution.py:348
  11.1 25.9 %collective-permute-start.19 = (bf16[512,128]{1,0:T(8,128)(2,1)}, bf16[512,128]{1,0:T(8,128)(2,1)S(1)}, u32[]{:S(2)}, u32[]{:S(2)}) collective-permute-start(bf16[512,128]{1,0:T(8,128)(2,1)} %get-tuple-element.35), channel_id=1, source_target_pairs={{0,16},{8,24},{16,0},{24,8},{1,17},{9,25},{17,1},{25,9},{2,18},{10... | collective-permute-start | bytes 393224 | tf_op jit(solution)/shard_map/ppermute | solution.py:348
  26.7 25.5 %collective-permute-start = (bf16[128,1024]{1,0:T(8,128)(2,1)}, bf16[128,1024]{1,0:T(8,128)(2,1)S(1)}, u32[]{:S(2)}, u32[]{:S(2)}) collective-permute-start(bf16[128,1024]{1,0:T(8,128)(2,1)} %get-tuple-element.27.refs_0_), channel_id=1, source_target_pairs={{0,2},{2,0},{4,6},{6,4},{1,3},{3,1},{5,7},{7,5},{8,10},{10,8},{12,... | collective-permute-start | bytes 786440 | tf_op jit(solution)/shard_map/ppermute | solution.py:348
  44.7 14.2 %collective-permute-start.1 = (bf16[128,1024]{1,0:T(8,128)(2,1)S(1)}, bf16[128,1024]{1,0:T(8,128)(2,1)S(1)}, u32[]{:S(2)}, u32[]{:S(2)}) collective-permute-start(bf16[128,1024]{1,0:T(8,128)(2,1)S(1)} %copy-done.8), channel_id=1, source_target_pairs={{0,4},{2,6},{4,0},{6,2},{1,5},{3,7},{5,1},{7,3},{8,12},{10,14},{12... | collective-permute-start | bytes 786440 | tf_op jit(solution)/shard_map/ppermute | solution.py:348
  47.9 11.7 %collective-permute-start.2 = (bf16[128,1024]{1,0:T(8,128)(2,1)S(1)}, bf16[128,1024]{1,0:T(8,128)(2,1)S(1)}, u32[]{:S(2)}, u32[]{:S(2)}) collective-permute-start(bf16[128,1024]{1,0:T(8,128)(2,1)S(1)} %copy-done.8), channel_id=1, source_target_pairs={{0,6},{2,4},{4,2},{6,0},{1,7},{3,5},{5,3},{7,1},{8,14},{10,12},{12... | collective-permute-start | bytes 786440 | tf_op jit(solution)/shard_map/ppermute | solution.py:348
  49.4 12.9 %collective-permute-start.23 = (bf16[1024,128]{1,0:T(8,128)(2,1)S(1)}, bf16[1024,128]{1,0:T(8,128)(2,1)S(1)}, u32[]{:S(2)}, u32[]{:S(2)}) collective-permute-start(bf16[1024,128]{1,0:T(8,128)(2,1)S(1)} %get-tuple-element.37.refs_0_), channel_id=1, source_target_pairs={{0,4},{2,6},{4,0},{6,2},{1,5},{3,7},{5,1},{7,3},{8,12},{10,14},{12... | collective-permute-start | bytes 786440 | tf_op jit(solution)/shard_map/ppermute | solution.py:348
  51.7 14.7 %collective-permute-start.22 = (bf16[1024,128]{1,0:T(8,128)(2,1)S(1)}, bf16[1024,128]{1,0:T(8,128)(2,1)S(1)}, u32[]{:S(2)}, u32[]{:S(2)}) collective-permute-start(bf16[1024,128]{1,0:T(8,128)(2,1)S(1)} %get-tuple-element.38.refs_1_), channel_id=1, source_target_pairs={{0,2},{2,0},{4,6},{6,4},{1,3},{3,1},{5,7},{7,5},{8,10},{10,8},{12,... | collective-permute-start | bytes 786440 | tf_op jit(solution)/shard_map/ppermute | solution.py:348
  52.9 22.3 %collective-permute-start.14 = (bf16[128,2048]{1,0:T(8,128)(2,1)S(1)}, bf16[128,2048]{1,0:T(8,128)(2,1)S(1)}, u32[]{:S(2)}, u32[]{:S(2)}) collective-permute-start(bf16[128,2048]{1,0:T(8,128)(2,1)S(1)} %constant_dynamic-slice_fusion), channel_id=1, source_target_pairs={{0,16},{8,24},{16,0},{24,8},{1,17},{9,25},{17,1},{25,9},{2,18},{10... | collective-permute-start | bytes 1572872 | tf_op jit(solution)/shard_map/ppermute | solution.py:348
  59.6 18.2 %collective-permute-start.12 = (bf16[128,2048]{1,0:T(8,128)(2,1)S(1)}, bf16[128,2048]{1,0:T(8,128)(2,1)S(1)}, u32[]{:S(2)}, u32[]{:S(2)}) collective-permute-start(bf16[128,2048]{1,0:T(8,128)(2,1)S(1)} %constant_dynamic-slice_fusion), channel_id=1, source_target_pairs={{0,8},{8,0},{16,24},{24,16},{1,9},{9,1},{17,25},{25,17},{2,10},{10... | collective-permute-start | bytes 1572872 | tf_op jit(solution)/shard_map/ppermute | solution.py:348
  68.1 12.1 %collective-permute-start.7 = (bf16[192,1024]{1,0:T(8,128)(2,1)S(1)}, bf16[192,1024]{1,0:T(8,128)(2,1)}, u32[]{:S(2)}, u32[]{:S(2)}) collective-permute-start(bf16[192,1024]{1,0:T(8,128)(2,1)S(1)} %get-tuple-element.32.refs_5_), channel_id=1, source_target_pairs={{0,2},{2,0},{4,6},{6,4},{1,3},{3,1},{5,7},{7,5},{8,10},{10,8},{12,... | collective-permute-start | bytes 1179656 | tf_op jit(solution)/shard_map/ppermute | solution.py:348
  72.0 15.6 %collective-permute-start.6 = (bf16[192,1024]{1,0:T(8,128)(2,1)S(1)}, bf16[192,1024]{1,0:T(8,128)(2,1)S(1)}, u32[]{:S(2)}, u32[]{:S(2)}) collective-permute-start(bf16[192,1024]{1,0:T(8,128)(2,1)S(1)} %get-tuple-element.31.refs_4_), channel_id=1, source_target_pairs={{0,2},{2,0},{4,6},{6,4},{1,3},{3,1},{5,7},{7,5},{8,10},{10,8},{12,... | collective-permute-start | bytes 1179656 | tf_op jit(solution)/shard_map/ppermute | solution.py:348
  75.2 13.2 %collective-permute-start.9 = (bf16[192,1024]{1,0:T(8,128)(2,1)S(1)}, bf16[192,1024]{1,0:T(8,128)(2,1)S(1)}, u32[]{:S(2)}, u32[]{:S(2)}) collective-permute-start(bf16[192,1024]{1,0:T(8,128)(2,1)S(1)} %get-tuple-element.32.refs_5_), channel_id=1, source_target_pairs={{0,4},{2,6},{4,0},{6,2},{1,5},{3,7},{5,1},{7,3},{8,12},{10,14},{12... | collective-permute-start | bytes 1179656 | tf_op jit(solution)/shard_map/ppermute | solution.py:348
  77.8 14.8 %collective-permute-start.16 = (bf16[128,2048]{1,0:T(8,128)(2,1)S(1)}, bf16[128,2048]{1,0:T(8,128)(2,1)S(1)}, u32[]{:S(2)}, u32[]{:S(2)}) collective-permute-start(bf16[128,2048]{1,0:T(8,128)(2,1)S(1)} %collective-permute-done.14.refs_0_), channel_id=1, source_target_pairs={{0,8},{8,0},{16,24},{24,16},{1,9},{9,1},{17,25},{25,17},{2,10},{10... | collective-permute-start | bytes 1572872 | tf_op jit(solution)/shard_map/ppermute | solution.py:348
  77.8 12.7 %collective-permute-start.25 = (bf16[1024,128]{1,0:T(8,128)(2,1)S(1)}, bf16[1024,128]{1,0:T(8,128)(2,1)S(1)}, u32[]{:S(2)}, u32[]{:S(2)}) collective-permute-start(bf16[1024,128]{1,0:T(8,128)(2,1)S(1)} %collective-permute-done.23.refs_4_), channel_id=1, source_target_pairs={{0,2},{2,0},{4,6},{6,4},{1,3},{3,1},{5,7},{7,5},{8,10},{10,8},{12,... | collective-permute-start | bytes 786440 | tf_op jit(solution)/shard_map/ppermute | solution.py:348
  88.4 19.1 %collective-permute-start.15 = (bf16[128,2048]{1,0:T(8,128)(2,1)S(1)}, bf16[128,2048]{1,0:T(8,128)(2,1)S(1)}, u32[]{:S(2)}, u32[]{:S(2)}) collective-permute-start(bf16[128,2048]{1,0:T(8,128)(2,1)S(1)} %collective-permute-done.14.refs_0_), channel_id=1, source_target_pairs={{0,1},{1,0},{2,3},{3,2},{4,5},{5,4},{6,7},{7,6},{8,9},{9,8},{10,11... | collective-permute-start | bytes 1572872 | tf_op jit(solution)/shard_map/ppermute | solution.py:348
  89.2 12.6 %collective-permute-start.10 = (bf16[192,1024]{1,0:T(8,128)(2,1)}, bf16[192,1024]{1,0:T(8,128)(2,1)}, u32[]{:S(2)}, u32[]{:S(2)}) collective-permute-start(bf16[192,1024]{1,0:T(8,128)(2,1)} %collective-permute-done.8.refs_8_), channel_id=1, source_target_pairs={{0,2},{2,0},{4,6},{6,4},{1,3},{3,1},{5,7},{7,5},{8,10},{10,8},{12,... | collective-permute-start | bytes 1179656 | tf_op jit(solution)/shard_map/ppermute | solution.py:348
  92.5 16.3 %collective-permute-start.13 = (bf16[128,2048]{1,0:T(8,128)(2,1)S(1)}, bf16[128,2048]{1,0:T(8,128)(2,1)}, u32[]{:S(2)}, u32[]{:S(2)}) collective-permute-start(bf16[128,2048]{1,0:T(8,128)(2,1)S(1)} %collective-permute-done.12.refs_0_), channel_id=1, source_target_pairs={{0,1},{1,0},{2,3},{3,2},{4,5},{5,4},{6,7},{7,6},{8,9},{9,8},{10,11... | collective-permute-start | bytes 1572872 | tf_op jit(solution)/shard_map/ppermute | solution.py:348
  92.6 18.7 %collective-permute-start.17 = (bf16[128,2048]{1,0:T(8,128)(2,1)S(1)}, bf16[128,2048]{1,0:T(8,128)(2,1)}, u32[]{:S(2)}, u32[]{:S(2)}) collective-permute-start(bf16[128,2048]{1,0:T(8,128)(2,1)S(1)} %collective-permute-done.16.refs_0_), channel_id=1, source_target_pairs={{0,1},{1,0},{2,3},{3,2},{4,5},{5,4},{6,7},{7,6},{8,9},{9,8},{10,11... | collective-permute-start | bytes 1572872 | tf_op jit(solution)/shard_map/ppermute | solution.py:348
  121.2 14.2 %collective-permute-start.30 = (bf16[256,1024]{1,0:T(8,128)(2,1)S(1)}, bf16[256,1024]{1,0:T(8,128)(2,1)S(1)}, u32[]{:S(2)}, u32[]{:S(2)}) collective-permute-start(bf16[256,1024]{1,0:T(8,128)(2,1)S(1)} %add_convert_fusion.3), channel_id=1, source_target_pairs={{0,8},{8,0},{16,24},{24,16},{1,9},{9,1},{17,25},{25,17},{2,10},{10... | collective-permute-start | bytes 1572872 | tf_op jit(solution)/shard_map/ppermute | solution.py:348
  135.4 24.1 %collective-permute-start.31 = (bf16[256,1024]{1,0:T(8,128)(2,1)S(1)}, bf16[256,1024]{1,0:T(8,128)(2,1)S(1)}, u32[]{:S(2)}, u32[]{:S(2)}) collective-permute-start(bf16[256,1024]{1,0:T(8,128)(2,1)S(1)} %add_convert_fusion.2), channel_id=1, source_target_pairs={{0,8},{8,0},{16,24},{24,16},{1,9},{9,1},{17,25},{25,17},{2,10},{10... | collective-permute-start | bytes 1572872 | tf_op jit(solution)/shard_map/ppermute | solution.py:348
  136.3 25.3 %collective-permute-start.33 = (bf16[256,1024]{1,0:T(8,128)(2,1)S(1)}, bf16[256,1024]{1,0:T(8,128)(2,1)S(1)}, u32[]{:S(2)}, u32[]{:S(2)}) collective-permute-start(bf16[256,1024]{1,0:T(8,128)(2,1)S(1)} %add_convert_fusion.1), channel_id=1, source_target_pairs={{0,16},{8,24},{16,0},{24,8},{1,17},{9,25},{17,1},{25,9},{2,18},{10... | collective-permute-start | bytes 1572872 | tf_op jit(solution)/shard_map/ppermute | solution.py:348
  (54 other events, 401.9 us)

commit v3 on v2

--- a/solution.py
+++ b/solution.py
@@ -194,7 +194,7 @@
 VMEM = pl.BlockSpec(memory_space=pltpu.VMEM)
 SMEM = pl.BlockSpec(memory_space=pltpu.SMEM)
 HBM = pl.BlockSpec(memory_space=pltpu.HBM)
-VMEM_LIMIT = 24 * 1024 * 1024
+VMEM_LIMIT = 16 * 1024 * 1024
 WHOLE_VMEM = 60 * 1024 * 1024
 
 
@@ -228,6 +228,15 @@
         kernel, outs, [pltpu.SemaphoreType.DMA((count,))], (0, moved, 0), [HBM] * len(args), *args,
         limit=limit,
     )
+
+
+def place(pairs_of, outs, *args):
+    def kernel(*refs):
+        for source, target in pairs_of(refs[: len(args)], refs[len(args) :]):
+            target[...] = source[...]
+
+    moved = sum(2 * math.prod(shape) * 2 for shape, _ in outs)
+    return call(kernel, outs, [], (0, moved, 0), [VMEM] * len(args), *args)
 
 
 def tiles(start, size):
@@ -336,7 +345,7 @@
     own_pos = block * rows + lax.broadcasted_iota(jnp.int32, (rows, GROUP_DIM), 0)
     counts = jnp.minimum(own_pos + 1, window).astype(jnp.float32)
     mixed = (picked / counts - flat[reach:]).astype(jnp.bfloat16)
-    pooled = jnp.dot(mixed, map_ref[place], preferred_element_type=jnp.float32) * scale_ref[pl.ds(place, 1)]
+    pooled = jnp.dot(mixed, map_ref[place], preferred_element_type=jnp.float32) * scale_ref[:, tiles(place, GROUP_DIM)]
     branch_ref[:, :GROUP_DIM] = pooled.astype(jnp.bfloat16)
     sent_ref[...] = jnp.dot(
         branch_ref[...], w_ref[1], preferred_element_type=jnp.float32
@@ -406,7 +415,7 @@
             for i, source in enumerate(sources)
         ]
 
-    bundled = move(bundle, [(((n_sp - 1) * half_shard, width), low)] * 2, 2 * (n_sp - 1), *far)
+    bundled = place(bundle, [(((n_sp - 1) * half_shard, width), low)] * 2, *far)
     distant = [part for pair in square(*bundled) for part in pair]
 
     def assemble(sources, targets):
@@ -421,7 +430,7 @@
                     pairs.append((source, targets[0].at[tiles(2 * place + side, half_shard)]))
         return pairs
 
-    (weight,) = move(assemble, [((depth, width), low)], n_fs * (2 * n_sp - 1), *near, *distant)
+    (weight,) = place(assemble, [((depth, width), low)], *near, *distant)
 
     size = channels // 2
 
@@ -446,7 +455,7 @@
             for j, source in enumerate(sources)
         ]
 
-    bundled_out = move(bundle_out, [((n_sp * size, shard), low)] * 2, 2 * n_sp, *far_out)
+    bundled_out = place(bundle_out, [((n_sp * size, shard), low)] * 2, *far_out)
 
     def assemble_out(sources, targets):
         sp, fs, tp = (lax.axis_index(axis) for axis in ("sp", "fs", "tp"))
@@ -462,8 +471,8 @@
                     pairs.append((source, target.at[tiles(side, size), here]))
         return pairs
 
-    (out_weight,) = move(
-        assemble_out, [((n_tp, channels, depth // n_tp), low)], 2 * n_sp * n_fs,
+    (out_weight,) = place(
+        assemble_out, [((n_tp, channels, depth // n_tp), low)],
         *[part for pair in square(*bundled_out) for part in pair],
     )
 
@@ -503,7 +512,7 @@
             (8 * rows * rows * n_sp * HEAD_DIM + 2 * rows * channels * depth, 8 * rows * width + 2 * depth * channels,
              2 * rows * rows * n_sp),
             [VMEM] * (n_sp + 3) + [SMEM, VMEM],
-            *projs, pool_map, pool_scale.reshape(n_sp, GROUP_DIM), gain, diff_lambda, out_weight,
+            *projs, pool_map, pool_scale[None], gain, diff_lambda, out_weight,
         )
         return kept + swap(sent, "tp", 1).astype(wide)
 

time: 163 us -> 154 us (0.945)
  local copies, waits for them, and re-layouts: 20 us -> 0.08 us
  waiting for transfers between devices: 73.4 us -> 89 us
  Pallas kernels: 28.7 us -> 21 us
  starting transfers between devices: 36.7 us -> 39.8 us
    unnamed x88 -> x18, local copies, waits for them, and re-layouts: 19.9 us -> 0.05 us
    ppermute x34, waiting for transfers between devices: 73.4 us -> 89 us  [swap(): lax.ppermute(value, axis, [(i, i ^ bits) for i in range(lax.axis_size(axi...]
    pallas_call x14, Pallas kernels: 28.7 us -> 21 us  [call(): pl.pallas_call(kernel, out_shape=[jax.ShapeDtypeStruct(shape, dtype) for...]
    ppermute x34, starting transfers between devices: 36.7 us -> 39.8 us  [swap(): lax.ppermute(value, axis, [(i, i ^ bits) for i in range(lax.axis_size(axi...]
  transfers between devices with their start and end apart: 34 -> 34, of which waited for: 17 -> 18; matrix products, arithmetic and copies ran while one was open for 1% -> 1% of each run, Pallas kernels for 12% -> 8%
where the time goes in v3:
time: 154 us
  waiting for transfers between devices  89 us (58%)
  starting transfers between devices  39.8 us (26%)
  Pallas kernels  21 us (14%)
  other arithmetic  3.49 us (2%)
    ppermute x34, waiting for transfers between devices, swap(): lax.ppermute(value, axis, [(i, i ^ bits) for i in range(lax.axis_size(axi...  89 us
    ppermute x34, starting transfers between devices, swap(): lax.ppermute(value, axis, [(i, i ^ bits) for i in range(lax.axis_size(axi...  39.8 us
    pallas_call x14, Pallas kernels, call(): pl.pallas_call(kernel, out_shape=[jax.ShapeDtypeStruct(shape, dtype) for...  21 us
  transfers between devices with their start and end apart: 34, of which 18 were waited for; matrix products, arithmetic and copies ran while one was open for 1% of the time, Pallas kernels for 8%

profile of v3, /device:TPU:0, one launch (start us, length us, event | category | flops | bytes accessed | tf_op | source)
XLA Modules:
  0.0 153.8 jit_solution(14107722563532574257)
XLA Ops:
  0.0 2.5 %shard_map.127 = (bf16[128,1024]{1,0:T(8,128)(2,1)}, bf16[128,1024]{1,0:T(8,128)(2,1)}, bf16[128,1024]{1,0:T(8,128)(2,1)}, bf16[128,1024]{1,0:T(8,128)(2,1)}) custom-call(bf16[128,1024]{1,0:T(8,128)(2,1)} %refs_0_.2, bf16[128,1024]{1,0:T(8,128)(2,1)} %refs_1_.2, bf16[128,1024]{1,0:T(8,128)(2,1)} %refs_2_.2, bf16[128,1024]{1,0:T(8,128)(2,1)} %refs_3_.4), custom_call_target="tpu_custom_call" | custom-call | bytes 2097152 | tf_op jit(solution)/shard_map/pallas_call | solution.py:203
  2.5 3.1 %collective-permute-start.3 = (bf16[128,1024]{1,0:T(8,128)(2,1)}, bf16[128,1024]{1,0:T(8,128)(2,1)S(1)}, u32[]{:S(2)}, u32[]{:S(2)}) collective-permute-start(bf16[128,1024]{1,0:T(8,128)(2,1)} %get-tuple-element.28), channel_id=1, source_target_pairs={{0,8},{8,0},{16,24},{24,16},{1,9},{9,1},{17,25},{25,17},{2,10},{10... | collective-permute-start | bytes 786440 | tf_op jit(solution)/shard_map/ppermute | solution.py:357
  5.6 2.6 %collective-permute-start.4 = (bf16[128,1024]{1,0:T(8,128)(2,1)}, bf16[128,1024]{1,0:T(8,128)(2,1)S(1)}, u32[]{:S(2)}, u32[]{:S(2)}) collective-permute-start(bf16[128,1024]{1,0:T(8,128)(2,1)} %get-tuple-element.29), channel_id=1, source_target_pairs={{0,16},{8,24},{16,0},{24,8},{1,17},{9,25},{17,1},{25,9},{2,18},{10... | collective-permute-start | bytes 786440 | tf_op jit(solution)/shard_map/ppermute | solution.py:357
  8.2 1.9 %shard_map.134 = (bf16[512,128]{1,0:T(8,128)(2,1)}, bf16[512,128]{1,0:T(8,128)(2,1)}, bf16[512,128]{1,0:T(8,128)(2,1)}, bf16[512,128]{1,0:T(8,128)(2,1)}) custom-call(bf16[1024,128]{1,0:T(8,128)(2,1)} %refs_0_.3, bf16[1024,128]{1,0:T(8,128)(2,1)} %refs_1_.3), custom_call_target="tpu_custom_call" | custom-call | bytes 1048576 | tf_op jit(solution)/shard_map/pallas_call | solution.py:203
  11.1 3.5 %collective-permute-start.19 = (bf16[512,128]{1,0:T(8,128)(2,1)}, bf16[512,128]{1,0:T(8,128)(2,1)S(1)}, u32[]{:S(2)}, u32[]{:S(2)}) collective-permute-start(bf16[512,128]{1,0:T(8,128)(2,1)} %get-tuple-element.35), channel_id=1, source_target_pairs={{0,16},{8,24},{16,0},{24,8},{1,17},{9,25},{17,1},{25,9},{2,18},{10... | collective-permute-start | bytes 393224 | tf_op jit(solution)/shard_map/ppermute | solution.py:357
  14.9 11.9 %collective-permute-done.18.refs_1_ = bf16[512,128]{1,0:T(8,128)(2,1)S(1)} collective-permute-done((bf16[512,128]{1,0:T(8,128)(2,1)}, bf16[512,128]{1,0:T(8,128)(2,1)S(1)}, u32[]{:S(2)}, u32[]{:S(2)}) %collective-permute-start.18) | collective-permute-done | bytes 131104 | tf_op jit(solution)/shard_map/ppermute | solution.py:357
  28.2 8.8 %collective-permute-done.19.refs_2_ = bf16[512,128]{1,0:T(8,128)(2,1)S(1)} collective-permute-done((bf16[512,128]{1,0:T(8,128)(2,1)}, bf16[512,128]{1,0:T(8,128)(2,1)S(1)}, u32[]{:S(2)}, u32[]{:S(2)}) %collective-permute-start.19) | collective-permute-done | bytes 131104 | tf_op jit(solution)/shard_map/ppermute | solution.py:357
  37.0 2.9 %collective-permute-start.20 = (bf16[512,128]{1,0:T(8,128)(2,1)}, bf16[512,128]{1,0:T(8,128)(2,1)S(1)}, u32[]{:S(2)}, u32[]{:S(2)}) collective-permute-start(bf16[512,128]{1,0:T(8,128)(2,1)} %get-tuple-element.36), channel_id=1, source_target_pairs={{0,24},{8,16},{16,8},{24,0},{1,25},{9,17},{17,9},{25,1},{2,26},{10... | collective-permute-start | bytes 393224 | tf_op jit(solution)/shard_map/ppermute | solution.py:357
  41.5 2.6 %collective-permute-done.20.refs_3_ = bf16[512,128]{1,0:T(8,128)(2,1)S(1)} collective-permute-done((bf16[512,128]{1,0:T(8,128)(2,1)}, bf16[512,128]{1,0:T(8,128)(2,1)S(1)}, u32[]{:S(2)}, u32[]{:S(2)}) %collective-permute-start.20) | collective-permute-done | bytes 131104 | tf_op jit(solution)/shard_map/ppermute | solution.py:357
  49.5 8.4 %collective-permute-done.1.refs_2_ = bf16[128,1024]{1,0:T(8,128)(2,1)S(1)} collective-permute-done((bf16[128,1024]{1,0:T(8,128)(2,1)S(1)}, bf16[128,1024]{1,0:T(8,128)(2,1)S(1)}, u32[]{:S(2)}, u32[]{:S(2)}) %collective-permute-start.1) | collective-permute-done | bytes 262176 | tf_op jit(solution)/shard_map/ppermute | solution.py:357
  66.0 4.3 %collective-permute-done.24.refs_5_ = bf16[1024,128]{1,0:T(8,128)(2,1)S(1)} collective-permute-done((bf16[1024,128]{1,0:T(8,128)(2,1)S(1)}, bf16[1024,128]{1,0:T(8,128)(2,1)S(1)}, u32[]{:S(2)}, u32[]{:S(2)}) %collective-permute-start.24) | collective-permute-done | bytes 262176 | tf_op jit(solution)/shard_map/ppermute | solution.py:357
  73.3 4.7 %collective-permute-done.12.refs_0_ = bf16[128,2048]{1,0:T(8,128)(2,1)S(1)} collective-permute-done((bf16[128,2048]{1,0:T(8,128)(2,1)S(1)}, bf16[128,2048]{1,0:T(8,128)(2,1)S(1)}, u32[]{:S(2)}, u32[]{:S(2)}) %collective-permute-start.12) | collective-permute-done | bytes 524320 | tf_op jit(solution)/shard_map/ppermute | solution.py:357
  79.9 2.4 %collective-permute-start.26 = (bf16[1024,128]{1,0:T(8,128)(2,1)S(1)}, bf16[1024,128]{1,0:T(8,128)(2,1)S(1)}, u32[]{:S(2)}, u32[]{:S(2)}) collective-permute-start(bf16[1024,128]{1,0:T(8,128)(2,1)S(1)} %collective-permute-done.22.refs_3_), channel_id=1, source_target_pairs={{0,4},{2,6},{4,0},{6,2},{1,5},{3,7},{5,1},{7,3},{8,12},{10,14},{12... | collective-permute-start | bytes 786440 | tf_op jit(solution)/shard_map/ppermute | solution.py:357
  83.9 2.9 %collective-permute-done.9.refs_9_ = bf16[192,1024]{1,0:T(8,128)(2,1)S(1)} collective-permute-done((bf16[192,1024]{1,0:T(8,128)(2,1)S(1)}, bf16[192,1024]{1,0:T(8,128)(2,1)S(1)}, u32[]{:S(2)}, u32[]{:S(2)}) %collective-permute-start.9) | collective-permute-done | bytes 393248 | tf_op jit(solution)/shard_map/ppermute | solution.py:357
  90.2 2.3 %collective-permute-done.26.refs_7_ = bf16[1024,128]{1,0:T(8,128)(2,1)S(1)} collective-permute-done((bf16[1024,128]{1,0:T(8,128)(2,1)S(1)}, bf16[1024,128]{1,0:T(8,128)(2,1)S(1)}, u32[]{:S(2)}, u32[]{:S(2)}) %collective-permute-start.26) | collective-permute-done | bytes 262176 | tf_op jit(solution)/shard_map/ppermute | solution.py:357
  95.4 3.3 %collective-permute-done.11.refs_11_ = bf16[192,1024]{1,0:T(8,128)(2,1)S(1)} collective-permute-done((bf16[192,1024]{1,0:T(8,128)(2,1)S(1)}, bf16[192,1024]{1,0:T(8,128)(2,1)S(1)}, u32[]{:S(2)}, u32[]{:S(2)}) %collective-permute-start.11) | collective-permute-done | bytes 393248 | tf_op jit(solution)/shard_map/ppermute | solution.py:357
  104.6 2.6 %shard_map.137 = (bf16[256,1024]{1,0:T(8,128)(2,1)S(1)}, f32[256,1024]{1,0:T(8,128)S(1)}) custom-call(bf16[256,1024]{1,0:T(8,128)(2,1)S(1)} %shard_map.130.refs_0_, bf16[256,1024]{1,0:T(8,128)(2,1)S(1)} %shard_map.131.refs_1_, bf16[256,1024]{1,0:T(8,128)(2,1)S(1)} %shard_map.132.refs_2_, bf16[256,1024]{1,0:T(8,128)(2,1)S(1)} %shard_map.133.refs_3_, ...), custom_call_target="tpu_custom_call" | custom-call | flops 805306368 | bytes 4194304 | tf_op jit(solution)/shard_map/pallas_call | solution.py:203
  109.4 2.6 %shard_map.139 = (bf16[256,1024]{1,0:T(8,128)(2,1)S(1)}, f32[256,1024]{1,0:T(8,128)S(1)}) custom-call(bf16[256,1024]{1,0:T(8,128)(2,1)S(1)} %shard_map.130.refs_0_, bf16[256,1024]{1,0:T(8,128)(2,1)S(1)} %shard_map.131.refs_1_, bf16[256,1024]{1,0:T(8,128)(2,1)S(1)} %shard_map.132.refs_2_, bf16[256,1024]{1,0:T(8,128)(2,1)S(1)} %shard_map.133.refs_3_, ...), custom_call_target="tpu_custom_call" | custom-call | flops 805306368 | bytes 4194304 | tf_op jit(solution)/shard_map/pallas_call | solution.py:203
  112.3 2.6 %shard_map.140 = (bf16[256,1024]{1,0:T(8,128)(2,1)S(1)}, f32[256,1024]{1,0:T(8,128)S(1)}) custom-call(bf16[256,1024]{1,0:T(8,128)(2,1)S(1)} %shard_map.130.refs_0_, bf16[256,1024]{1,0:T(8,128)(2,1)S(1)} %shard_map.131.refs_1_, bf16[256,1024]{1,0:T(8,128)(2,1)S(1)} %shard_map.132.refs_2_, bf16[256,1024]{1,0:T(8,128)(2,1)S(1)} %shard_map.133.refs_3_, ...), custom_call_target="tpu_custom_call" | custom-call | flops 805306368 | bytes 4194304 | tf_op jit(solution)/shard_map/pallas_call | solution.py:203
  115.3 2.5 %shard_map.138 = (bf16[256,1024]{1,0:T(8,128)(2,1)S(1)}, f32[256,1024]{1,0:T(8,128)S(1)}) custom-call(bf16[256,1024]{1,0:T(8,128)(2,1)S(1)} %shard_map.130.refs_0_, bf16[256,1024]{1,0:T(8,128)(2,1)S(1)} %shard_map.131.refs_1_, bf16[256,1024]{1,0:T(8,128)(2,1)S(1)} %shard_map.132.refs_2_, bf16[256,1024]{1,0:T(8,128)(2,1)S(1)} %shard_map.133.refs_3_, ...), custom_call_target="tpu_custom_call" | custom-call | flops 805306368 | bytes 4194304 | tf_op jit(solution)/shard_map/pallas_call | solution.py:203
  118.2 8.3 %collective-permute-done.30 = bf16[256,1024]{1,0:T(8,128)(2,1)S(1)} collective-permute-done((bf16[256,1024]{1,0:T(8,128)(2,1)S(1)}, bf16[256,1024]{1,0:T(8,128)(2,1)S(1)}, u32[]{:S(2)}, u32[]{:S(2)}) %collective-permute-start.30) | collective-permute-done | bytes 524320 | tf_op jit(solution)/shard_map/ppermute | solution.py:357
  127.0 2.8 %collective-permute-start.33 = (bf16[256,1024]{1,0:T(8,128)(2,1)S(1)}, bf16[256,1024]{1,0:T(8,128)(2,1)S(1)}, u32[]{:S(2)}, u32[]{:S(2)}) collective-permute-start(bf16[256,1024]{1,0:T(8,128)(2,1)S(1)} %add_convert_fusion.1), channel_id=1, source_target_pairs={{0,16},{8,24},{16,0},{24,8},{1,17},{9,25},{17,1},{25,9},{2,18},{10... | collective-permute-start | bytes 1572872 | tf_op jit(solution)/shard_map/ppermute | solution.py:357
  129.8 20.8 %collective-permute-done.31 = bf16[256,1024]{1,0:T(8,128)(2,1)S(1)} collective-permute-done((bf16[256,1024]{1,0:T(8,128)(2,1)S(1)}, bf16[256,1024]{1,0:T(8,128)(2,1)S(1)}, u32[]{:S(2)}, u32[]{:S(2)}) %collective-permute-start.31) | collective-permute-done | bytes 524320 | tf_op jit(solution)/shard_map/ppermute | solution.py:357
  150.6 2.0 %collective-permute-done.33 = bf16[256,1024]{1,0:T(8,128)(2,1)S(1)} collective-permute-done((bf16[256,1024]{1,0:T(8,128)(2,1)S(1)}, bf16[256,1024]{1,0:T(8,128)(2,1)S(1)}, u32[]{:S(2)}, u32[]{:S(2)}) %collective-permute-start.33) | collective-permute-done | bytes 524320 | tf_op jit(solution)/shard_map/ppermute | solution.py:357
  (84 shorter events, 41.3 us)
Async XLA Ops:
  2.5 43.2 %collective-permute-start.3 = (bf16[128,1024]{1,0:T(8,128)(2,1)}, bf16[128,1024]{1,0:T(8,128)(2,1)S(1)}, u32[]{:S(2)}, u32[]{:S(2)}) collective-permute-start(bf16[128,1024]{1,0:T(8,128)(2,1)} %get-tuple-element.28), channel_id=1, source_target_pairs={{0,8},{8,0},{16,24},{24,16},{1,9},{9,1},{17,25},{25,17},{2,10},{10... | collective-permute-start | bytes 786440 | tf_op jit(solution)/shard_map/ppermute | solution.py:357
  5.6 41.5 %collective-permute-start.4 = (bf16[128,1024]{1,0:T(8,128)(2,1)}, bf16[128,1024]{1,0:T(8,128)(2,1)S(1)}, u32[]{:S(2)}, u32[]{:S(2)}) collective-permute-start(bf16[128,1024]{1,0:T(8,128)(2,1)} %get-tuple-element.29), channel_id=1, source_target_pairs={{0,16},{8,24},{16,0},{24,8},{1,17},{9,25},{17,1},{25,9},{2,18},{10... | collective-permute-start | bytes 786440 | tf_op jit(solution)/shard_map/ppermute | solution.py:357
  8.2 40.5 %collective-permute-start.5 = (bf16[128,1024]{1,0:T(8,128)(2,1)}, bf16[128,1024]{1,0:T(8,128)(2,1)S(1)}, u32[]{:S(2)}, u32[]{:S(2)}) collective-permute-start(bf16[128,1024]{1,0:T(8,128)(2,1)} %get-tuple-element.30), channel_id=1, source_target_pairs={{0,24},{8,16},{16,8},{24,0},{1,25},{9,17},{17,9},{25,1},{2,26},{10... | collective-permute-start | bytes 786440 | tf_op jit(solution)/shard_map/ppermute | solution.py:357
  10.1 16.6 %collective-permute-start.18 = (bf16[512,128]{1,0:T(8,128)(2,1)}, bf16[512,128]{1,0:T(8,128)(2,1)S(1)}, u32[]{:S(2)}, u32[]{:S(2)}) collective-permute-start(bf16[512,128]{1,0:T(8,128)(2,1)} %get-tuple-element.34), channel_id=1, source_target_pairs={{0,8},{8,0},{16,24},{24,16},{1,9},{9,1},{17,25},{25,17},{2,10},{10... | collective-permute-start | bytes 393224 | tf_op jit(solution)/shard_map/ppermute | solution.py:357
  11.1 25.9 %collective-permute-start.19 = (bf16[512,128]{1,0:T(8,128)(2,1)}, bf16[512,128]{1,0:T(8,128)(2,1)S(1)}, u32[]{:S(2)}, u32[]{:S(2)}) collective-permute-start(bf16[512,128]{1,0:T(8,128)(2,1)} %get-tuple-element.35), channel_id=1, source_target_pairs={{0,16},{8,24},{16,0},{24,8},{1,17},{9,25},{17,1},{25,9},{2,18},{10... | collective-permute-start | bytes 393224 | tf_op jit(solution)/shard_map/ppermute | solution.py:357
  26.7 22.6 %collective-permute-start = (bf16[128,1024]{1,0:T(8,128)(2,1)}, bf16[128,1024]{1,0:T(8,128)(2,1)S(1)}, u32[]{:S(2)}, u32[]{:S(2)}) collective-permute-start(bf16[128,1024]{1,0:T(8,128)(2,1)} %get-tuple-element.27.refs_0_), channel_id=1, source_target_pairs={{0,2},{2,0},{4,6},{6,4},{1,3},{3,1},{5,7},{7,5},{8,10},{10,8},{12,... | collective-permute-start | bytes 786440 | tf_op jit(solution)/shard_map/ppermute | solution.py:357
  44.1 13.8 %collective-permute-start.1 = (bf16[128,1024]{1,0:T(8,128)(2,1)S(1)}, bf16[128,1024]{1,0:T(8,128)(2,1)S(1)}, u32[]{:S(2)}, u32[]{:S(2)}) collective-permute-start(bf16[128,1024]{1,0:T(8,128)(2,1)S(1)} %copy-done.2), channel_id=1, source_target_pairs={{0,4},{2,6},{4,0},{6,2},{1,5},{3,7},{5,1},{7,3},{8,12},{10,14},{12... | collective-permute-start | bytes 786440 | tf_op jit(solution)/shard_map/ppermute | solution.py:357
  45.6 12.2 %collective-permute-start.2 = (bf16[128,1024]{1,0:T(8,128)(2,1)S(1)}, bf16[128,1024]{1,0:T(8,128)(2,1)S(1)}, u32[]{:S(2)}, u32[]{:S(2)}) collective-permute-start(bf16[128,1024]{1,0:T(8,128)(2,1)S(1)} %copy-done.2), channel_id=1, source_target_pairs={{0,6},{2,4},{4,2},{6,0},{1,7},{3,5},{5,3},{7,1},{8,14},{10,12},{12... | collective-permute-start | bytes 786440 | tf_op jit(solution)/shard_map/ppermute | solution.py:357
  47.1 14.0 %collective-permute-start.23 = (bf16[1024,128]{1,0:T(8,128)(2,1)S(1)}, bf16[1024,128]{1,0:T(8,128)(2,1)S(1)}, u32[]{:S(2)}, u32[]{:S(2)}) collective-permute-start(bf16[1024,128]{1,0:T(8,128)(2,1)S(1)} %get-tuple-element.37.refs_0_), channel_id=1, source_target_pairs={{0,4},{2,6},{4,0},{6,2},{1,5},{3,7},{5,1},{7,3},{8,12},{10,14},{12... | collective-permute-start | bytes 786440 | tf_op jit(solution)/shard_map/ppermute | solution.py:357
  48.7 14.0 %collective-permute-start.22 = (bf16[1024,128]{1,0:T(8,128)(2,1)S(1)}, bf16[1024,128]{1,0:T(8,128)(2,1)S(1)}, u32[]{:S(2)}, u32[]{:S(2)}) collective-permute-start(bf16[1024,128]{1,0:T(8,128)(2,1)S(1)} %get-tuple-element.38.refs_1_), channel_id=1, source_target_pairs={{0,2},{2,0},{4,6},{6,4},{1,3},{3,1},{5,7},{7,5},{8,10},{10,8},{12,... | collective-permute-start | bytes 786440 | tf_op jit(solution)/shard_map/ppermute | solution.py:357
  49.3 22.5 %collective-permute-start.14 = (bf16[128,2048]{1,0:T(8,128)(2,1)S(1)}, bf16[128,2048]{1,0:T(8,128)(2,1)S(1)}, u32[]{:S(2)}, u32[]{:S(2)}) collective-permute-start(bf16[128,2048]{1,0:T(8,128)(2,1)S(1)} %constant_dynamic-slice_fusion), channel_id=1, source_target_pairs={{0,16},{8,24},{16,0},{24,8},{1,17},{9,25},{17,1},{25,9},{2,18},{10... | collective-permute-start | bytes 1572872 | tf_op jit(solution)/shard_map/ppermute | solution.py:357
  57.9 20.2 %collective-permute-start.12 = (bf16[128,2048]{1,0:T(8,128)(2,1)S(1)}, bf16[128,2048]{1,0:T(8,128)(2,1)S(1)}, u32[]{:S(2)}, u32[]{:S(2)}) collective-permute-start(bf16[128,2048]{1,0:T(8,128)(2,1)S(1)} %constant_dynamic-slice_fusion), channel_id=1, source_target_pairs={{0,8},{8,0},{16,24},{24,16},{1,9},{9,1},{17,25},{25,17},{2,10},{10... | collective-permute-start | bytes 1572872 | tf_op jit(solution)/shard_map/ppermute | solution.py:357
  62.7 15.7 %collective-permute-start.8 = (bf16[192,1024]{1,0:T(8,128)(2,1)S(1)}, bf16[192,1024]{1,0:T(8,128)(2,1)S(1)}, u32[]{:S(2)}, u32[]{:S(2)}) collective-permute-start(bf16[192,1024]{1,0:T(8,128)(2,1)S(1)} %get-tuple-element.31.refs_4_), channel_id=1, source_target_pairs={{0,4},{2,6},{4,0},{6,2},{1,5},{3,7},{5,1},{7,3},{8,12},{10,14},{12... | collective-permute-start | bytes 1179656 | tf_op jit(solution)/shard_map/ppermute | solution.py:357
  64.5 15.4 %collective-permute-start.7 = (bf16[192,1024]{1,0:T(8,128)(2,1)S(1)}, bf16[192,1024]{1,0:T(8,128)(2,1)S(1)}, u32[]{:S(2)}, u32[]{:S(2)}) collective-permute-start(bf16[192,1024]{1,0:T(8,128)(2,1)S(1)} %get-tuple-element.32.refs_5_), channel_id=1, source_target_pairs={{0,2},{2,0},{4,6},{6,4},{1,3},{3,1},{5,7},{7,5},{8,10},{10,8},{12,... | collective-permute-start | bytes 1179656 | tf_op jit(solution)/shard_map/ppermute | solution.py:357
  70.3 13.6 %collective-permute-start.6 = (bf16[192,1024]{1,0:T(8,128)(2,1)S(1)}, bf16[192,1024]{1,0:T(8,128)(2,1)S(1)}, u32[]{:S(2)}, u32[]{:S(2)}) collective-permute-start(bf16[192,1024]{1,0:T(8,128)(2,1)S(1)} %get-tuple-element.31.refs_4_), channel_id=1, source_target_pairs={{0,2},{2,0},{4,6},{6,4},{1,3},{3,1},{5,7},{7,5},{8,10},{10,8},{12,... | collective-permute-start | bytes 1179656 | tf_op jit(solution)/shard_map/ppermute | solution.py:357
  71.8 15.0 %collective-permute-start.9 = (bf16[192,1024]{1,0:T(8,128)(2,1)S(1)}, bf16[192,1024]{1,0:T(8,128)(2,1)S(1)}, u32[]{:S(2)}, u32[]{:S(2)}) collective-permute-start(bf16[192,1024]{1,0:T(8,128)(2,1)S(1)} %get-tuple-element.32.refs_5_), channel_id=1, source_target_pairs={{0,4},{2,6},{4,0},{6,2},{1,5},{3,7},{5,1},{7,3},{8,12},{10,14},{12... | collective-permute-start | bytes 1179656 | tf_op jit(solution)/shard_map/ppermute | solution.py:357
  78.0 14.4 %collective-permute-start.16 = (bf16[128,2048]{1,0:T(8,128)(2,1)S(1)}, bf16[128,2048]{1,0:T(8,128)(2,1)S(1)}, u32[]{:S(2)}, u32[]{:S(2)}) collective-permute-start(bf16[128,2048]{1,0:T(8,128)(2,1)S(1)} %collective-permute-done.14.refs_0_), channel_id=1, source_target_pairs={{0,8},{8,0},{16,24},{24,16},{1,9},{9,1},{17,25},{25,17},{2,10},{10... | collective-permute-start | bytes 1572872 | tf_op jit(solution)/shard_map/ppermute | solution.py:357
  79.9 12.5 %collective-permute-start.26 = (bf16[1024,128]{1,0:T(8,128)(2,1)S(1)}, bf16[1024,128]{1,0:T(8,128)(2,1)S(1)}, u32[]{:S(2)}, u32[]{:S(2)}) collective-permute-start(bf16[1024,128]{1,0:T(8,128)(2,1)S(1)} %collective-permute-done.22.refs_3_), channel_id=1, source_target_pairs={{0,4},{2,6},{4,0},{6,2},{1,5},{3,7},{5,1},{7,3},{8,12},{10,14},{12... | collective-permute-start | bytes 786440 | tf_op jit(solution)/shard_map/ppermute | solution.py:357
  83.9 16.5 %collective-permute-start.15 = (bf16[128,2048]{1,0:T(8,128)(2,1)S(1)}, bf16[128,2048]{1,0:T(8,128)(2,1)S(1)}, u32[]{:S(2)}, u32[]{:S(2)}) collective-permute-start(bf16[128,2048]{1,0:T(8,128)(2,1)S(1)} %collective-permute-done.14.refs_0_), channel_id=1, source_target_pairs={{0,1},{1,0},{2,3},{3,2},{4,5},{5,4},{6,7},{7,6},{8,9},{9,8},{10,11... | collective-permute-start | bytes 1572872 | tf_op jit(solution)/shard_map/ppermute | solution.py:357
  112.3 14.2 %collective-permute-start.30 = (bf16[256,1024]{1,0:T(8,128)(2,1)S(1)}, bf16[256,1024]{1,0:T(8,128)(2,1)S(1)}, u32[]{:S(2)}, u32[]{:S(2)}) collective-permute-start(bf16[256,1024]{1,0:T(8,128)(2,1)S(1)} %add_convert_fusion.3), channel_id=1, source_target_pairs={{0,8},{8,0},{16,24},{24,16},{1,9},{9,1},{17,25},{25,17},{2,10},{10... | collective-permute-start | bytes 1572872 | tf_op jit(solution)/shard_map/ppermute | solution.py:357
  114.9 11.9 %collective-permute-start.32 = (bf16[256,1024]{1,0:T(8,128)(2,1)S(1)}, bf16[256,1024]{1,0:T(8,128)(2,1)S(1)}, u32[]{:S(2)}, u32[]{:S(2)}) collective-permute-start(bf16[256,1024]{1,0:T(8,128)(2,1)S(1)} %get-tuple-element.48), channel_id=1, source_target_pairs={{0,1},{1,0},{2,3},{3,2},{4,5},{5,4},{6,7},{7,6},{8,9},{9,8},{10,11... | collective-permute-start | bytes 1572872 | tf_op jit(solution)/shard_map/ppermute | solution.py:357
  117.8 12.0 %collective-permute-start.28 = (bf16[256,1024]{1,0:T(8,128)(2,1)S(1)}, bf16[256,1024]{1,0:T(8,128)(2,1)S(1)}, u32[]{:S(2)}, u32[]{:S(2)}) collective-permute-start(bf16[256,1024]{1,0:T(8,128)(2,1)S(1)} %get-tuple-element.43), channel_id=1, source_target_pairs={{0,1},{1,0},{2,3},{3,2},{4,5},{5,4},{6,7},{7,6},{8,9},{9,8},{10,11... | collective-permute-start | bytes 1572872 | tf_op jit(solution)/shard_map/ppermute | solution.py:357
  126.5 24.1 %collective-permute-start.31 = (bf16[256,1024]{1,0:T(8,128)(2,1)S(1)}, bf16[256,1024]{1,0:T(8,128)(2,1)S(1)}, u32[]{:S(2)}, u32[]{:S(2)}) collective-permute-start(bf16[256,1024]{1,0:T(8,128)(2,1)S(1)} %add_convert_fusion.2), channel_id=1, source_target_pairs={{0,8},{8,0},{16,24},{24,16},{1,9},{9,1},{17,25},{25,17},{2,10},{10... | collective-permute-start | bytes 1572872 | tf_op jit(solution)/shard_map/ppermute | solution.py:357
  127.0 25.6 %collective-permute-start.33 = (bf16[256,1024]{1,0:T(8,128)(2,1)S(1)}, bf16[256,1024]{1,0:T(8,128)(2,1)S(1)}, u32[]{:S(2)}, u32[]{:S(2)}) collective-permute-start(bf16[256,1024]{1,0:T(8,128)(2,1)S(1)} %add_convert_fusion.1), channel_id=1, source_target_pairs={{0,16},{8,24},{16,0},{24,8},{1,17},{9,25},{17,1},{25,9},{2,18},{10... | collective-permute-start | bytes 1572872 | tf_op jit(solution)/shard_map/ppermute | solution.py:357
  (19 other events, 222.8 us)

commit v4 on v3

--- a/solution.py
+++ b/solution.py
@@ -194,6 +194,7 @@
 VMEM = pl.BlockSpec(memory_space=pltpu.VMEM)
 SMEM = pl.BlockSpec(memory_space=pltpu.SMEM)
 HBM = pl.BlockSpec(memory_space=pltpu.HBM)
+CHUNKS = 2
 VMEM_LIMIT = 16 * 1024 * 1024
 WHOLE_VMEM = 60 * 1024 * 1024
 
@@ -249,9 +250,11 @@
     if slot:
         x_ref = refs[-1]
         tp = lax.axis_index("tp")
-        half = xs[0].shape[0]
-        x_ref[tiles(tp, half)] = xs[0][...]
-        x_ref[tiles(1 - tp, half)] = xs[1][...]
+        size = xs[0].shape[0]
+        each = len(xs) // 2
+        for c in range(each):
+            x_ref[tiles(tp * each + c, size)] = xs[c][...]
+            x_ref[tiles((1 - tp) * each + c, size)] = xs[each + c][...]
     else:
         x_ref = xs[0]
     width = w_ref.shape[1] // 4
@@ -481,11 +484,14 @@
         floated * lax.rsqrt(jnp.mean(floated * floated, -1, keepdims=True) + NORM_EPS) * norm_gain
     ).astype(low)
     half = rows // n_tp
-    mine = lax.dynamic_slice_in_dim(own, tp * half, half, 0)
-    slots = {0: mine}
-    for bit in (2, 1):
-        for j in sorted(slots, reverse=True):
-            slots[j ^ bit] = swap(slots[j], "sp", bit)
+    size_of = half // CHUNKS
+    mine = [
+        lax.dynamic_slice_in_dim(own, tp * half + c * size_of, size_of, 0) for c in range(CHUNKS)
+    ]
+    whole = lax.dynamic_slice_in_dim(own, tp * half, half, 0)
+    slots = {1: [swap(whole, "sp", 1)]}
+    slots[2] = [swap(piece, "sp", 2) for piece in mine]
+    slots[3] = [swap(piece, "sp", 1) for piece in slots[2]]
 
     half_dim = HEAD_DIM // 2
     freqs = 1.0 / THETA ** (np.arange(half_dim, dtype=np.float32) * 2.0 / HEAD_DIM)
@@ -493,7 +499,9 @@
     table = jnp.asarray(np.concatenate([np.cos(angles), np.sin(angles)], 1).astype(np.float32))
 
     def project(j):
-        xs = [own] if j == 0 else [slots[j], swap(slots[j], "tp", 1)]
+        xs = [own]
+        if j:
+            xs = slots[j] + [swap(piece, "tp", 1) for piece in slots[j]]
         scratch = [pltpu.VMEM((rows, depth), low)] if j else []
         return call(
             functools.partial(project_kernel, j), [((rows, width), low)], scratch,

time: 154 us -> 169 us (1.097)
  waiting for transfers between devices: 89 us -> 103 us
    ppermute x34 -> x38, waiting for transfers between devices: 89 us -> 103 us  [swap(): lax.ppermute(value, axis, [(i, i ^ bits) for i in range(lax.axis_size(axi...]
    ppermute x34 -> x38, starting transfers between devices: 39.8 us -> 40.3 us  [swap(): lax.ppermute(value, axis, [(i, i ^ bits) for i in range(lax.axis_size(axi...]
  transfers between devices with their start and end apart: 34 -> 38, of which waited for: 18 -> 15; matrix products, arithmetic and copies ran while one was open for 1% -> 1% of each run, Pallas kernels for 8% -> 7%
where the time goes in v4:
time: 169 us
  waiting for transfers between devices  103 us (61%)
  starting transfers between devices  40.3 us (24%)
  Pallas kernels  21.2 us (13%)
  other arithmetic  3.46 us (2%)
    ppermute x38, waiting for transfers between devices, swap(): lax.ppermute(value, axis, [(i, i ^ bits) for i in range(lax.axis_size(axi...  103 us
    ppermute x38, starting transfers between devices, swap(): lax.ppermute(value, axis, [(i, i ^ bits) for i in range(lax.axis_size(axi...  40.3 us
    pallas_call x14, Pallas kernels, call(): pl.pallas_call(kernel, out_shape=[jax.ShapeDtypeStruct(shape, dtype) for...  21.2 us
  transfers between devices with their start and end apart: 38, of which 15 were waited for; matrix products, arithmetic and copies ran while one was open for 1% of the time, Pallas kernels for 7%

profile of v4, /device:TPU:0, one launch (start us, length us, event | category | flops | bytes accessed | tf_op | source)
XLA Modules:
  0.0 168.6 jit_solution(2023606310285963570)
XLA Ops:
  0.0 2.4 %shard_map.127 = (bf16[128,1024]{1,0:T(8,128)(2,1)}, bf16[128,1024]{1,0:T(8,128)(2,1)}, bf16[128,1024]{1,0:T(8,128)(2,1)}, bf16[128,1024]{1,0:T(8,128)(2,1)}) custom-call(bf16[128,1024]{1,0:T(8,128)(2,1)} %refs_0_.2, bf16[128,1024]{1,0:T(8,128)(2,1)} %refs_1_.2, bf16[128,1024]{1,0:T(8,128)(2,1)} %refs_2_.2, bf16[128,1024]{1,0:T(8,128)(2,1)} %refs_3_.2), custom_call_target="tpu_custom_call" | custom-call | bytes 2097152 | tf_op jit(solution)/shard_map/pallas_call | solution.py:204
  2.5 3.1 %collective-permute-start.3 = (bf16[128,1024]{1,0:T(8,128)(2,1)}, bf16[128,1024]{1,0:T(8,128)(2,1)S(1)}, u32[]{:S(2)}, u32[]{:S(2)}) collective-permute-start(bf16[128,1024]{1,0:T(8,128)(2,1)} %get-tuple-element.28), channel_id=1, source_target_pairs={{0,8},{8,0},{16,24},{24,16},{1,9},{9,1},{17,25},{25,17},{2,10},{10... | collective-permute-start | bytes 786440 | tf_op jit(solution)/shard_map/ppermute | solution.py:360
  5.6 2.6 %collective-permute-start.4 = (bf16[128,1024]{1,0:T(8,128)(2,1)}, bf16[128,1024]{1,0:T(8,128)(2,1)S(1)}, u32[]{:S(2)}, u32[]{:S(2)}) collective-permute-start(bf16[128,1024]{1,0:T(8,128)(2,1)} %get-tuple-element.29), channel_id=1, source_target_pairs={{0,16},{8,24},{16,0},{24,8},{1,17},{9,25},{17,1},{25,9},{2,18},{10... | collective-permute-start | bytes 786440 | tf_op jit(solution)/shard_map/ppermute | solution.py:360
  11.1 3.5 %collective-permute-start.23 = (bf16[512,128]{1,0:T(8,128)(2,1)}, bf16[512,128]{1,0:T(8,128)(2,1)S(1)}, u32[]{:S(2)}, u32[]{:S(2)}) collective-permute-start(bf16[512,128]{1,0:T(8,128)(2,1)} %get-tuple-element.35), channel_id=1, source_target_pairs={{0,16},{8,24},{16,0},{24,8},{1,17},{9,25},{17,1},{25,9},{2,18},{10... | collective-permute-start | bytes 393224 | tf_op jit(solution)/shard_map/ppermute | solution.py:360
  14.9 11.9 %collective-permute-done.22.refs_1_ = bf16[512,128]{1,0:T(8,128)(2,1)S(1)} collective-permute-done((bf16[512,128]{1,0:T(8,128)(2,1)}, bf16[512,128]{1,0:T(8,128)(2,1)S(1)}, u32[]{:S(2)}, u32[]{:S(2)}) %collective-permute-start.22) | collective-permute-done | bytes 131104 | tf_op jit(solution)/shard_map/ppermute | solution.py:360
  28.2 8.8 %collective-permute-done.23.refs_2_ = bf16[512,128]{1,0:T(8,128)(2,1)S(1)} collective-permute-done((bf16[512,128]{1,0:T(8,128)(2,1)}, bf16[512,128]{1,0:T(8,128)(2,1)S(1)}, u32[]{:S(2)}, u32[]{:S(2)}) %collective-permute-start.23) | collective-permute-done | bytes 131104 | tf_op jit(solution)/shard_map/ppermute | solution.py:360
  37.0 2.9 %collective-permute-start.24 = (bf16[512,128]{1,0:T(8,128)(2,1)}, bf16[512,128]{1,0:T(8,128)(2,1)S(1)}, u32[]{:S(2)}, u32[]{:S(2)}) collective-permute-start(bf16[512,128]{1,0:T(8,128)(2,1)} %get-tuple-element.36), channel_id=1, source_target_pairs={{0,24},{8,16},{16,8},{24,0},{1,25},{9,17},{17,9},{25,1},{2,26},{10... | collective-permute-start | bytes 393224 | tf_op jit(solution)/shard_map/ppermute | solution.py:360
  41.4 2.6 %collective-permute-done.24.refs_3_ = bf16[512,128]{1,0:T(8,128)(2,1)S(1)} collective-permute-done((bf16[512,128]{1,0:T(8,128)(2,1)}, bf16[512,128]{1,0:T(8,128)(2,1)S(1)}, u32[]{:S(2)}, u32[]{:S(2)}) %collective-permute-start.24) | collective-permute-done | bytes 131104 | tf_op jit(solution)/shard_map/ppermute | solution.py:360
  47.3 2.8 %collective-permute-start.15 = (bf16[64,2048]{1,0:T(8,128)(2,1)S(1)}, bf16[64,2048]{1,0:T(8,128)(2,1)S(1)}, u32[]{:S(2)}, u32[]{:S(2)}) collective-permute-start(bf16[64,2048]{1,0:T(8,128)(2,1)S(1)} %get-tuple-element.49), channel_id=1, source_target_pairs={{0,16},{8,24},{16,0},{24,8},{1,17},{9,25},{17,1},{25,9},{2,18},{10... | collective-permute-start | bytes 786440 | tf_op jit(solution)/shard_map/ppermute | solution.py:360
  51.6 6.2 %collective-permute-done.1.refs_2_ = bf16[128,1024]{1,0:T(8,128)(2,1)S(1)} collective-permute-done((bf16[128,1024]{1,0:T(8,128)(2,1)S(1)}, bf16[128,1024]{1,0:T(8,128)(2,1)S(1)}, u32[]{:S(2)}, u32[]{:S(2)}) %collective-permute-start.1) | collective-permute-done | bytes 262176 | tf_op jit(solution)/shard_map/ppermute | solution.py:360
  59.9 4.5 %collective-permute-done.14.refs_0_ = bf16[64,2048]{1,0:T(8,128)(2,1)S(1)} collective-permute-done((bf16[64,2048]{1,0:T(8,128)(2,1)S(1)}, bf16[64,2048]{1,0:T(8,128)(2,1)S(1)}, u32[]{:S(2)}, u32[]{:S(2)}) %collective-permute-start.14) | collective-permute-done | bytes 262176 | tf_op jit(solution)/shard_map/ppermute | solution.py:360
  65.9 4.0 %collective-permute-done.15.refs_1_ = bf16[64,2048]{1,0:T(8,128)(2,1)S(1)} collective-permute-done((bf16[64,2048]{1,0:T(8,128)(2,1)S(1)}, bf16[64,2048]{1,0:T(8,128)(2,1)S(1)}, u32[]{:S(2)}, u32[]{:S(2)}) %collective-permute-start.15) | collective-permute-done | bytes 262176 | tf_op jit(solution)/shard_map/ppermute | solution.py:360
  70.0 2.0 %collective-permute-start.19 = (bf16[64,2048]{1,0:T(8,128)(2,1)S(1)}, bf16[64,2048]{1,0:T(8,128)(2,1)S(1)}, u32[]{:S(2)}, u32[]{:S(2)}) collective-permute-start(bf16[64,2048]{1,0:T(8,128)(2,1)S(1)} %collective-permute-done.15.refs_1_), channel_id=1, source_target_pairs={{0,8},{8,0},{16,24},{24,16},{1,9},{9,1},{17,25},{25,17},{2,10},{10... | collective-permute-start | bytes 786440 | tf_op jit(solution)/shard_map/ppermute | solution.py:360
  74.3 4.8 %collective-permute-done.18.refs_0_ = bf16[64,2048]{1,0:T(8,128)(2,1)S(1)} collective-permute-done((bf16[64,2048]{1,0:T(8,128)(2,1)S(1)}, bf16[64,2048]{1,0:T(8,128)(2,1)S(1)}, u32[]{:S(2)}, u32[]{:S(2)}) %collective-permute-start.18) | collective-permute-done | bytes 262176 | tf_op jit(solution)/shard_map/ppermute | solution.py:360
  79.7 5.1 %collective-permute-done.19.refs_1_ = bf16[64,2048]{1,0:T(8,128)(2,1)S(1)} collective-permute-done((bf16[64,2048]{1,0:T(8,128)(2,1)S(1)}, bf16[64,2048]{1,0:T(8,128)(2,1)S(1)}, u32[]{:S(2)}, u32[]{:S(2)}) %collective-permute-start.19) | collective-permute-done | bytes 262176 | tf_op jit(solution)/shard_map/ppermute | solution.py:360
  86.3 8.8 %collective-permute-done.12.refs_0_ = bf16[128,2048]{1,0:T(8,128)(2,1)S(1)} collective-permute-done((bf16[128,2048]{1,0:T(8,128)(2,1)S(1)}, bf16[128,2048]{1,0:T(8,128)(2,1)S(1)}, u32[]{:S(2)}, u32[]{:S(2)}) %collective-permute-start.12) | collective-permute-done | bytes 524320 | tf_op jit(solution)/shard_map/ppermute | solution.py:360
  99.1 13.1 %collective-permute-done.29.refs_6_ = bf16[1024,128]{1,0:T(8,128)(2,1)S(1)} collective-permute-done((bf16[1024,128]{1,0:T(8,128)(2,1)S(1)}, bf16[1024,128]{1,0:T(8,128)(2,1)S(1)}, u32[]{:S(2)}, u32[]{:S(2)}) %collective-permute-start.29) | collective-permute-done | bytes 262176 | tf_op jit(solution)/shard_map/ppermute | solution.py:360
  119.9 2.6 %shard_map.137 = (bf16[256,1024]{1,0:T(8,128)(2,1)S(1)}, f32[256,1024]{1,0:T(8,128)S(1)}) custom-call(bf16[256,1024]{1,0:T(8,128)(2,1)S(1)} %shard_map.130.refs_0_, bf16[256,1024]{1,0:T(8,128)(2,1)S(1)} %shard_map.131.refs_1_, bf16[256,1024]{1,0:T(8,128)(2,1)S(1)} %shard_map.132.refs_2_, bf16[256,1024]{1,0:T(8,128)(2,1)S(1)} %shard_map.133.refs_3_, ...), custom_call_target="tpu_custom_call" | custom-call | flops 805306368 | bytes 4194304 | tf_op jit(solution)/shard_map/pallas_call | solution.py:204
  124.6 2.8 %shard_map.139 = (bf16[256,1024]{1,0:T(8,128)(2,1)S(1)}, f32[256,1024]{1,0:T(8,128)S(1)}) custom-call(bf16[256,1024]{1,0:T(8,128)(2,1)S(1)} %shard_map.130.refs_0_, bf16[256,1024]{1,0:T(8,128)(2,1)S(1)} %shard_map.131.refs_1_, bf16[256,1024]{1,0:T(8,128)(2,1)S(1)} %shard_map.132.refs_2_, bf16[256,1024]{1,0:T(8,128)(2,1)S(1)} %shard_map.133.refs_3_, ...), custom_call_target="tpu_custom_call" | custom-call | flops 805306368 | bytes 4194304 | tf_op jit(solution)/shard_map/pallas_call | solution.py:204
  128.0 2.6 %shard_map.140 = (bf16[256,1024]{1,0:T(8,128)(2,1)S(1)}, f32[256,1024]{1,0:T(8,128)S(1)}) custom-call(bf16[256,1024]{1,0:T(8,128)(2,1)S(1)} %shard_map.130.refs_0_, bf16[256,1024]{1,0:T(8,128)(2,1)S(1)} %shard_map.131.refs_1_, bf16[256,1024]{1,0:T(8,128)(2,1)S(1)} %shard_map.132.refs_2_, bf16[256,1024]{1,0:T(8,128)(2,1)S(1)} %shard_map.133.refs_3_, ...), custom_call_target="tpu_custom_call" | custom-call | flops 805306368 | bytes 4194304 | tf_op jit(solution)/shard_map/pallas_call | solution.py:204
  130.6 2.5 %shard_map.138 = (bf16[256,1024]{1,0:T(8,128)(2,1)S(1)}, f32[256,1024]{1,0:T(8,128)S(1)}) custom-call(bf16[256,1024]{1,0:T(8,128)(2,1)S(1)} %shard_map.130.refs_0_, bf16[256,1024]{1,0:T(8,128)(2,1)S(1)} %shard_map.131.refs_1_, bf16[256,1024]{1,0:T(8,128)(2,1)S(1)} %shard_map.132.refs_2_, bf16[256,1024]{1,0:T(8,128)(2,1)S(1)} %shard_map.133.refs_3_, ...), custom_call_target="tpu_custom_call" | custom-call | flops 805306368 | bytes 4194304 | tf_op jit(solution)/shard_map/pallas_call | solution.py:204
  133.9 7.9 %collective-permute-done.34 = bf16[256,1024]{1,0:T(8,128)(2,1)S(1)} collective-permute-done((bf16[256,1024]{1,0:T(8,128)(2,1)S(1)}, bf16[256,1024]{1,0:T(8,128)(2,1)S(1)}, u32[]{:S(2)}, u32[]{:S(2)}) %collective-permute-start.34) | collective-permute-done | bytes 524320 | tf_op jit(solution)/shard_map/ppermute | solution.py:360
  144.1 20.7 %collective-permute-done.35 = bf16[256,1024]{1,0:T(8,128)(2,1)S(1)} collective-permute-done((bf16[256,1024]{1,0:T(8,128)(2,1)S(1)}, bf16[256,1024]{1,0:T(8,128)(2,1)S(1)}, u32[]{:S(2)}, u32[]{:S(2)}) %collective-permute-start.35) | collective-permute-done | bytes 524320 | tf_op jit(solution)/shard_map/ppermute | solution.py:360
  164.8 2.7 %collective-permute-done.37 = bf16[256,1024]{1,0:T(8,128)(2,1)S(1)} collective-permute-done((bf16[256,1024]{1,0:T(8,128)(2,1)S(1)}, bf16[256,1024]{1,0:T(8,128)(2,1)S(1)}, u32[]{:S(2)}, u32[]{:S(2)}) %collective-permute-start.37) | collective-permute-done | bytes 524320 | tf_op jit(solution)/shard_map/ppermute | solution.py:360
  (93 shorter events, 37.4 us)
Async XLA Ops:
  2.5 43.2 %collective-permute-start.3 = (bf16[128,1024]{1,0:T(8,128)(2,1)}, bf16[128,1024]{1,0:T(8,128)(2,1)S(1)}, u32[]{:S(2)}, u32[]{:S(2)}) collective-permute-start(bf16[128,1024]{1,0:T(8,128)(2,1)} %get-tuple-element.28), channel_id=1, source_target_pairs={{0,8},{8,0},{16,24},{24,16},{1,9},{9,1},{17,25},{25,17},{2,10},{10... | collective-permute-start | bytes 786440 | tf_op jit(solution)/shard_map/ppermute | solution.py:360
  5.6 41.6 %collective-permute-start.4 = (bf16[128,1024]{1,0:T(8,128)(2,1)}, bf16[128,1024]{1,0:T(8,128)(2,1)S(1)}, u32[]{:S(2)}, u32[]{:S(2)}) collective-permute-start(bf16[128,1024]{1,0:T(8,128)(2,1)} %get-tuple-element.29), channel_id=1, source_target_pairs={{0,16},{8,24},{16,0},{24,8},{1,17},{9,25},{17,1},{25,9},{2,18},{10... | collective-permute-start | bytes 786440 | tf_op jit(solution)/shard_map/ppermute | solution.py:360
  8.2 39.2 %collective-permute-start.5 = (bf16[128,1024]{1,0:T(8,128)(2,1)}, bf16[128,1024]{1,0:T(8,128)(2,1)S(1)}, u32[]{:S(2)}, u32[]{:S(2)}) collective-permute-start(bf16[128,1024]{1,0:T(8,128)(2,1)} %get-tuple-element.30), channel_id=1, source_target_pairs={{0,24},{8,16},{16,8},{24,0},{1,25},{9,17},{17,9},{25,1},{2,26},{10... | collective-permute-start | bytes 786440 | tf_op jit(solution)/shard_map/ppermute | solution.py:360
  10.1 16.6 %collective-permute-start.22 = (bf16[512,128]{1,0:T(8,128)(2,1)}, bf16[512,128]{1,0:T(8,128)(2,1)S(1)}, u32[]{:S(2)}, u32[]{:S(2)}) collective-permute-start(bf16[512,128]{1,0:T(8,128)(2,1)} %get-tuple-element.34), channel_id=1, source_target_pairs={{0,8},{8,0},{16,24},{24,16},{1,9},{9,1},{17,25},{25,17},{2,10},{10... | collective-permute-start | bytes 393224 | tf_op jit(solution)/shard_map/ppermute | solution.py:360
  11.1 25.9 %collective-permute-start.23 = (bf16[512,128]{1,0:T(8,128)(2,1)}, bf16[512,128]{1,0:T(8,128)(2,1)S(1)}, u32[]{:S(2)}, u32[]{:S(2)}) collective-permute-start(bf16[512,128]{1,0:T(8,128)(2,1)} %get-tuple-element.35), channel_id=1, source_target_pairs={{0,16},{8,24},{16,0},{24,8},{1,17},{9,25},{17,1},{25,9},{2,18},{10... | collective-permute-start | bytes 393224 | tf_op jit(solution)/shard_map/ppermute | solution.py:360
  26.7 23.4 %collective-permute-start = (bf16[128,1024]{1,0:T(8,128)(2,1)}, bf16[128,1024]{1,0:T(8,128)(2,1)S(1)}, u32[]{:S(2)}, u32[]{:S(2)}) collective-permute-start(bf16[128,1024]{1,0:T(8,128)(2,1)} %get-tuple-element.27.refs_0_), channel_id=1, source_target_pairs={{0,2},{2,0},{4,6},{6,4},{1,3},{3,1},{5,7},{7,5},{8,10},{10,8},{12,... | collective-permute-start | bytes 786440 | tf_op jit(solution)/shard_map/ppermute | solution.py:360
  47.2 17.2 %collective-permute-start.14 = (bf16[64,2048]{1,0:T(8,128)(2,1)S(1)}, bf16[64,2048]{1,0:T(8,128)(2,1)S(1)}, u32[]{:S(2)}, u32[]{:S(2)}) collective-permute-start(bf16[64,2048]{1,0:T(8,128)(2,1)S(1)} %get-tuple-element.50), channel_id=1, source_target_pairs={{0,16},{8,24},{16,0},{24,8},{1,17},{9,25},{17,1},{25,9},{2,18},{10... | collective-permute-start | bytes 786440 | tf_op jit(solution)/shard_map/ppermute | solution.py:360
  47.3 22.6 %collective-permute-start.15 = (bf16[64,2048]{1,0:T(8,128)(2,1)S(1)}, bf16[64,2048]{1,0:T(8,128)(2,1)S(1)}, u32[]{:S(2)}, u32[]{:S(2)}) collective-permute-start(bf16[64,2048]{1,0:T(8,128)(2,1)S(1)} %get-tuple-element.49), channel_id=1, source_target_pairs={{0,16},{8,24},{16,0},{24,8},{1,17},{9,25},{17,1},{25,9},{2,18},{10... | collective-permute-start | bytes 786440 | tf_op jit(solution)/shard_map/ppermute | solution.py:360
  50.1 19.8 %collective-permute-start.27 = (bf16[1024,128]{1,0:T(8,128)(2,1)S(1)}, bf16[1024,128]{1,0:T(8,128)(2,1)S(1)}, u32[]{:S(2)}, u32[]{:S(2)}) collective-permute-start(bf16[1024,128]{1,0:T(8,128)(2,1)S(1)} %get-tuple-element.37.refs_0_), channel_id=1, source_target_pairs={{0,4},{2,6},{4,0},{6,2},{1,5},{3,7},{5,1},{7,3},{8,12},{10,14},{12... | collective-permute-start | bytes 786440 | tf_op jit(solution)/shard_map/ppermute | solution.py:360
  57.9 14.1 %collective-permute-start.26 = (bf16[1024,128]{1,0:T(8,128)(2,1)S(1)}, bf16[1024,128]{1,0:T(8,128)(2,1)S(1)}, u32[]{:S(2)}, u32[]{:S(2)}) collective-permute-start(bf16[1024,128]{1,0:T(8,128)(2,1)S(1)} %get-tuple-element.38.refs_1_), channel_id=1, source_target_pairs={{0,2},{2,0},{4,6},{6,4},{1,3},{3,1},{5,7},{7,5},{8,10},{10,8},{12,... | collective-permute-start | bytes 786440 | tf_op jit(solution)/shard_map/ppermute | solution.py:360
  70.0 14.8 %collective-permute-start.19 = (bf16[64,2048]{1,0:T(8,128)(2,1)S(1)}, bf16[64,2048]{1,0:T(8,128)(2,1)S(1)}, u32[]{:S(2)}, u32[]{:S(2)}) collective-permute-start(bf16[64,2048]{1,0:T(8,128)(2,1)S(1)} %collective-permute-done.15.refs_1_), channel_id=1, source_target_pairs={{0,8},{8,0},{16,24},{24,16},{1,9},{9,1},{17,25},{25,17},{2,10},{10... | collective-permute-start | bytes 786440 | tf_op jit(solution)/shard_map/ppermute | solution.py:360
  72.0 23.0 %collective-permute-start.12 = (bf16[128,2048]{1,0:T(8,128)(2,1)S(1)}, bf16[128,2048]{1,0:T(8,128)(2,1)S(1)}, u32[]{:S(2)}, u32[]{:S(2)}) collective-permute-start(bf16[128,2048]{1,0:T(8,128)(2,1)S(1)} %constant_dynamic-slice_fusion.2), channel_id=1, source_target_pairs={{0,8},{8,0},{16,24},{24,16},{1,9},{9,1},{17,25},{25,17},{2,10},{10... | collective-permute-start | bytes 1572872 | tf_op jit(solution)/shard_map/ppermute | solution.py:360
  72.2 22.9 %collective-permute-start.8 = (bf16[192,1024]{1,0:T(8,128)(2,1)S(1)}, bf16[192,1024]{1,0:T(8,128)(2,1)S(1)}, u32[]{:S(2)}, u32[]{:S(2)}) collective-permute-start(bf16[192,1024]{1,0:T(8,128)(2,1)S(1)} %get-tuple-element.31.refs_4_), channel_id=1, source_target_pairs={{0,4},{2,6},{4,0},{6,2},{1,5},{3,7},{5,1},{7,3},{8,12},{10,14},{12... | collective-permute-start | bytes 1179656 | tf_op jit(solution)/shard_map/ppermute | solution.py:360
  73.8 21.8 %collective-permute-start.7 = (bf16[192,1024]{1,0:T(8,128)(2,1)S(1)}, bf16[192,1024]{1,0:T(8,128)(2,1)S(1)}, u32[]{:S(2)}, u32[]{:S(2)}) collective-permute-start(bf16[192,1024]{1,0:T(8,128)(2,1)S(1)} %get-tuple-element.32.refs_5_), channel_id=1, source_target_pairs={{0,2},{2,0},{4,6},{6,4},{1,3},{3,1},{5,7},{7,5},{8,10},{10,8},{12,... | collective-permute-start | bytes 1179656 | tf_op jit(solution)/shard_map/ppermute | solution.py:360
  79.1 18.0 %collective-permute-start.6 = (bf16[192,1024]{1,0:T(8,128)(2,1)S(1)}, bf16[192,1024]{1,0:T(8,128)(2,1)S(1)}, u32[]{:S(2)}, u32[]{:S(2)}) collective-permute-start(bf16[192,1024]{1,0:T(8,128)(2,1)S(1)} %get-tuple-element.31.refs_4_), channel_id=1, source_target_pairs={{0,2},{2,0},{4,6},{6,4},{1,3},{3,1},{5,7},{7,5},{8,10},{10,8},{12,... | collective-permute-start | bytes 1179656 | tf_op jit(solution)/shard_map/ppermute | solution.py:360
  84.7 13.9 %collective-permute-start.9 = (bf16[192,1024]{1,0:T(8,128)(2,1)S(1)}, bf16[192,1024]{1,0:T(8,128)(2,1)S(1)}, u32[]{:S(2)}, u32[]{:S(2)}) collective-permute-start(bf16[192,1024]{1,0:T(8,128)(2,1)S(1)} %get-tuple-element.32.refs_5_), channel_id=1, source_target_pairs={{0,4},{2,6},{4,0},{6,2},{1,5},{3,7},{5,1},{7,3},{8,12},{10,14},{12... | collective-permute-start | bytes 1179656 | tf_op jit(solution)/shard_map/ppermute | solution.py:360
  95.0 20.7 %collective-permute-start.13 = (bf16[128,2048]{1,0:T(8,128)(2,1)S(1)}, bf16[128,2048]{1,0:T(8,128)(2,1)S(1)}, u32[]{:S(2)}, u32[]{:S(2)}) collective-permute-start(bf16[128,2048]{1,0:T(8,128)(2,1)S(1)} %collective-permute-done.12.refs_0_), channel_id=1, source_target_pairs={{0,1},{1,0},{2,3},{3,2},{4,5},{5,4},{6,7},{7,6},{8,9},{9,8},{10,11... | collective-permute-start | bytes 1572872 | tf_op jit(solution)/shard_map/ppermute | solution.py:360
  95.0 18.3 %collective-permute-start.10 = (bf16[192,1024]{1,0:T(8,128)(2,1)S(1)}, bf16[192,1024]{1,0:T(8,128)(2,1)S(1)}, u32[]{:S(2)}, u32[]{:S(2)}) collective-permute-start(bf16[192,1024]{1,0:T(8,128)(2,1)S(1)} %collective-permute-done.8.refs_8_), channel_id=1, source_target_pairs={{0,2},{2,0},{4,6},{6,4},{1,3},{3,1},{5,7},{7,5},{8,10},{10,8},{12,... | collective-permute-start | bytes 1179656 | tf_op jit(solution)/shard_map/ppermute | solution.py:360
  95.6 18.1 %collective-permute-start.11 = (bf16[192,1024]{1,0:T(8,128)(2,1)S(1)}, bf16[192,1024]{1,0:T(8,128)(2,1)S(1)}, u32[]{:S(2)}, u32[]{:S(2)}) collective-permute-start(bf16[192,1024]{1,0:T(8,128)(2,1)S(1)} %collective-permute-done.7.refs_7_), channel_id=1, source_target_pairs={{0,4},{2,6},{4,0},{6,2},{1,5},{3,7},{5,1},{7,3},{8,12},{10,14},{12... | collective-permute-start | bytes 1179656 | tf_op jit(solution)/shard_map/ppermute | solution.py:360
  97.1 15.1 %collective-permute-start.29 = (bf16[1024,128]{1,0:T(8,128)(2,1)S(1)}, bf16[1024,128]{1,0:T(8,128)(2,1)S(1)}, u32[]{:S(2)}, u32[]{:S(2)}) collective-permute-start(bf16[1024,128]{1,0:T(8,128)(2,1)S(1)} %collective-permute-done.27.refs_4_), channel_id=1, source_target_pairs={{0,2},{2,0},{4,6},{6,4},{1,3},{3,1},{5,7},{7,5},{8,10},{10,8},{12,... | collective-permute-start | bytes 786440 | tf_op jit(solution)/shard_map/ppermute | solution.py:360
  98.6 13.8 %collective-permute-start.30 = (bf16[1024,128]{1,0:T(8,128)(2,1)S(1)}, bf16[1024,128]{1,0:T(8,128)(2,1)S(1)}, u32[]{:S(2)}, u32[]{:S(2)}) collective-permute-start(bf16[1024,128]{1,0:T(8,128)(2,1)S(1)} %collective-permute-done.26.refs_3_), channel_id=1, source_target_pairs={{0,4},{2,6},{4,0},{6,2},{1,5},{3,7},{5,1},{7,3},{8,12},{10,14},{12... | collective-permute-start | bytes 786440 | tf_op jit(solution)/shard_map/ppermute | solution.py:360
  127.7 14.1 %collective-permute-start.34 = (bf16[256,1024]{1,0:T(8,128)(2,1)S(1)}, bf16[256,1024]{1,0:T(8,128)(2,1)S(1)}, u32[]{:S(2)}, u32[]{:S(2)}) collective-permute-start(bf16[256,1024]{1,0:T(8,128)(2,1)S(1)} %add_convert_fusion.3), channel_id=1, source_target_pairs={{0,8},{8,0},{16,24},{24,16},{1,9},{9,1},{17,25},{25,17},{2,10},{10... | collective-permute-start | bytes 1572872 | tf_op jit(solution)/shard_map/ppermute | solution.py:360
  141.8 23.0 %collective-permute-start.35 = (bf16[256,1024]{1,0:T(8,128)(2,1)S(1)}, bf16[256,1024]{1,0:T(8,128)(2,1)S(1)}, u32[]{:S(2)}, u32[]{:S(2)}) collective-permute-start(bf16[256,1024]{1,0:T(8,128)(2,1)S(1)} %add_convert_fusion.2), channel_id=1, source_target_pairs={{0,8},{8,0},{16,24},{24,16},{1,9},{9,1},{17,25},{25,17},{2,10},{10... | collective-permute-start | bytes 1572872 | tf_op jit(solution)/shard_map/ppermute | solution.py:360
  142.3 25.2 %collective-permute-start.37 = (bf16[256,1024]{1,0:T(8,128)(2,1)S(1)}, bf16[256,1024]{1,0:T(8,128)(2,1)S(1)}, u32[]{:S(2)}, u32[]{:S(2)}) collective-permute-start(bf16[256,1024]{1,0:T(8,128)(2,1)S(1)} %add_convert_fusion.1), channel_id=1, source_target_pairs={{0,16},{8,24},{16,0},{24,8},{1,17},{9,25},{17,1},{25,9},{2,18},{10... | collective-permute-start | bytes 1572872 | tf_op jit(solution)/shard_map/ppermute | solution.py:360
  (23 other events, 253.5 us)

commit v5 on v4

--- a/solution.py
+++ b/solution.py
@@ -277,25 +277,28 @@
         out_ref[:, part * width : (part + 1) * width] = product
 
 
-def mix_kernel(slot, total, *refs):
+def mix_kernel(slot, total, part, parts, *refs):
     projs, (map_ref, scale_ref, gain_ref, lam_ref, w_ref, sent_ref, kept_ref, branch_ref) = (
         refs[:total],
         refs[total:],
     )
     rows = projs[0].shape[0]
+    size = rows // parts
+    first = part * size
+    mine = slice(first, first + size)
     width = 2 * HEAD_DIM
     place = lax.axis_index("sp")
     group = lax.axis_index("tp") * total + place
     level = lax.rem(group, 4)
     block = place ^ slot
     scale = HEAD_DIM ** (-0.5)
-    ahead = lax.broadcasted_iota(jnp.int32, (rows, rows), 0) >= lax.broadcasted_iota(
-        jnp.int32, (rows, rows), 1
+    ahead = lax.broadcasted_iota(jnp.int32, (size, rows), 0) + first >= lax.broadcasted_iota(
+        jnp.int32, (size, rows), 1
     )
     halves = []
     for m in range(2):
         begin = GROUP_DIM + m * HEAD_DIM
-        query = projs[slot][:, begin : begin + HEAD_DIM]
+        query = projs[slot][mine, begin : begin + HEAD_DIM]
         scores, tops = [], []
         for j in range(total):
             score = lax.dot_general(
@@ -335,17 +338,20 @@
     branch_ref[:, GROUP_DIM:] = attn
 
     reach = 16
-    rim = jnp.zeros((reach, GROUP_DIM), jnp.bfloat16)
-    for j in range(total):
-        rim = jnp.where((place ^ j) == block - 1, projs[j][rows - reach :, :GROUP_DIM], rim)
-    flat = jnp.concatenate([rim, projs[slot][:, :GROUP_DIM]], 0).astype(jnp.float32)
+    if first:
+        rim = projs[slot][first - reach : first, :GROUP_DIM]
+    else:
+        rim = jnp.zeros((reach, GROUP_DIM), jnp.bfloat16)
+        for j in range(total):
+            rim = jnp.where((place ^ j) == block - 1, projs[j][rows - reach :, :GROUP_DIM], rim)
+    flat = jnp.concatenate([rim, projs[slot][mine, :GROUP_DIM]], 0).astype(jnp.float32)
     sums = flat
-    picked = jnp.zeros((rows, GROUP_DIM), jnp.float32)
+    picked = jnp.zeros((size, GROUP_DIM), jnp.float32)
     for power in range(4):
         sums = sums + pltpu.roll(sums, 2**power, 0)
         picked = jnp.where(level == power, sums[reach:], picked)
     window = lax.shift_left(jnp.int32(2), level)
-    own_pos = block * rows + lax.broadcasted_iota(jnp.int32, (rows, GROUP_DIM), 0)
+    own_pos = block * rows + first + lax.broadcasted_iota(jnp.int32, (size, GROUP_DIM), 0)
     counts = jnp.minimum(own_pos + 1, window).astype(jnp.float32)
     mixed = (picked / counts - flat[reach:]).astype(jnp.bfloat16)
     pooled = jnp.dot(mixed, map_ref[place], preferred_element_type=jnp.float32) * scale_ref[:, tiles(place, GROUP_DIM)]
@@ -512,27 +518,39 @@
     projs = [project(j) for j in range(n_sp)]
     gain = head_gain[None]
 
-    def block_sum(slot, gain):
+    def mixed(slot, gain, part=0, parts=1):
+        size = rows // parts
         sent, kept = call(
-            functools.partial(mix_kernel, slot, n_sp),
-            [((rows, depth // n_tp), low), ((rows, depth // n_tp), wide)],
-            [pltpu.VMEM((rows, channels), low)],
-            (8 * rows * rows * n_sp * HEAD_DIM + 2 * rows * channels * depth, 8 * rows * width + 2 * depth * channels,
-             2 * rows * rows * n_sp),
+            functools.partial(mix_kernel, slot, n_sp, part, parts),
+            [((size, depth // n_tp), low), ((size, depth // n_tp), wide)],
+            [pltpu.VMEM((size, channels), low)],
+            (8 * size * rows * n_sp * HEAD_DIM + 2 * size * channels * depth, 8 * rows * width + 2 * depth * channels,
+             2 * size * rows * n_sp),
             [VMEM] * (n_sp + 3) + [SMEM, VMEM],
             *projs, pool_map, pool_scale[None], gain, diff_lambda, out_weight,
         )
-        return kept + swap(sent, "tp", 1).astype(wide)
-
-    sum_three = block_sum(3, gain).astype(low)
-    from_three = swap(sum_three, "sp", 1)
-    gain = after(gain, sum_three)
-    sum_two = (block_sum(2, gain) + from_three.astype(wide)).astype(low)
-    sum_one = after(block_sum(1, gain).astype(low), from_three)
-    from_two = swap(sum_two, "sp", 2)
-    from_one = swap(sum_one, "sp", 1)
-    result = block_sum(0, gain) + from_one.astype(wide) + from_two.astype(wide)
-    return result.astype(low)[None]
+        return kept, swap(sent, "tp", 1)
+
+    def total(parts, c=None, *more):
+        if c is not None:
+            parts = [part[c * half : (c + 1) * half] for part in parts]
+        return sum(part.astype(wide) for part in (*parts, *more))
+
+    early = mixed(3, gain, 0, 2)
+    late = mixed(3, after(gain, early[0]), 1, 2)
+    sum_three = total(early).astype(low)
+    from_three = [swap(sum_three, "sp", 1)]
+    gain = after(gain, late[0], sum_three)
+    two = mixed(2, gain)
+    from_three.append(swap(after(total(late).astype(low), two[0]), "sp", 1))
+    one = mixed(1, gain)
+    sum_two = [total(two, 0, from_three[0]).astype(low)]
+    sum_two.append(total(two, 1, after(from_three[1], sum_two[0])).astype(low))
+    from_two = [swap(sum_two[c], "sp", 2) for c in range(2)]
+    zero = mixed(0, gain)
+    from_one = swap(total(one).astype(low), "sp", 1)
+    result = [total((*zero, from_one), c, from_two[c]).astype(low) for c in range(2)]
+    return jnp.concatenate(result, 0)[None]
 
 
 def solution(mesh):

time: 169 us -> 168 us (level)
  waiting for transfers between devices: 103 us -> 98.4 us
  starting transfers between devices: 40.3 us -> 43.5 us
    ppermute x38 -> x41, waiting for transfers between devices: 103 us -> 98.4 us  [swap(): lax.ppermute(value, axis, [(i, i ^ bits) for i in range(lax.axis_size(axi...]
    ppermute x38 -> x41, starting transfers between devices: 40.3 us -> 43.5 us  [swap(): lax.ppermute(value, axis, [(i, i ^ bits) for i in range(lax.axis_size(axi...]
    pallas_call x14 -> x15, Pallas kernels: 21.2 us -> 22.1 us  [call(): pl.pallas_call(kernel, out_shape=[jax.ShapeDtypeStruct(shape, dtype) for...]
  transfers between devices with their start and end apart: 38 -> 41, of which waited for: 15 -> 15; matrix products, arithmetic and copies ran while one was open for 1% -> 1% of each run, Pallas kernels for 7% -> 10%
where the time goes in v5:
time: 168 us
  waiting for transfers between devices  98.4 us (59%)
  starting transfers between devices  43.5 us (26%)
  Pallas kernels  22.1 us (13%)
  other arithmetic  3.41 us (2%)
    ppermute x41, waiting for transfers between devices, swap(): lax.ppermute(value, axis, [(i, i ^ bits) for i in range(lax.axis_size(axi...  98.4 us
    ppermute x41, starting transfers between devices, swap(): lax.ppermute(value, axis, [(i, i ^ bits) for i in range(lax.axis_size(axi...  43.5 us
    pallas_call x15, Pallas kernels, call(): pl.pallas_call(kernel, out_shape=[jax.ShapeDtypeStruct(shape, dtype) for...  22.1 us
  transfers between devices with their start and end apart: 41, of which 15 were waited for; matrix products, arithmetic and copies ran while one was open for 1% of the time, Pallas kernels for 10%

profile of v5, /device:TPU:0, one launch (start us, length us, event | category | flops | bytes accessed | tf_op | source)
XLA Modules:
  0.0 168.0 jit_solution(708981561851095192)
XLA Ops:
  0.0 2.4 %shard_map.127 = (bf16[128,1024]{1,0:T(8,128)(2,1)}, bf16[128,1024]{1,0:T(8,128)(2,1)}, bf16[128,1024]{1,0:T(8,128)(2,1)}, bf16[128,1024]{1,0:T(8,128)(2,1)}) custom-call(bf16[128,1024]{1,0:T(8,128)(2,1)} %refs_0_.2, bf16[128,1024]{1,0:T(8,128)(2,1)} %refs_1_.2, bf16[128,1024]{1,0:T(8,128)(2,1)} %refs_2_.2, bf16[128,1024]{1,0:T(8,128)(2,1)} %refs_3_.2), custom_call_target="tpu_custom_call" | custom-call | bytes 2097152 | tf_op jit(solution)/shard_map/pallas_call | solution.py:204
  2.5 3.1 %collective-permute-start.3 = (bf16[128,1024]{1,0:T(8,128)(2,1)}, bf16[128,1024]{1,0:T(8,128)(2,1)S(1)}, u32[]{:S(2)}, u32[]{:S(2)}) collective-permute-start(bf16[128,1024]{1,0:T(8,128)(2,1)} %get-tuple-element.32), channel_id=1, source_target_pairs={{0,8},{8,0},{16,24},{24,16},{1,9},{9,1},{17,25},{25,17},{2,10},{10... | collective-permute-start | bytes 786440 | tf_op jit(solution)/shard_map/ppermute | solution.py:366
  5.6 2.6 %collective-permute-start.4 = (bf16[128,1024]{1,0:T(8,128)(2,1)}, bf16[128,1024]{1,0:T(8,128)(2,1)S(1)}, u32[]{:S(2)}, u32[]{:S(2)}) collective-permute-start(bf16[128,1024]{1,0:T(8,128)(2,1)} %get-tuple-element.33), channel_id=1, source_target_pairs={{0,16},{8,24},{16,0},{24,8},{1,17},{9,25},{17,1},{25,9},{2,18},{10... | collective-permute-start | bytes 786440 | tf_op jit(solution)/shard_map/ppermute | solution.py:366
  11.1 3.5 %collective-permute-start.23 = (bf16[512,128]{1,0:T(8,128)(2,1)}, bf16[512,128]{1,0:T(8,128)(2,1)S(1)}, u32[]{:S(2)}, u32[]{:S(2)}) collective-permute-start(bf16[512,128]{1,0:T(8,128)(2,1)} %get-tuple-element.39), channel_id=1, source_target_pairs={{0,16},{8,24},{16,0},{24,8},{1,17},{9,25},{17,1},{25,9},{2,18},{10... | collective-permute-start | bytes 393224 | tf_op jit(solution)/shard_map/ppermute | solution.py:366
  14.9 11.8 %collective-permute-done.22.refs_1_ = bf16[512,128]{1,0:T(8,128)(2,1)S(1)} collective-permute-done((bf16[512,128]{1,0:T(8,128)(2,1)}, bf16[512,128]{1,0:T(8,128)(2,1)S(1)}, u32[]{:S(2)}, u32[]{:S(2)}) %collective-permute-start.22) | collective-permute-done | bytes 131104 | tf_op jit(solution)/shard_map/ppermute | solution.py:366
  28.2 8.8 %collective-permute-done.23.refs_2_ = bf16[512,128]{1,0:T(8,128)(2,1)S(1)} collective-permute-done((bf16[512,128]{1,0:T(8,128)(2,1)}, bf16[512,128]{1,0:T(8,128)(2,1)S(1)}, u32[]{:S(2)}, u32[]{:S(2)}) %collective-permute-start.23) | collective-permute-done | bytes 131104 | tf_op jit(solution)/shard_map/ppermute | solution.py:366
  37.0 2.9 %collective-permute-start.24 = (bf16[512,128]{1,0:T(8,128)(2,1)}, bf16[512,128]{1,0:T(8,128)(2,1)S(1)}, u32[]{:S(2)}, u32[]{:S(2)}) collective-permute-start(bf16[512,128]{1,0:T(8,128)(2,1)} %get-tuple-element.40), channel_id=1, source_target_pairs={{0,24},{8,16},{16,8},{24,0},{1,25},{9,17},{17,9},{25,1},{2,26},{10... | collective-permute-start | bytes 393224 | tf_op jit(solution)/shard_map/ppermute | solution.py:366
  41.4 2.6 %collective-permute-done.24.refs_3_ = bf16[512,128]{1,0:T(8,128)(2,1)S(1)} collective-permute-done((bf16[512,128]{1,0:T(8,128)(2,1)}, bf16[512,128]{1,0:T(8,128)(2,1)S(1)}, u32[]{:S(2)}, u32[]{:S(2)}) %collective-permute-start.24) | collective-permute-done | bytes 131104 | tf_op jit(solution)/shard_map/ppermute | solution.py:366
  47.4 2.8 %collective-permute-start.15 = (bf16[64,2048]{1,0:T(8,128)(2,1)S(1)}, bf16[64,2048]{1,0:T(8,128)(2,1)S(1)}, u32[]{:S(2)}, u32[]{:S(2)}) collective-permute-start(bf16[64,2048]{1,0:T(8,128)(2,1)S(1)} %get-tuple-element.59), channel_id=1, source_target_pairs={{0,16},{8,24},{16,0},{24,8},{1,17},{9,25},{17,1},{25,9},{2,18},{10... | collective-permute-start | bytes 786440 | tf_op jit(solution)/shard_map/ppermute | solution.py:366
  51.6 6.2 %collective-permute-done.1.refs_2_ = bf16[128,1024]{1,0:T(8,128)(2,1)S(1)} collective-permute-done((bf16[128,1024]{1,0:T(8,128)(2,1)S(1)}, bf16[128,1024]{1,0:T(8,128)(2,1)S(1)}, u32[]{:S(2)}, u32[]{:S(2)}) %collective-permute-start.1) | collective-permute-done | bytes 262176 | tf_op jit(solution)/shard_map/ppermute | solution.py:366
  59.9 4.5 %collective-permute-done.14.refs_0_ = bf16[64,2048]{1,0:T(8,128)(2,1)S(1)} collective-permute-done((bf16[64,2048]{1,0:T(8,128)(2,1)S(1)}, bf16[64,2048]{1,0:T(8,128)(2,1)S(1)}, u32[]{:S(2)}, u32[]{:S(2)}) %collective-permute-start.14) | collective-permute-done | bytes 262176 | tf_op jit(solution)/shard_map/ppermute | solution.py:366
  66.0 4.0 %collective-permute-done.15.refs_1_ = bf16[64,2048]{1,0:T(8,128)(2,1)S(1)} collective-permute-done((bf16[64,2048]{1,0:T(8,128)(2,1)S(1)}, bf16[64,2048]{1,0:T(8,128)(2,1)S(1)}, u32[]{:S(2)}, u32[]{:S(2)}) %collective-permute-start.15) | collective-permute-done | bytes 262176 | tf_op jit(solution)/shard_map/ppermute | solution.py:366
  70.0 2.0 %collective-permute-start.19 = (bf16[64,2048]{1,0:T(8,128)(2,1)S(1)}, bf16[64,2048]{1,0:T(8,128)(2,1)S(1)}, u32[]{:S(2)}, u32[]{:S(2)}) collective-permute-start(bf16[64,2048]{1,0:T(8,128)(2,1)S(1)} %collective-permute-done.15.refs_1_), channel_id=1, source_target_pairs={{0,8},{8,0},{16,24},{24,16},{1,9},{9,1},{17,25},{25,17},{2,10},{10... | collective-permute-start | bytes 786440 | tf_op jit(solution)/shard_map/ppermute | solution.py:366
  74.3 4.8 %collective-permute-done.18.refs_0_ = bf16[64,2048]{1,0:T(8,128)(2,1)S(1)} collective-permute-done((bf16[64,2048]{1,0:T(8,128)(2,1)S(1)}, bf16[64,2048]{1,0:T(8,128)(2,1)S(1)}, u32[]{:S(2)}, u32[]{:S(2)}) %collective-permute-start.18) | collective-permute-done | bytes 262176 | tf_op jit(solution)/shard_map/ppermute | solution.py:366
  79.7 5.1 %collective-permute-done.19.refs_1_ = bf16[64,2048]{1,0:T(8,128)(2,1)S(1)} collective-permute-done((bf16[64,2048]{1,0:T(8,128)(2,1)S(1)}, bf16[64,2048]{1,0:T(8,128)(2,1)S(1)}, u32[]{:S(2)}, u32[]{:S(2)}) %collective-permute-start.19) | collective-permute-done | bytes 262176 | tf_op jit(solution)/shard_map/ppermute | solution.py:366
  86.3 8.8 %collective-permute-done.12.refs_0_ = bf16[128,2048]{1,0:T(8,128)(2,1)S(1)} collective-permute-done((bf16[128,2048]{1,0:T(8,128)(2,1)S(1)}, bf16[128,2048]{1,0:T(8,128)(2,1)S(1)}, u32[]{:S(2)}, u32[]{:S(2)}) %collective-permute-start.12) | collective-permute-done | bytes 524320 | tf_op jit(solution)/shard_map/ppermute | solution.py:366
  99.1 13.1 %collective-permute-done.29.refs_6_ = bf16[1024,128]{1,0:T(8,128)(2,1)S(1)} collective-permute-done((bf16[1024,128]{1,0:T(8,128)(2,1)S(1)}, bf16[1024,128]{1,0:T(8,128)(2,1)S(1)}, u32[]{:S(2)}, u32[]{:S(2)}) %collective-permute-start.29) | collective-permute-done | bytes 262176 | tf_op jit(solution)/shard_map/ppermute | solution.py:366
  124.1 2.7 %shard_map.140 = (bf16[256,1024]{1,0:T(8,128)(2,1)S(1)}, f32[256,1024]{1,0:T(8,128)S(1)}) custom-call(bf16[256,1024]{1,0:T(8,128)(2,1)S(1)} %shard_map.130.refs_0_, bf16[256,1024]{1,0:T(8,128)(2,1)S(1)} %shard_map.131.refs_1_, bf16[256,1024]{1,0:T(8,128)(2,1)S(1)} %shard_map.132.refs_2_, bf16[256,1024]{1,0:T(8,128)(2,1)S(1)} %shard_map.133.refs_3_, ...), custom_call_target="tpu_custom_call" | custom-call | flops 805306368 | bytes 4194304 | tf_op jit(solution)/shard_map/pallas_call | solution.py:204
  127.5 2.6 %shard_map.141 = (bf16[256,1024]{1,0:T(8,128)(2,1)S(1)}, f32[256,1024]{1,0:T(8,128)S(1)}) custom-call(bf16[256,1024]{1,0:T(8,128)(2,1)S(1)} %shard_map.130.refs_0_, bf16[256,1024]{1,0:T(8,128)(2,1)S(1)} %shard_map.131.refs_1_, bf16[256,1024]{1,0:T(8,128)(2,1)S(1)} %shard_map.132.refs_2_, bf16[256,1024]{1,0:T(8,128)(2,1)S(1)} %shard_map.133.refs_3_, ...), custom_call_target="tpu_custom_call" | custom-call | flops 805306368 | bytes 4194304 | tf_op jit(solution)/shard_map/pallas_call | solution.py:204
  132.0 2.5 %shard_map.139 = (bf16[256,1024]{1,0:T(8,128)(2,1)S(1)}, f32[256,1024]{1,0:T(8,128)S(1)}) custom-call(bf16[256,1024]{1,0:T(8,128)(2,1)S(1)} %shard_map.130.refs_0_, bf16[256,1024]{1,0:T(8,128)(2,1)S(1)} %shard_map.131.refs_1_, bf16[256,1024]{1,0:T(8,128)(2,1)S(1)} %shard_map.132.refs_2_, bf16[256,1024]{1,0:T(8,128)(2,1)S(1)} %shard_map.133.refs_3_, ...), custom_call_target="tpu_custom_call" | custom-call | flops 805306368 | bytes 4194304 | tf_op jit(solution)/shard_map/pallas_call | solution.py:204
  136.5 5.5 %collective-permute-done.39 = bf16[128,1024]{1,0:T(8,128)(2,1)S(1)} collective-permute-done((bf16[128,1024]{1,0:T(8,128)(2,1)S(1)}, bf16[128,1024]{1,0:T(8,128)(2,1)S(1)}, u32[]{:S(2)}, u32[]{:S(2)}) %collective-permute-start.39) | collective-permute-done | bytes 262176 | tf_op jit(solution)/shard_map/ppermute | solution.py:366
  142.4 2.7 %collective-permute-start.37 = (bf16[128,1024]{1,0:T(8,128)(2,1)S(1)}, bf16[128,1024]{1,0:T(8,128)(2,1)S(1)}, u32[]{:S(2)}, u32[]{:S(2)}) collective-permute-start(bf16[128,1024]{1,0:T(8,128)(2,1)S(1)} %add_convert_fusion.5), channel_id=1, source_target_pairs={{0,16},{8,24},{16,0},{24,8},{1,17},{9,25},{17,1},{25,9},{2,18},{10... | collective-permute-start | bytes 786440 | tf_op jit(solution)/shard_map/ppermute | solution.py:366
  145.1 11.6 %collective-permute-done.40 = bf16[128,1024]{1,0:T(8,128)(2,1)S(1)} collective-permute-done((bf16[128,1024]{1,0:T(8,128)(2,1)S(1)}, bf16[128,1024]{1,0:T(8,128)(2,1)S(1)}, u32[]{:S(2)}, u32[]{:S(2)}) %collective-permute-start.40) | collective-permute-done | bytes 262176 | tf_op jit(solution)/shard_map/ppermute | solution.py:366
  156.7 10.1 %collective-permute-done.37 = bf16[128,1024]{1,0:T(8,128)(2,1)S(1)} collective-permute-done((bf16[128,1024]{1,0:T(8,128)(2,1)S(1)}, bf16[128,1024]{1,0:T(8,128)(2,1)S(1)}, u32[]{:S(2)}, u32[]{:S(2)}) %collective-permute-start.37) | collective-permute-done | bytes 262176 | tf_op jit(solution)/shard_map/ppermute | solution.py:366
  (103 shorter events, 40.8 us)
Async XLA Ops:
  2.5 43.2 %collective-permute-start.3 = (bf16[128,1024]{1,0:T(8,128)(2,1)}, bf16[128,1024]{1,0:T(8,128)(2,1)S(1)}, u32[]{:S(2)}, u32[]{:S(2)}) collective-permute-start(bf16[128,1024]{1,0:T(8,128)(2,1)} %get-tuple-element.32), channel_id=1, source_target_pairs={{0,8},{8,0},{16,24},{24,16},{1,9},{9,1},{17,25},{25,17},{2,10},{10... | collective-permute-start | bytes 786440 | tf_op jit(solution)/shard_map/ppermute | solution.py:366
  5.6 41.6 %collective-permute-start.4 = (bf16[128,1024]{1,0:T(8,128)(2,1)}, bf16[128,1024]{1,0:T(8,128)(2,1)S(1)}, u32[]{:S(2)}, u32[]{:S(2)}) collective-permute-start(bf16[128,1024]{1,0:T(8,128)(2,1)} %get-tuple-element.33), channel_id=1, source_target_pairs={{0,16},{8,24},{16,0},{24,8},{1,17},{9,25},{17,1},{25,9},{2,18},{10... | collective-permute-start | bytes 786440 | tf_op jit(solution)/shard_map/ppermute | solution.py:366
  8.2 39.2 %collective-permute-start.5 = (bf16[128,1024]{1,0:T(8,128)(2,1)}, bf16[128,1024]{1,0:T(8,128)(2,1)S(1)}, u32[]{:S(2)}, u32[]{:S(2)}) collective-permute-start(bf16[128,1024]{1,0:T(8,128)(2,1)} %get-tuple-element.34), channel_id=1, source_target_pairs={{0,24},{8,16},{16,8},{24,0},{1,25},{9,17},{17,9},{25,1},{2,26},{10... | collective-permute-start | bytes 786440 | tf_op jit(solution)/shard_map/ppermute | solution.py:366
  10.1 16.6 %collective-permute-start.22 = (bf16[512,128]{1,0:T(8,128)(2,1)}, bf16[512,128]{1,0:T(8,128)(2,1)S(1)}, u32[]{:S(2)}, u32[]{:S(2)}) collective-permute-start(bf16[512,128]{1,0:T(8,128)(2,1)} %get-tuple-element.38), channel_id=1, source_target_pairs={{0,8},{8,0},{16,24},{24,16},{1,9},{9,1},{17,25},{25,17},{2,10},{10... | collective-permute-start | bytes 393224 | tf_op jit(solution)/shard_map/ppermute | solution.py:366
  11.1 25.9 %collective-permute-start.23 = (bf16[512,128]{1,0:T(8,128)(2,1)}, bf16[512,128]{1,0:T(8,128)(2,1)S(1)}, u32[]{:S(2)}, u32[]{:S(2)}) collective-permute-start(bf16[512,128]{1,0:T(8,128)(2,1)} %get-tuple-element.39), channel_id=1, source_target_pairs={{0,16},{8,24},{16,0},{24,8},{1,17},{9,25},{17,1},{25,9},{2,18},{10... | collective-permute-start | bytes 393224 | tf_op jit(solution)/shard_map/ppermute | solution.py:366
  26.7 23.4 %collective-permute-start = (bf16[128,1024]{1,0:T(8,128)(2,1)}, bf16[128,1024]{1,0:T(8,128)(2,1)S(1)}, u32[]{:S(2)}, u32[]{:S(2)}) collective-permute-start(bf16[128,1024]{1,0:T(8,128)(2,1)} %get-tuple-element.31.refs_0_), channel_id=1, source_target_pairs={{0,2},{2,0},{4,6},{6,4},{1,3},{3,1},{5,7},{7,5},{8,10},{10,8},{12,... | collective-permute-start | bytes 786440 | tf_op jit(solution)/shard_map/ppermute | solution.py:366
  47.2 17.2 %collective-permute-start.14 = (bf16[64,2048]{1,0:T(8,128)(2,1)S(1)}, bf16[64,2048]{1,0:T(8,128)(2,1)S(1)}, u32[]{:S(2)}, u32[]{:S(2)}) collective-permute-start(bf16[64,2048]{1,0:T(8,128)(2,1)S(1)} %get-tuple-element.60), channel_id=1, source_target_pairs={{0,16},{8,24},{16,0},{24,8},{1,17},{9,25},{17,1},{25,9},{2,18},{10... | collective-permute-start | bytes 786440 | tf_op jit(solution)/shard_map/ppermute | solution.py:366
  47.4 22.6 %collective-permute-start.15 = (bf16[64,2048]{1,0:T(8,128)(2,1)S(1)}, bf16[64,2048]{1,0:T(8,128)(2,1)S(1)}, u32[]{:S(2)}, u32[]{:S(2)}) collective-permute-start(bf16[64,2048]{1,0:T(8,128)(2,1)S(1)} %get-tuple-element.59), channel_id=1, source_target_pairs={{0,16},{8,24},{16,0},{24,8},{1,17},{9,25},{17,1},{25,9},{2,18},{10... | collective-permute-start | bytes 786440 | tf_op jit(solution)/shard_map/ppermute | solution.py:366
  50.1 19.8 %collective-permute-start.27 = (bf16[1024,128]{1,0:T(8,128)(2,1)S(1)}, bf16[1024,128]{1,0:T(8,128)(2,1)S(1)}, u32[]{:S(2)}, u32[]{:S(2)}) collective-permute-start(bf16[1024,128]{1,0:T(8,128)(2,1)S(1)} %get-tuple-element.41.refs_0_), channel_id=1, source_target_pairs={{0,4},{2,6},{4,0},{6,2},{1,5},{3,7},{5,1},{7,3},{8,12},{10,14},{12... | collective-permute-start | bytes 786440 | tf_op jit(solution)/shard_map/ppermute | solution.py:366
  57.9 14.1 %collective-permute-start.26 = (bf16[1024,128]{1,0:T(8,128)(2,1)S(1)}, bf16[1024,128]{1,0:T(8,128)(2,1)S(1)}, u32[]{:S(2)}, u32[]{:S(2)}) collective-permute-start(bf16[1024,128]{1,0:T(8,128)(2,1)S(1)} %get-tuple-element.42.refs_1_), channel_id=1, source_target_pairs={{0,2},{2,0},{4,6},{6,4},{1,3},{3,1},{5,7},{7,5},{8,10},{10,8},{12,... | collective-permute-start | bytes 786440 | tf_op jit(solution)/shard_map/ppermute | solution.py:366
  70.0 14.8 %collective-permute-start.19 = (bf16[64,2048]{1,0:T(8,128)(2,1)S(1)}, bf16[64,2048]{1,0:T(8,128)(2,1)S(1)}, u32[]{:S(2)}, u32[]{:S(2)}) collective-permute-start(bf16[64,2048]{1,0:T(8,128)(2,1)S(1)} %collective-permute-done.15.refs_1_), channel_id=1, source_target_pairs={{0,8},{8,0},{16,24},{24,16},{1,9},{9,1},{17,25},{25,17},{2,10},{10... | collective-permute-start | bytes 786440 | tf_op jit(solution)/shard_map/ppermute | solution.py:366
  72.0 23.0 %collective-permute-start.12 = (bf16[128,2048]{1,0:T(8,128)(2,1)S(1)}, bf16[128,2048]{1,0:T(8,128)(2,1)S(1)}, u32[]{:S(2)}, u32[]{:S(2)}) collective-permute-start(bf16[128,2048]{1,0:T(8,128)(2,1)S(1)} %constant_dynamic-slice_fusion.2), channel_id=1, source_target_pairs={{0,8},{8,0},{16,24},{24,16},{1,9},{9,1},{17,25},{25,17},{2,10},{10... | collective-permute-start | bytes 1572872 | tf_op jit(solution)/shard_map/ppermute | solution.py:366
  72.2 22.9 %collective-permute-start.8 = (bf16[192,1024]{1,0:T(8,128)(2,1)S(1)}, bf16[192,1024]{1,0:T(8,128)(2,1)S(1)}, u32[]{:S(2)}, u32[]{:S(2)}) collective-permute-start(bf16[192,1024]{1,0:T(8,128)(2,1)S(1)} %get-tuple-element.35.refs_4_), channel_id=1, source_target_pairs={{0,4},{2,6},{4,0},{6,2},{1,5},{3,7},{5,1},{7,3},{8,12},{10,14},{12... | collective-permute-start | bytes 1179656 | tf_op jit(solution)/shard_map/ppermute | solution.py:366
  73.8 21.8 %collective-permute-start.7 = (bf16[192,1024]{1,0:T(8,128)(2,1)S(1)}, bf16[192,1024]{1,0:T(8,128)(2,1)S(1)}, u32[]{:S(2)}, u32[]{:S(2)}) collective-permute-start(bf16[192,1024]{1,0:T(8,128)(2,1)S(1)} %get-tuple-element.36.refs_5_), channel_id=1, source_target_pairs={{0,2},{2,0},{4,6},{6,4},{1,3},{3,1},{5,7},{7,5},{8,10},{10,8},{12,... | collective-permute-start | bytes 1179656 | tf_op jit(solution)/shard_map/ppermute | solution.py:366
  79.1 18.0 %collective-permute-start.6 = (bf16[192,1024]{1,0:T(8,128)(2,1)S(1)}, bf16[192,1024]{1,0:T(8,128)(2,1)S(1)}, u32[]{:S(2)}, u32[]{:S(2)}) collective-permute-start(bf16[192,1024]{1,0:T(8,128)(2,1)S(1)} %get-tuple-element.35.refs_4_), channel_id=1, source_target_pairs={{0,2},{2,0},{4,6},{6,4},{1,3},{3,1},{5,7},{7,5},{8,10},{10,8},{12,... | collective-permute-start | bytes 1179656 | tf_op jit(solution)/shard_map/ppermute | solution.py:366
  84.8 13.9 %collective-permute-start.9 = (bf16[192,1024]{1,0:T(8,128)(2,1)S(1)}, bf16[192,1024]{1,0:T(8,128)(2,1)S(1)}, u32[]{:S(2)}, u32[]{:S(2)}) collective-permute-start(bf16[192,1024]{1,0:T(8,128)(2,1)S(1)} %get-tuple-element.36.refs_5_), channel_id=1, source_target_pairs={{0,4},{2,6},{4,0},{6,2},{1,5},{3,7},{5,1},{7,3},{8,12},{10,14},{12... | collective-permute-start | bytes 1179656 | tf_op jit(solution)/shard_map/ppermute | solution.py:366
  95.0 20.7 %collective-permute-start.13 = (bf16[128,2048]{1,0:T(8,128)(2,1)S(1)}, bf16[128,2048]{1,0:T(8,128)(2,1)S(1)}, u32[]{:S(2)}, u32[]{:S(2)}) collective-permute-start(bf16[128,2048]{1,0:T(8,128)(2,1)S(1)} %collective-permute-done.12.refs_0_), channel_id=1, source_target_pairs={{0,1},{1,0},{2,3},{3,2},{4,5},{5,4},{6,7},{7,6},{8,9},{9,8},{10,11... | collective-permute-start | bytes 1572872 | tf_op jit(solution)/shard_map/ppermute | solution.py:366
  95.0 18.3 %collective-permute-start.10 = (bf16[192,1024]{1,0:T(8,128)(2,1)S(1)}, bf16[192,1024]{1,0:T(8,128)(2,1)S(1)}, u32[]{:S(2)}, u32[]{:S(2)}) collective-permute-start(bf16[192,1024]{1,0:T(8,128)(2,1)S(1)} %collective-permute-done.8.refs_8_), channel_id=1, source_target_pairs={{0,2},{2,0},{4,6},{6,4},{1,3},{3,1},{5,7},{7,5},{8,10},{10,8},{12,... | collective-permute-start | bytes 1179656 | tf_op jit(solution)/shard_map/ppermute | solution.py:366
  95.6 18.1 %collective-permute-start.11 = (bf16[192,1024]{1,0:T(8,128)(2,1)S(1)}, bf16[192,1024]{1,0:T(8,128)(2,1)S(1)}, u32[]{:S(2)}, u32[]{:S(2)}) collective-permute-start(bf16[192,1024]{1,0:T(8,128)(2,1)S(1)} %collective-permute-done.7.refs_7_), channel_id=1, source_target_pairs={{0,4},{2,6},{4,0},{6,2},{1,5},{3,7},{5,1},{7,3},{8,12},{10,14},{12... | collective-permute-start | bytes 1179656 | tf_op jit(solution)/shard_map/ppermute | solution.py:366
  97.1 15.1 %collective-permute-start.29 = (bf16[1024,128]{1,0:T(8,128)(2,1)S(1)}, bf16[1024,128]{1,0:T(8,128)(2,1)S(1)}, u32[]{:S(2)}, u32[]{:S(2)}) collective-permute-start(bf16[1024,128]{1,0:T(8,128)(2,1)S(1)} %collective-permute-done.27.refs_4_), channel_id=1, source_target_pairs={{0,2},{2,0},{4,6},{6,4},{1,3},{3,1},{5,7},{7,5},{8,10},{10,8},{12,... | collective-permute-start | bytes 786440 | tf_op jit(solution)/shard_map/ppermute | solution.py:366
  98.6 13.8 %collective-permute-start.30 = (bf16[1024,128]{1,0:T(8,128)(2,1)S(1)}, bf16[1024,128]{1,0:T(8,128)(2,1)S(1)}, u32[]{:S(2)}, u32[]{:S(2)}) collective-permute-start(bf16[1024,128]{1,0:T(8,128)(2,1)S(1)} %collective-permute-done.26.refs_3_), channel_id=1, source_target_pairs={{0,4},{2,6},{4,0},{6,2},{1,5},{3,7},{5,1},{7,3},{8,12},{10,14},{12... | collective-permute-start | bytes 786440 | tf_op jit(solution)/shard_map/ppermute | solution.py:366
  135.0 31.9 %collective-permute-start.34 = (bf16[256,1024]{1,0:T(8,128)(2,1)S(1)}, bf16[256,1024]{1,0:T(8,128)(2,1)S(1)}, u32[]{:S(2)}, u32[]{:S(2)}) collective-permute-start(bf16[256,1024]{1,0:T(8,128)(2,1)S(1)} %add_convert_fusion), channel_id=1, source_target_pairs={{0,8},{8,0},{16,24},{24,16},{1,9},{9,1},{17,25},{25,17},{2,10},{10... | collective-permute-start | bytes 1572872 | tf_op jit(solution)/shard_map/ppermute | solution.py:366
  142.1 14.6 %collective-permute-start.40 = (bf16[128,1024]{1,0:T(8,128)(2,1)S(1)}, bf16[128,1024]{1,0:T(8,128)(2,1)S(1)}, u32[]{:S(2)}, u32[]{:S(2)}) collective-permute-start(bf16[128,1024]{1,0:T(8,128)(2,1)S(1)} %add_convert_fusion.2), channel_id=1, source_target_pairs={{0,16},{8,24},{16,0},{24,8},{1,17},{9,25},{17,1},{25,9},{2,18},{10... | collective-permute-start | bytes 786440 | tf_op jit(solution)/shard_map/ppermute | solution.py:366
  142.4 24.4 %collective-permute-start.37 = (bf16[128,1024]{1,0:T(8,128)(2,1)S(1)}, bf16[128,1024]{1,0:T(8,128)(2,1)S(1)}, u32[]{:S(2)}, u32[]{:S(2)}) collective-permute-start(bf16[128,1024]{1,0:T(8,128)(2,1)S(1)} %add_convert_fusion.5), channel_id=1, source_target_pairs={{0,16},{8,24},{16,0},{24,8},{1,17},{9,25},{17,1},{25,9},{2,18},{10... | collective-permute-start | bytes 786440 | tf_op jit(solution)/shard_map/ppermute | solution.py:366
  (26 other events, 277.4 us)

commit v6 on v5

--- a/solution.py
+++ b/solution.py
@@ -443,18 +443,22 @@
 
     size = channels // 2
 
-    def rows_of(sources, targets):
-        sp = lax.axis_index("sp")
-        return [
-            (source.at[tiles(sp ^ j, size)], targets[j].at[tiles(i, size)])
-            for j in range(n_sp)
-            for i, source in enumerate(sources)
-        ]
-
-    pieces_out = move(
-        rows_of, [((channels, shard), low)] * n_sp, 2 * n_sp, out_pool, out_heads,
-        limit=WHOLE_VMEM,
-    )
+    def rows_of(steps):
+        def pairs(sources, targets):
+            sp = lax.axis_index("sp")
+            return [
+                (source.at[tiles(sp ^ j, size)], target.at[tiles(i, size)])
+                for j, target in zip(steps, targets, strict=True)
+                for i, source in enumerate(sources)
+            ]
+
+        return move(
+            pairs, [((channels, shard), low)] * len(steps), 2 * len(steps),
+            out_pool, out_heads, limit=WHOLE_VMEM,
+        )
+
+    pieces_out = rows_of((3, 2)) + rows_of((1, 0))
+    pieces_out = pieces_out[::-1]
     far_out = [pieces_out[0]] + [swap(pieces_out[j], "sp", j) for j in range(1, n_sp)]
 
     def bundle_out(sources, targets):

time: 168 us -> 168 us (level)
    pallas_call x15 -> x16, Pallas kernels: 22.1 us -> 23.5 us  [call(): pl.pallas_call(kernel, out_shape=[jax.ShapeDtypeStruct(shape, dtype) for...]
  transfers between devices with their start and end apart: 41 -> 41, of which waited for: 15 -> 15; matrix products, arithmetic and copies ran while one was open for 1% -> 1% of each run, Pallas kernels for 10% -> 11%
where the time goes in v6:
time: 168 us
  waiting for transfers between devices  96.9 us (58%)
  starting transfers between devices  43.6 us (26%)
  Pallas kernels  23.5 us (14%)
  other arithmetic  3.41 us (2%)
    ppermute x41, waiting for transfers between devices, swap(): lax.ppermute(value, axis, [(i, i ^ bits) for i in range(lax.axis_size(axi...  96.9 us
    ppermute x41, starting transfers between devices, swap(): lax.ppermute(value, axis, [(i, i ^ bits) for i in range(lax.axis_size(axi...  43.6 us
    pallas_call x16, Pallas kernels, call(): pl.pallas_call(kernel, out_shape=[jax.ShapeDtypeStruct(shape, dtype) for...  23.5 us
  transfers between devices with their start and end apart: 41, of which 15 were waited for; matrix products, arithmetic and copies ran while one was open for 1% of the time, Pallas kernels for 11%

profile of v6, /device:TPU:0, one launch (start us, length us, event | category | flops | bytes accessed | tf_op | source)
XLA Modules:
  0.0 168.0 jit_solution(16012098947695827871)
XLA Ops:
  0.0 2.4 %shard_map.127 = (bf16[128,1024]{1,0:T(8,128)(2,1)}, bf16[128,1024]{1,0:T(8,128)(2,1)}, bf16[128,1024]{1,0:T(8,128)(2,1)}, bf16[128,1024]{1,0:T(8,128)(2,1)}) custom-call(bf16[128,1024]{1,0:T(8,128)(2,1)} %refs_0_.3, bf16[128,1024]{1,0:T(8,128)(2,1)} %refs_1_.3, bf16[128,1024]{1,0:T(8,128)(2,1)} %refs_2_.2, bf16[128,1024]{1,0:T(8,128)(2,1)} %refs_3_.2), custom_call_target="tpu_custom_call" | custom-call | bytes 2097152 | tf_op jit(solution)/shard_map/pallas_call | solution.py:204
  2.4 3.1 %collective-permute-start.3 = (bf16[128,1024]{1,0:T(8,128)(2,1)}, bf16[128,1024]{1,0:T(8,128)(2,1)S(1)}, u32[]{:S(2)}, u32[]{:S(2)}) collective-permute-start(bf16[128,1024]{1,0:T(8,128)(2,1)} %get-tuple-element.32), channel_id=1, source_target_pairs={{0,8},{8,0},{16,24},{24,16},{1,9},{9,1},{17,25},{25,17},{2,10},{10... | collective-permute-start | bytes 786440 | tf_op jit(solution)/shard_map/ppermute | solution.py:366
  5.6 2.6 %collective-permute-start.4 = (bf16[128,1024]{1,0:T(8,128)(2,1)}, bf16[128,1024]{1,0:T(8,128)(2,1)S(1)}, u32[]{:S(2)}, u32[]{:S(2)}) collective-permute-start(bf16[128,1024]{1,0:T(8,128)(2,1)} %get-tuple-element.33), channel_id=1, source_target_pairs={{0,16},{8,24},{16,0},{24,8},{1,17},{9,25},{17,1},{25,9},{2,18},{10... | collective-permute-start | bytes 786440 | tf_op jit(solution)/shard_map/ppermute | solution.py:366
  12.5 3.6 %collective-permute-start.23 = (bf16[512,128]{1,0:T(8,128)(2,1)}, bf16[512,128]{1,0:T(8,128)(2,1)S(1)}, u32[]{:S(2)}, u32[]{:S(2)}) collective-permute-start(bf16[512,128]{1,0:T(8,128)(2,1)} %get-tuple-element.39), channel_id=1, source_target_pairs={{0,16},{8,24},{16,0},{24,8},{1,17},{9,25},{17,1},{25,9},{2,18},{10... | collective-permute-start | bytes 393224 | tf_op jit(solution)/shard_map/ppermute | solution.py:366
  16.4 10.4 %collective-permute-done.22.refs_1_ = bf16[512,128]{1,0:T(8,128)(2,1)S(1)} collective-permute-done((bf16[512,128]{1,0:T(8,128)(2,1)}, bf16[512,128]{1,0:T(8,128)(2,1)S(1)}, u32[]{:S(2)}, u32[]{:S(2)}) %collective-permute-start.22) | collective-permute-done | bytes 131104 | tf_op jit(solution)/shard_map/ppermute | solution.py:366
  28.2 8.8 %collective-permute-done.23.refs_2_ = bf16[512,128]{1,0:T(8,128)(2,1)S(1)} collective-permute-done((bf16[512,128]{1,0:T(8,128)(2,1)}, bf16[512,128]{1,0:T(8,128)(2,1)S(1)}, u32[]{:S(2)}, u32[]{:S(2)}) %collective-permute-start.23) | collective-permute-done | bytes 131104 | tf_op jit(solution)/shard_map/ppermute | solution.py:366
  37.0 2.9 %collective-permute-start.24 = (bf16[512,128]{1,0:T(8,128)(2,1)}, bf16[512,128]{1,0:T(8,128)(2,1)S(1)}, u32[]{:S(2)}, u32[]{:S(2)}) collective-permute-start(bf16[512,128]{1,0:T(8,128)(2,1)} %get-tuple-element.40), channel_id=1, source_target_pairs={{0,24},{8,16},{16,8},{24,0},{1,25},{9,17},{17,9},{25,1},{2,26},{10... | collective-permute-start | bytes 393224 | tf_op jit(solution)/shard_map/ppermute | solution.py:366
  41.4 2.6 %collective-permute-done.24.refs_3_ = bf16[512,128]{1,0:T(8,128)(2,1)S(1)} collective-permute-done((bf16[512,128]{1,0:T(8,128)(2,1)}, bf16[512,128]{1,0:T(8,128)(2,1)S(1)}, u32[]{:S(2)}, u32[]{:S(2)}) %collective-permute-start.24) | collective-permute-done | bytes 131104 | tf_op jit(solution)/shard_map/ppermute | solution.py:366
  47.3 2.8 %collective-permute-start.15 = (bf16[64,2048]{1,0:T(8,128)(2,1)S(1)}, bf16[64,2048]{1,0:T(8,128)(2,1)S(1)}, u32[]{:S(2)}, u32[]{:S(2)}) collective-permute-start(bf16[64,2048]{1,0:T(8,128)(2,1)S(1)} %get-tuple-element.59), channel_id=1, source_target_pairs={{0,16},{8,24},{16,0},{24,8},{1,17},{9,25},{17,1},{25,9},{2,18},{10... | collective-permute-start | bytes 786440 | tf_op jit(solution)/shard_map/ppermute | solution.py:366
  51.6 6.2 %collective-permute-done.1.refs_2_ = bf16[128,1024]{1,0:T(8,128)(2,1)S(1)} collective-permute-done((bf16[128,1024]{1,0:T(8,128)(2,1)S(1)}, bf16[128,1024]{1,0:T(8,128)(2,1)S(1)}, u32[]{:S(2)}, u32[]{:S(2)}) %collective-permute-start.1) | collective-permute-done | bytes 262176 | tf_op jit(solution)/shard_map/ppermute | solution.py:366
  59.9 4.5 %collective-permute-done.14.refs_0_ = bf16[64,2048]{1,0:T(8,128)(2,1)S(1)} collective-permute-done((bf16[64,2048]{1,0:T(8,128)(2,1)S(1)}, bf16[64,2048]{1,0:T(8,128)(2,1)S(1)}, u32[]{:S(2)}, u32[]{:S(2)}) %collective-permute-start.14) | collective-permute-done | bytes 262176 | tf_op jit(solution)/shard_map/ppermute | solution.py:366
  65.9 4.0 %collective-permute-done.15.refs_1_ = bf16[64,2048]{1,0:T(8,128)(2,1)S(1)} collective-permute-done((bf16[64,2048]{1,0:T(8,128)(2,1)S(1)}, bf16[64,2048]{1,0:T(8,128)(2,1)S(1)}, u32[]{:S(2)}, u32[]{:S(2)}) %collective-permute-start.15) | collective-permute-done | bytes 262176 | tf_op jit(solution)/shard_map/ppermute | solution.py:366
  69.9 2.0 %collective-permute-start.19 = (bf16[64,2048]{1,0:T(8,128)(2,1)S(1)}, bf16[64,2048]{1,0:T(8,128)(2,1)S(1)}, u32[]{:S(2)}, u32[]{:S(2)}) collective-permute-start(bf16[64,2048]{1,0:T(8,128)(2,1)S(1)} %collective-permute-done.15.refs_1_), channel_id=1, source_target_pairs={{0,8},{8,0},{16,24},{24,16},{1,9},{9,1},{17,25},{25,17},{2,10},{10... | collective-permute-start | bytes 786440 | tf_op jit(solution)/shard_map/ppermute | solution.py:366
  74.3 4.8 %collective-permute-done.18.refs_0_ = bf16[64,2048]{1,0:T(8,128)(2,1)S(1)} collective-permute-done((bf16[64,2048]{1,0:T(8,128)(2,1)S(1)}, bf16[64,2048]{1,0:T(8,128)(2,1)S(1)}, u32[]{:S(2)}, u32[]{:S(2)}) %collective-permute-start.18) | collective-permute-done | bytes 262176 | tf_op jit(solution)/shard_map/ppermute | solution.py:366
  79.7 5.1 %collective-permute-done.19.refs_1_ = bf16[64,2048]{1,0:T(8,128)(2,1)S(1)} collective-permute-done((bf16[64,2048]{1,0:T(8,128)(2,1)S(1)}, bf16[64,2048]{1,0:T(8,128)(2,1)S(1)}, u32[]{:S(2)}, u32[]{:S(2)}) %collective-permute-start.19) | collective-permute-done | bytes 262176 | tf_op jit(solution)/shard_map/ppermute | solution.py:366
  86.3 8.8 %collective-permute-done.12.refs_0_ = bf16[128,2048]{1,0:T(8,128)(2,1)S(1)} collective-permute-done((bf16[128,2048]{1,0:T(8,128)(2,1)S(1)}, bf16[128,2048]{1,0:T(8,128)(2,1)S(1)}, u32[]{:S(2)}, u32[]{:S(2)}) %collective-permute-start.12) | collective-permute-done | bytes 524320 | tf_op jit(solution)/shard_map/ppermute | solution.py:366
  99.1 13.1 %collective-permute-done.29.refs_6_ = bf16[1024,128]{1,0:T(8,128)(2,1)S(1)} collective-permute-done((bf16[1024,128]{1,0:T(8,128)(2,1)S(1)}, bf16[1024,128]{1,0:T(8,128)(2,1)S(1)}, u32[]{:S(2)}, u32[]{:S(2)}) %collective-permute-start.29) | collective-permute-done | bytes 262176 | tf_op jit(solution)/shard_map/ppermute | solution.py:366
  124.1 2.7 %shard_map.141 = (bf16[256,1024]{1,0:T(8,128)(2,1)S(1)}, f32[256,1024]{1,0:T(8,128)S(1)}) custom-call(bf16[256,1024]{1,0:T(8,128)(2,1)S(1)} %shard_map.130.refs_0_, bf16[256,1024]{1,0:T(8,128)(2,1)S(1)} %shard_map.131.refs_1_, bf16[256,1024]{1,0:T(8,128)(2,1)S(1)} %shard_map.132.refs_2_, bf16[256,1024]{1,0:T(8,128)(2,1)S(1)} %shard_map.133.refs_3_, ...), custom_call_target="tpu_custom_call" | custom-call | flops 805306368 | bytes 4194304 | tf_op jit(solution)/shard_map/pallas_call | solution.py:204
  127.5 2.5 %shard_map.142 = (bf16[256,1024]{1,0:T(8,128)(2,1)S(1)}, f32[256,1024]{1,0:T(8,128)S(1)}) custom-call(bf16[256,1024]{1,0:T(8,128)(2,1)S(1)} %shard_map.130.refs_0_, bf16[256,1024]{1,0:T(8,128)(2,1)S(1)} %shard_map.131.refs_1_, bf16[256,1024]{1,0:T(8,128)(2,1)S(1)} %shard_map.132.refs_2_, bf16[256,1024]{1,0:T(8,128)(2,1)S(1)} %shard_map.133.refs_3_, ...), custom_call_target="tpu_custom_call" | custom-call | flops 805306368 | bytes 4194304 | tf_op jit(solution)/shard_map/pallas_call | solution.py:204
  132.0 2.5 %shard_map.140 = (bf16[256,1024]{1,0:T(8,128)(2,1)S(1)}, f32[256,1024]{1,0:T(8,128)S(1)}) custom-call(bf16[256,1024]{1,0:T(8,128)(2,1)S(1)} %shard_map.130.refs_0_, bf16[256,1024]{1,0:T(8,128)(2,1)S(1)} %shard_map.131.refs_1_, bf16[256,1024]{1,0:T(8,128)(2,1)S(1)} %shard_map.132.refs_2_, bf16[256,1024]{1,0:T(8,128)(2,1)S(1)} %shard_map.133.refs_3_, ...), custom_call_target="tpu_custom_call" | custom-call | flops 805306368 | bytes 4194304 | tf_op jit(solution)/shard_map/pallas_call | solution.py:204
  136.5 5.5 %collective-permute-done.39 = bf16[128,1024]{1,0:T(8,128)(2,1)S(1)} collective-permute-done((bf16[128,1024]{1,0:T(8,128)(2,1)S(1)}, bf16[128,1024]{1,0:T(8,128)(2,1)S(1)}, u32[]{:S(2)}, u32[]{:S(2)}) %collective-permute-start.39) | collective-permute-done | bytes 262176 | tf_op jit(solution)/shard_map/ppermute | solution.py:366
  142.4 2.7 %collective-permute-start.37 = (bf16[128,1024]{1,0:T(8,128)(2,1)S(1)}, bf16[128,1024]{1,0:T(8,128)(2,1)S(1)}, u32[]{:S(2)}, u32[]{:S(2)}) collective-permute-start(bf16[128,1024]{1,0:T(8,128)(2,1)S(1)} %add_convert_fusion.5), channel_id=1, source_target_pairs={{0,16},{8,24},{16,0},{24,8},{1,17},{9,25},{17,1},{25,9},{2,18},{10... | collective-permute-start | bytes 786440 | tf_op jit(solution)/shard_map/ppermute | solution.py:366
  145.1 11.6 %collective-permute-done.40 = bf16[128,1024]{1,0:T(8,128)(2,1)S(1)} collective-permute-done((bf16[128,1024]{1,0:T(8,128)(2,1)S(1)}, bf16[128,1024]{1,0:T(8,128)(2,1)S(1)}, u32[]{:S(2)}, u32[]{:S(2)}) %collective-permute-start.40) | collective-permute-done | bytes 262176 | tf_op jit(solution)/shard_map/ppermute | solution.py:366
  156.7 10.1 %collective-permute-done.37 = bf16[128,1024]{1,0:T(8,128)(2,1)S(1)} collective-permute-done((bf16[128,1024]{1,0:T(8,128)(2,1)S(1)}, bf16[128,1024]{1,0:T(8,128)(2,1)S(1)}, u32[]{:S(2)}, u32[]{:S(2)}) %collective-permute-start.37) | collective-permute-done | bytes 262176 | tf_op jit(solution)/shard_map/ppermute | solution.py:366
  (104 shorter events, 42.2 us)
Async XLA Ops:
  2.4 43.2 %collective-permute-start.3 = (bf16[128,1024]{1,0:T(8,128)(2,1)}, bf16[128,1024]{1,0:T(8,128)(2,1)S(1)}, u32[]{:S(2)}, u32[]{:S(2)}) collective-permute-start(bf16[128,1024]{1,0:T(8,128)(2,1)} %get-tuple-element.32), channel_id=1, source_target_pairs={{0,8},{8,0},{16,24},{24,16},{1,9},{9,1},{17,25},{25,17},{2,10},{10... | collective-permute-start | bytes 786440 | tf_op jit(solution)/shard_map/ppermute | solution.py:366
  5.6 41.6 %collective-permute-start.4 = (bf16[128,1024]{1,0:T(8,128)(2,1)}, bf16[128,1024]{1,0:T(8,128)(2,1)S(1)}, u32[]{:S(2)}, u32[]{:S(2)}) collective-permute-start(bf16[128,1024]{1,0:T(8,128)(2,1)} %get-tuple-element.33), channel_id=1, source_target_pairs={{0,16},{8,24},{16,0},{24,8},{1,17},{9,25},{17,1},{25,9},{2,18},{10... | collective-permute-start | bytes 786440 | tf_op jit(solution)/shard_map/ppermute | solution.py:366
  8.2 39.2 %collective-permute-start.5 = (bf16[128,1024]{1,0:T(8,128)(2,1)}, bf16[128,1024]{1,0:T(8,128)(2,1)S(1)}, u32[]{:S(2)}, u32[]{:S(2)}) collective-permute-start(bf16[128,1024]{1,0:T(8,128)(2,1)} %get-tuple-element.34), channel_id=1, source_target_pairs={{0,24},{8,16},{16,8},{24,0},{1,25},{9,17},{17,9},{25,1},{2,26},{10... | collective-permute-start | bytes 786440 | tf_op jit(solution)/shard_map/ppermute | solution.py:366
  9.8 16.9 %collective-permute-start.22 = (bf16[512,128]{1,0:T(8,128)(2,1)}, bf16[512,128]{1,0:T(8,128)(2,1)S(1)}, u32[]{:S(2)}, u32[]{:S(2)}) collective-permute-start(bf16[512,128]{1,0:T(8,128)(2,1)} %get-tuple-element.38), channel_id=1, source_target_pairs={{0,8},{8,0},{16,24},{24,16},{1,9},{9,1},{17,25},{25,17},{2,10},{10... | collective-permute-start | bytes 393224 | tf_op jit(solution)/shard_map/ppermute | solution.py:366
  12.5 24.5 %collective-permute-start.23 = (bf16[512,128]{1,0:T(8,128)(2,1)}, bf16[512,128]{1,0:T(8,128)(2,1)S(1)}, u32[]{:S(2)}, u32[]{:S(2)}) collective-permute-start(bf16[512,128]{1,0:T(8,128)(2,1)} %get-tuple-element.39), channel_id=1, source_target_pairs={{0,16},{8,24},{16,0},{24,8},{1,17},{9,25},{17,1},{25,9},{2,18},{10... | collective-permute-start | bytes 393224 | tf_op jit(solution)/shard_map/ppermute | solution.py:366
  26.7 23.4 %collective-permute-start = (bf16[128,1024]{1,0:T(8,128)(2,1)S(1)}, bf16[128,1024]{1,0:T(8,128)(2,1)S(1)}, u32[]{:S(2)}, u32[]{:S(2)}) collective-permute-start(bf16[128,1024]{1,0:T(8,128)(2,1)S(1)} %copy-done.2), channel_id=1, source_target_pairs={{0,2},{2,0},{4,6},{6,4},{1,3},{3,1},{5,7},{7,5},{8,10},{10,8},{12,... | collective-permute-start | bytes 786440 | tf_op jit(solution)/shard_map/ppermute | solution.py:366
  47.2 17.2 %collective-permute-start.14 = (bf16[64,2048]{1,0:T(8,128)(2,1)S(1)}, bf16[64,2048]{1,0:T(8,128)(2,1)S(1)}, u32[]{:S(2)}, u32[]{:S(2)}) collective-permute-start(bf16[64,2048]{1,0:T(8,128)(2,1)S(1)} %get-tuple-element.60), channel_id=1, source_target_pairs={{0,16},{8,24},{16,0},{24,8},{1,17},{9,25},{17,1},{25,9},{2,18},{10... | collective-permute-start | bytes 786440 | tf_op jit(solution)/shard_map/ppermute | solution.py:366
  47.3 22.6 %collective-permute-start.15 = (bf16[64,2048]{1,0:T(8,128)(2,1)S(1)}, bf16[64,2048]{1,0:T(8,128)(2,1)S(1)}, u32[]{:S(2)}, u32[]{:S(2)}) collective-permute-start(bf16[64,2048]{1,0:T(8,128)(2,1)S(1)} %get-tuple-element.59), channel_id=1, source_target_pairs={{0,16},{8,24},{16,0},{24,8},{1,17},{9,25},{17,1},{25,9},{2,18},{10... | collective-permute-start | bytes 786440 | tf_op jit(solution)/shard_map/ppermute | solution.py:366
  50.1 19.8 %collective-permute-start.27 = (bf16[1024,128]{1,0:T(8,128)(2,1)S(1)}, bf16[1024,128]{1,0:T(8,128)(2,1)S(1)}, u32[]{:S(2)}, u32[]{:S(2)}) collective-permute-start(bf16[1024,128]{1,0:T(8,128)(2,1)S(1)} %get-tuple-element.41.refs_0_), channel_id=1, source_target_pairs={{0,4},{2,6},{4,0},{6,2},{1,5},{3,7},{5,1},{7,3},{8,12},{10,14},{12... | collective-permute-start | bytes 786440 | tf_op jit(solution)/shard_map/ppermute | solution.py:366
  57.9 14.1 %collective-permute-start.26 = (bf16[1024,128]{1,0:T(8,128)(2,1)S(1)}, bf16[1024,128]{1,0:T(8,128)(2,1)S(1)}, u32[]{:S(2)}, u32[]{:S(2)}) collective-permute-start(bf16[1024,128]{1,0:T(8,128)(2,1)S(1)} %get-tuple-element.42.refs_1_), channel_id=1, source_target_pairs={{0,2},{2,0},{4,6},{6,4},{1,3},{3,1},{5,7},{7,5},{8,10},{10,8},{12,... | collective-permute-start | bytes 786440 | tf_op jit(solution)/shard_map/ppermute | solution.py:366
  69.9 14.8 %collective-permute-start.19 = (bf16[64,2048]{1,0:T(8,128)(2,1)S(1)}, bf16[64,2048]{1,0:T(8,128)(2,1)S(1)}, u32[]{:S(2)}, u32[]{:S(2)}) collective-permute-start(bf16[64,2048]{1,0:T(8,128)(2,1)S(1)} %collective-permute-done.15.refs_1_), channel_id=1, source_target_pairs={{0,8},{8,0},{16,24},{24,16},{1,9},{9,1},{17,25},{25,17},{2,10},{10... | collective-permute-start | bytes 786440 | tf_op jit(solution)/shard_map/ppermute | solution.py:366
  72.0 23.0 %collective-permute-start.12 = (bf16[128,2048]{1,0:T(8,128)(2,1)S(1)}, bf16[128,2048]{1,0:T(8,128)(2,1)S(1)}, u32[]{:S(2)}, u32[]{:S(2)}) collective-permute-start(bf16[128,2048]{1,0:T(8,128)(2,1)S(1)} %constant_dynamic-slice_fusion.2), channel_id=1, source_target_pairs={{0,8},{8,0},{16,24},{24,16},{1,9},{9,1},{17,25},{25,17},{2,10},{10... | collective-permute-start | bytes 1572872 | tf_op jit(solution)/shard_map/ppermute | solution.py:366
  72.2 22.9 %collective-permute-start.8 = (bf16[192,1024]{1,0:T(8,128)(2,1)S(1)}, bf16[192,1024]{1,0:T(8,128)(2,1)S(1)}, u32[]{:S(2)}, u32[]{:S(2)}) collective-permute-start(bf16[192,1024]{1,0:T(8,128)(2,1)S(1)} %get-tuple-element.35.refs_4_), channel_id=1, source_target_pairs={{0,4},{2,6},{4,0},{6,2},{1,5},{3,7},{5,1},{7,3},{8,12},{10,14},{12... | collective-permute-start | bytes 1179656 | tf_op jit(solution)/shard_map/ppermute | solution.py:366
  73.8 21.8 %collective-permute-start.7 = (bf16[192,1024]{1,0:T(8,128)(2,1)S(1)}, bf16[192,1024]{1,0:T(8,128)(2,1)S(1)}, u32[]{:S(2)}, u32[]{:S(2)}) collective-permute-start(bf16[192,1024]{1,0:T(8,128)(2,1)S(1)} %get-tuple-element.36.refs_5_), channel_id=1, source_target_pairs={{0,2},{2,0},{4,6},{6,4},{1,3},{3,1},{5,7},{7,5},{8,10},{10,8},{12,... | collective-permute-start | bytes 1179656 | tf_op jit(solution)/shard_map/ppermute | solution.py:366
  79.1 18.0 %collective-permute-start.6 = (bf16[192,1024]{1,0:T(8,128)(2,1)S(1)}, bf16[192,1024]{1,0:T(8,128)(2,1)S(1)}, u32[]{:S(2)}, u32[]{:S(2)}) collective-permute-start(bf16[192,1024]{1,0:T(8,128)(2,1)S(1)} %get-tuple-element.35.refs_4_), channel_id=1, source_target_pairs={{0,2},{2,0},{4,6},{6,4},{1,3},{3,1},{5,7},{7,5},{8,10},{10,8},{12,... | collective-permute-start | bytes 1179656 | tf_op jit(solution)/shard_map/ppermute | solution.py:366
  84.7 13.9 %collective-permute-start.9 = (bf16[192,1024]{1,0:T(8,128)(2,1)S(1)}, bf16[192,1024]{1,0:T(8,128)(2,1)S(1)}, u32[]{:S(2)}, u32[]{:S(2)}) collective-permute-start(bf16[192,1024]{1,0:T(8,128)(2,1)S(1)} %get-tuple-element.36.refs_5_), channel_id=1, source_target_pairs={{0,4},{2,6},{4,0},{6,2},{1,5},{3,7},{5,1},{7,3},{8,12},{10,14},{12... | collective-permute-start | bytes 1179656 | tf_op jit(solution)/shard_map/ppermute | solution.py:366
  95.0 20.7 %collective-permute-start.13 = (bf16[128,2048]{1,0:T(8,128)(2,1)S(1)}, bf16[128,2048]{1,0:T(8,128)(2,1)S(1)}, u32[]{:S(2)}, u32[]{:S(2)}) collective-permute-start(bf16[128,2048]{1,0:T(8,128)(2,1)S(1)} %collective-permute-done.12.refs_0_), channel_id=1, source_target_pairs={{0,1},{1,0},{2,3},{3,2},{4,5},{5,4},{6,7},{7,6},{8,9},{9,8},{10,11... | collective-permute-start | bytes 1572872 | tf_op jit(solution)/shard_map/ppermute | solution.py:366
  95.0 18.3 %collective-permute-start.10 = (bf16[192,1024]{1,0:T(8,128)(2,1)S(1)}, bf16[192,1024]{1,0:T(8,128)(2,1)S(1)}, u32[]{:S(2)}, u32[]{:S(2)}) collective-permute-start(bf16[192,1024]{1,0:T(8,128)(2,1)S(1)} %collective-permute-done.8.refs_8_), channel_id=1, source_target_pairs={{0,2},{2,0},{4,6},{6,4},{1,3},{3,1},{5,7},{7,5},{8,10},{10,8},{12,... | collective-permute-start | bytes 1179656 | tf_op jit(solution)/shard_map/ppermute | solution.py:366
  95.6 18.1 %collective-permute-start.11 = (bf16[192,1024]{1,0:T(8,128)(2,1)S(1)}, bf16[192,1024]{1,0:T(8,128)(2,1)S(1)}, u32[]{:S(2)}, u32[]{:S(2)}) collective-permute-start(bf16[192,1024]{1,0:T(8,128)(2,1)S(1)} %collective-permute-done.7.refs_7_), channel_id=1, source_target_pairs={{0,4},{2,6},{4,0},{6,2},{1,5},{3,7},{5,1},{7,3},{8,12},{10,14},{12... | collective-permute-start | bytes 1179656 | tf_op jit(solution)/shard_map/ppermute | solution.py:366
  97.1 15.1 %collective-permute-start.29 = (bf16[1024,128]{1,0:T(8,128)(2,1)S(1)}, bf16[1024,128]{1,0:T(8,128)(2,1)S(1)}, u32[]{:S(2)}, u32[]{:S(2)}) collective-permute-start(bf16[1024,128]{1,0:T(8,128)(2,1)S(1)} %collective-permute-done.27.refs_4_), channel_id=1, source_target_pairs={{0,2},{2,0},{4,6},{6,4},{1,3},{3,1},{5,7},{7,5},{8,10},{10,8},{12,... | collective-permute-start | bytes 786440 | tf_op jit(solution)/shard_map/ppermute | solution.py:366
  98.6 13.8 %collective-permute-start.30 = (bf16[1024,128]{1,0:T(8,128)(2,1)S(1)}, bf16[1024,128]{1,0:T(8,128)(2,1)S(1)}, u32[]{:S(2)}, u32[]{:S(2)}) collective-permute-start(bf16[1024,128]{1,0:T(8,128)(2,1)S(1)} %collective-permute-done.26.refs_3_), channel_id=1, source_target_pairs={{0,4},{2,6},{4,0},{6,2},{1,5},{3,7},{5,1},{7,3},{8,12},{10,14},{12... | collective-permute-start | bytes 786440 | tf_op jit(solution)/shard_map/ppermute | solution.py:366
  135.0 31.9 %collective-permute-start.34 = (bf16[256,1024]{1,0:T(8,128)(2,1)S(1)}, bf16[256,1024]{1,0:T(8,128)(2,1)S(1)}, u32[]{:S(2)}, u32[]{:S(2)}) collective-permute-start(bf16[256,1024]{1,0:T(8,128)(2,1)S(1)} %add_convert_fusion), channel_id=1, source_target_pairs={{0,8},{8,0},{16,24},{24,16},{1,9},{9,1},{17,25},{25,17},{2,10},{10... | collective-permute-start | bytes 1572872 | tf_op jit(solution)/shard_map/ppermute | solution.py:366
  142.1 14.6 %collective-permute-start.40 = (bf16[128,1024]{1,0:T(8,128)(2,1)S(1)}, bf16[128,1024]{1,0:T(8,128)(2,1)S(1)}, u32[]{:S(2)}, u32[]{:S(2)}) collective-permute-start(bf16[128,1024]{1,0:T(8,128)(2,1)S(1)} %add_convert_fusion.2), channel_id=1, source_target_pairs={{0,16},{8,24},{16,0},{24,8},{1,17},{9,25},{17,1},{25,9},{2,18},{10... | collective-permute-start | bytes 786440 | tf_op jit(solution)/shard_map/ppermute | solution.py:366
  142.4 24.5 %collective-permute-start.37 = (bf16[128,1024]{1,0:T(8,128)(2,1)S(1)}, bf16[128,1024]{1,0:T(8,128)(2,1)S(1)}, u32[]{:S(2)}, u32[]{:S(2)}) collective-permute-start(bf16[128,1024]{1,0:T(8,128)(2,1)S(1)} %add_convert_fusion.5), channel_id=1, source_target_pairs={{0,16},{8,24},{16,0},{24,8},{1,17},{9,25},{17,1},{25,9},{2,18},{10... | collective-permute-start | bytes 786440 | tf_op jit(solution)/shard_map/ppermute | solution.py:366
  (26 other events, 260.1 us)
